TPU v7x, 512 devices: a 4x2x32 block of a 4x8x32 slice. The times are simulated.
512 devices in a mesh: grp: 2 (over y), sp: 64 (over z, core), tp: 4 (over x).
Axes of the slice: x: 4, y: 2, z: 32, core: 2. Of those that a mesh axis runs over, the one named last changes fastest.
The devices are a block of a 4x8x32 slice.
Arguments:
- tokens: bfloat16 [65536, 2048], P(('grp', 'sp', 'tp')), parts along dimension 0, may hold values from -6 to 6
- norm_gain: bfloat16 [2048], replicated, may hold values from 0.099609375 to 1.8984375
- conv_outer_weight: bfloat16 [2048, 1024], P('sp', 'tp'), may hold values from -0.125 to 0.125
- conv_inner_weight: bfloat16 [2048, 1024], P('sp', 'tp'), may hold values from -0.125 to 0.125
- conv_input_weight: bfloat16 [2048, 1024], P('sp', 'tp'), may hold values from -0.125 to 0.125
- query_matrix: bfloat16 [2048, 1024], P('sp', 'tp'), may hold values from -0.125 to 0.125
- key_weight: bfloat16 [2048, 1024], P('sp', 'tp'), may hold values from -0.125 to 0.125
- value_weight: bfloat16 [2048, 1024], P('sp', 'tp'), may hold values from -0.125 to 0.125
- gate_weight: bfloat16 [2048, 1024], P('sp', 'tp'), may hold values from -0.125 to 0.125
- conv_taps: bfloat16 [3, 1024], P(None, 'tp'), may hold values from -3.5 to 3.5
- conv_out_weight: bfloat16 [1024, 2048], P('tp', 'sp'), may hold values from -0.125 to 0.125
- ret_out_weight: bfloat16 [1024, 2048], P('tp', 'sp'), may hold values from -0.125 to 0.125
- log_decay: float32 [65536, 8], P(('grp', 'sp'), 'tp'), parts along dimension 0, may hold values from -0.75 to 0
Outputs:
- mixed: bfloat16 [65536, 2048], P(('grp', 'sp', 'tp')), parts along dimension 0
There are 2 independent parts, one for each index of `grp`. A program takes and returns all parts, laid end to end along the dimension named above; an argument that names none is the same for every part. Nothing has to cross between parts.
All inputs are finite; a program needn't handle non-finite values.
Results may differ from a plain program's by a relative error of at most 0.025.
Values may be sent and summed in bfloat16 or wider, within the bound.
No kernel may reach another device: no remote copies, remote signals or barrier semaphores. Data moves between devices by JAX's collectives and lax.ppermute only.
A program may use at most 64 MiB of HBM per device.

v0:
```python
import jax
import jax.numpy as jnp
from jax import lax
from jax.sharding import PartitionSpec as P

HEAD = 128
CONV_K = 3
BLOCK = 128


EPSILON = 1e-06
ROTARY_BASE = 10000.0


def joined_along(blocks, dim):
    lengths = list(blocks.shape[1:])
    lengths[dim] *= blocks.shape[0]
    return jnp.moveaxis(blocks, 0, dim).reshape(lengths)


def from_everyone(x, axis):
    copies = jnp.broadcast_to(x, (lax.axis_size(axis), *x.shape))
    return lax.all_to_all(copies, axis, split_axis=0, concat_axis=0, tiled=True)


def gather_directly(x, axis, dim):
    return joined_along(from_everyone(x, axis), dim)


def sent_together(arrays, axis, dim, along):
    both = jnp.concatenate(arrays, axis=along)
    whole, at, gathered = (lax.all_gather(both, axis, axis=dim, tiled=True), 0, [])
    for a in arrays:
        gathered.append(lax.slice_in_dim(whole, at, at + a.shape[along], axis=along))
        at += a.shape[along]
    return tuple(gathered)


def prefix_2(x, axis, join, neutral):
    place = lax.axis_index(axis)
    gathered = jax.tree.map(
        lambda a, kind: lax.all_gather(a.astype(kind), axis), x, (jnp.bfloat16, jnp.bfloat16)
    )
    state = jax.tree.map(lambda a, e: jnp.zeros_like(a) + jnp.asarray(e, a.dtype), x, neutral)

    def one(turn, state):
        return join(
            state,
            jax.tree.map(
                lambda a, own: lax.dynamic_index_in_dim(a, turn, 0, False).astype(own.dtype),
                gathered,
                x,
            ),
        )

    return lax.fori_loop(0, place, one, state)


def shifted(x, axis, by):
    count = lax.axis_size(axis)
    pairs = [(i, i + by) for i in range(count) if 0 <= i + by < count]
    return lax.ppermute(x, axis, pairs)


def rows_first(arrays, axis, dims):
    turned = [jnp.moveaxis(a, dim, 0) for a, dim in zip(arrays, dims)]
    both = jnp.concatenate([t.reshape(len(t), -1) for t in turned], axis=1)
    whole, at, gathered = (lax.all_gather(both, axis, axis=0, tiled=True), 0, [])
    for t, dim in zip(turned, dims):
        share = whole[:, at : at + t[0].size].reshape(-1, *t.shape[1:])
        gathered.append(jnp.moveaxis(share, 0, dim))
        at += t[0].size
    return tuple(gathered)


def split_up(x, dim, count):
    lengths = x.shape
    blocks = x.reshape(*lengths[:dim], count, lengths[dim] // count, *lengths[dim + 1 :])
    return jnp.moveaxis(blocks, dim, 0)


def summed_on_arrival(x, axis, dim):
    count = lax.axis_size(axis)
    blocks = lax.all_to_all(split_up(x, dim, count), axis, 0, 0, tiled=True)
    return jnp.sum(blocks.astype(jnp.float32), axis=0)


def rotate(head_data, positions):
    half_width = head_data.shape[-1] // 2
    inv_freq = ROTARY_BASE ** (-jnp.arange(half_width, dtype=jnp.float32) / half_width)
    angles = positions[:, None] * inv_freq[None, :]
    cosine = jnp.cos(angles)[:, None, :]
    sine_part = jnp.sin(angles)[:, None, :]
    first_half = head_data[..., :half_width]
    second_half = head_data[..., half_width:]
    return jnp.concatenate(
        [
            first_half * cosine - second_half * sine_part,
            second_half * cosine + first_half * sine_part,
        ],
        axis=-1,
    )


def head_norm(head_data):
    return head_data * lax.rsqrt(jnp.mean(head_data * head_data, axis=-1, keepdims=True) + EPSILON)


def combine_states(earlier, later):
    return (earlier[0] * later[0], later[0][:, None, None] * earlier[1] + later[1])


def body(
    tokens,
    norm_gain,
    conv_outer_weight,
    conv_inner_weight,
    conv_input_weight,
    query_matrix,
    key_weight,
    value_weight,
    gate_weight,
    conv_taps,
    conv_out_weight,
    ret_out_weight,
    log_decay,
):
    values32 = tokens.astype(jnp.float32)
    normed = (
        values32
        * lax.rsqrt(jnp.mean(values32 * values32, axis=-1, keepdims=True) + EPSILON)
        * norm_gain.astype(jnp.float32)
    ).astype(jnp.bfloat16)
    gathered = gather_directly(normed, "tp", 0)
    row_total = gathered.shape[0]
    whole = sent_together(
        (
            conv_outer_weight,
            conv_inner_weight,
            conv_input_weight,
            query_matrix,
            key_weight,
            value_weight,
            gate_weight,
        ),
        "sp",
        0,
        1,
    )
    projected = tuple(
        (
            jnp.dot(gathered, weight, preferred_element_type=jnp.float32).astype(jnp.bfloat16)
            for weight in whole
        )
    )
    conv_outer, conv_inner, conv_input, query_proj, key_proj, value_proj, gate_proj = projected
    heads_here = query_proj.shape[1] // HEAD
    offset = (lax.axis_index("sp") * row_total).astype(jnp.float32)
    positions = offset + jnp.arange(row_total, dtype=jnp.float32)
    head_shape = (row_total, heads_here, HEAD)
    queries = rotate(query_proj.astype(jnp.float32).reshape(head_shape), positions)
    keys_rot = rotate(key_proj.astype(jnp.float32).reshape(head_shape), positions) * HEAD ** (-0.5)
    head_values = value_proj.astype(jnp.float32).reshape(head_shape)
    block_count = row_total // BLOCK
    block_shape = (block_count, BLOCK, heads_here, HEAD)
    query_blocks = queries.reshape(block_shape)
    key_blocks = keys_rot.reshape(block_shape)
    value_blocks = head_values.reshape(block_shape)
    log_blocks = log_decay.reshape(block_count, BLOCK, heads_here)
    offsets = jnp.arange(BLOCK, dtype=jnp.int32)
    causal_mask = offsets[:, None] >= offsets[None, :]
    lower_ones = causal_mask.astype(jnp.float32)
    cumulative = jnp.einsum("ij,njh->nih", lower_ones, log_blocks)
    block_end = cumulative[:, -1, :]
    mixed_in = conv_inner.astype(jnp.float32) * conv_input.astype(jnp.float32)
    rim = shifted(mixed_in[row_total - (CONV_K - 1) :], "sp", 1)
    extended = jnp.concatenate([rim, mixed_in], axis=0)
    taps = conv_taps.astype(jnp.float32)
    conv_out = jnp.zeros(mixed_in.shape, jnp.float32)
    for tap_index in range(CONV_K):
        conv_out = conv_out + taps[tap_index][None, :] * extended[tap_index : tap_index + row_total]
    conv_branch = (conv_outer.astype(jnp.float32) * conv_out).astype(jnp.bfloat16)
    weights = jnp.exp(block_end[:, None, :] - cumulative)
    increments = jnp.einsum("njh,njhd,njhe->nhde", weights, key_blocks, value_blocks)

    def carry_on(carried, pieces):
        block_decay, increment = pieces
        return (block_decay[:, None, None] * carried + increment, carried)

    start_state = jnp.zeros((heads_here, HEAD, HEAD), jnp.float32)
    local_end, local_before = lax.scan(carry_on, start_state, (jnp.exp(block_end), increments))
    device_decay = jnp.exp(jnp.sum(block_end, axis=0))
    incoming = prefix_2(
        (device_decay, local_end),
        "sp",
        combine_states,
        (jnp.ones_like(device_decay), jnp.zeros_like(local_end)),
    )
    local_before, incoming_state = (local_before, incoming[1])
    spread = cumulative[:, :, None, :] - cumulative[:, None, :, :]
    grid_mask = causal_mask[None, :, :, None]
    decay_grid = jnp.where(grid_mask, jnp.exp(jnp.where(grid_mask, spread, 0.0)), 0.0)
    scores = jnp.einsum("nihd,njhd->nijh", query_blocks, key_blocks) * decay_grid
    within = jnp.einsum("nijh,njhe->nihe", scores, value_blocks)
    prefix = jnp.exp(jnp.cumsum(block_end, axis=0) - block_end)
    before = local_before + prefix[:, :, None, None] * incoming_state[None]
    across = jnp.einsum("nihd,nhde->nihe", query_blocks, before)
    across = across * jnp.exp(cumulative)[..., None]
    retained = (within + across).reshape(head_shape)
    ret_branch = (
        head_norm(retained).reshape(row_total, heads_here * HEAD)
        * jax.nn.silu(gate_proj.astype(jnp.float32))
    ).astype(jnp.bfloat16)
    conv_rows_weight, ret_rows_weight = rows_first((conv_out_weight, ret_out_weight), "sp", (1, 1))
    mixed = summed_on_arrival(
        (
            jnp.dot(conv_branch, conv_rows_weight, preferred_element_type=jnp.float32)
            + jnp.dot(ret_branch, ret_rows_weight, preferred_element_type=jnp.float32)
        ).astype(jnp.bfloat16),
        "tp",
        0,
    )
    return mixed.astype(jnp.bfloat16)


def solution(mesh):
    placed = (
        P(("grp", "sp", "tp"), None),
        P(),
        P("sp", "tp"),
        P("sp", "tp"),
        P("sp", "tp"),
        P("sp", "tp"),
        P("sp", "tp"),
        P("sp", "tp"),
        P("sp", "tp"),
        P(None, "tp"),
        P("tp", "sp"),
        P("tp", "sp"),
        P(("grp", "sp"), "tp"),
    )
    return jax.shard_map(
        body, mesh=mesh, in_specs=placed, out_specs=P(("grp", "sp", "tp"), None), check_vma=False
    )
```

profile of v0, /device:TPU:2017, one launch (start us, length us, event | category | flops | bytes accessed | tf_op | source)
XLA Modules:
  0.0 504.1 jit_solution(9460209912085768720)
XLA Ops:
  13.0 1.2 fusion.9
  14.2 1.2 fusion.11
  15.5 1.6 broadcast_in_dim.25
  17.1 4.4 all-to-all-start
  24.3 1.0 multiply_cosine_fusion
  25.3 21.8 %all-to-all-done = bf16[4,128,2048]{2,1,0:T(8,128)(2,1)S(1)} async-done(((bf16[4,128,2048]{2,1,0:T(8,128)(2,1)}), bf16[4,128,2048]{2,1,0:T(8,128)(2,1)S(1)}, u32[]{:S(2)}, u32[]{:S(2)}) %all-to-all-start) | async-done | bytes 2097184 | tf_op jit(solution)/shard_map/all_to_all | solution.py:23
  47.1 88.8 %all-gather.6.cloned.1.call-done = bf16[2048,1792]{1,0:T(8,128)(2,1)} async-done(((bf16[32,1792]{1,0:T(8,128)(2,1)}), bf16[2048,1792]{1,0:T(8,128)(2,1)}) %all-gather.6.cloned.1.call-update) | async-done | bytes 7340048 | tf_op jit(solution)/shard_map/all_gather | solution.py:32
  135.8 1.9 convolution_convert_fusion.3
  137.9 2.1 convolution_convert_fusion.2
  140.8 1.1 copy.96
  142.0 2.0 copy.95
  143.9 1.2 multiply_subtract_fusion.1
  146.5 5.7 %while.26 = (s32[]{:T(128)}, f32[2,128,128]{2,1,0:T(8,128)S(1)}, f32[4,2,128,128]{3,2,1,0:T(8,128)}, f32[4,2]{1,0:T(4,128)}, f32[4,2,128,128]{3,2,1,0:T(8,128)S(1)}, /*index=5*/s32[]{:T(128)}, s32[]{:T(128)}) while((s32[]{:T(128)}, f32[2,128,128]{2,1,0:T(8,128)S(1)}, f32[4,2,128,128]{3,2,1,0:T(8,128)}, f32[4,2]{1,0:T(4,128)}, ...), condition=%wide.region_2.3_spmd.clone, body=%wide.region_1.2_spmd.clone.sunk | while | flops 131075 | bytes 655492 | solution.py:191
  153.1 1.3 dynamic-slice
  155.3 92.0 %all-reduce = bf16[128]{0:T(256)(128)(2,1)S(1)} all-reduce(bf16[128]{0:T(256)(128)(2,1)S(1)} %dynamic-update-slice), channel_id=2, replica_groups=mesh['grp'=2,'sp'=64,'tp'=4] {'sp'}, use_global_device_ids=true, to_apply=%add | all-reduce | flops 128 | bytes 512
  247.6 2.0 convolution_convert_fusion.1
  249.6 1.0 copy.98
  250.7 1.0 copy.97
  251.7 1.9 fusion.7
  253.7 2.0 fusion.6
  256.5 1.3 collective-permute-start
  258.2 2.5 convolution_bitcast_fusion
  260.7 3.5 all-gather.8.cloned.1.call-done
  264.2 5.9 %fusion.17 = f32[512,2048]{1,0:T(8,128)} fusion(bf16[2048,512]{1,0:T(8,128)(2,1)} %all-gather.8.cloned.1.call-done, f32[2,256]{1,0:T(2,128)S(1)} %collective-permute-done, f32[512,256]{1,0:T(8,128)S(1)} %copy-done.7, bf16[512,2048]{1,0:T(8,128)(2,1)S(1)} %bitcast.89, bf16[2048,1792]{1,0:T(8,128)(2,1)} %all-gather.6.cloned.1.call-done, ...), kind=kOutput, calls=%fused_computation.36 | convolution fusion | flops 1075183616 | bytes 8918016 | tf_op jit(solution)/shard_map/dot_general | solution.py:217
  270.1 124.6 %all-gather.10.cloned.1.call-done = bf16[128,128,128]{2,1,0:T(8,128)(2,1)} async-done(((bf16[2,128,128]{2,1,0:T(8,128)(2,1)}), bf16[128,128,128]{2,1,0:T(8,128)(2,1)}) %all-gather.10.cloned.1.call-update) | async-done | bytes 4194320 | tf_op jit(solution)/shard_map/all_gather | solution.py:42
  394.7 61.4 %while.25 = (s32[]{:T(128)}, f32[2,128,128]{2,1,0:T(8,128)S(1)}, s32[]{:T(128)}, bf16[64,2]{1,0:T(8,128)(2,1)S(1)}, bf16[64,2,128,128]{3,2,1,0:T(8,128)(2,1)}, /*index=5*/s32[]{:T(128)}, s32[]{:T(128)}, s32[]{:T(128)}) while((s32[]{:T(128)}, f32[2,128,128]{2,1,0:T(8,128)S(1)}, s32[]{:T(128)}, bf16[64,2]{1,0:T(8,128)(2,1)S(1)}, ...), condition=%wide.region_6.7_spmd, body=%wide.region_5.6_spmd.sunk | while | flops 98311 | bytes 327835 | solution.py:56
  395.7 0.9 convert_add_fusion.2
  396.7 0.9 convert_add_fusion.2
  397.7 0.9 convert_add_fusion.2
  398.7 0.9 convert_add_fusion.2
  399.6 0.9 convert_add_fusion.2
  400.6 0.9 convert_add_fusion.2
  401.6 0.9 convert_add_fusion.2
  402.5 0.9 convert_add_fusion.2
  403.5 0.9 convert_add_fusion.2
  404.5 0.9 convert_add_fusion.2
  405.5 0.9 convert_add_fusion.2
  406.4 0.9 convert_add_fusion.2
  414.2 0.9 convert_add_fusion.2
  415.2 0.9 convert_add_fusion.2
  416.1 0.9 convert_add_fusion.2
  417.1 0.9 convert_add_fusion.2
  418.1 0.9 convert_add_fusion.2
  419.1 0.9 convert_add_fusion.2
  420.0 0.9 convert_add_fusion.2
  421.0 0.9 convert_add_fusion.2
  422.0 0.9 convert_add_fusion.2
  422.9 0.9 convert_add_fusion.2
  423.9 0.9 convert_add_fusion.2
  424.9 0.9 convert_add_fusion.2
  432.7 0.9 convert_add_fusion.2
  433.6 0.9 convert_add_fusion.2
  434.6 0.9 convert_add_fusion.2
  435.6 0.9 convert_add_fusion.2
  436.5 0.9 convert_add_fusion.2
  437.5 0.9 convert_add_fusion.2
  438.5 0.9 convert_add_fusion.2
  439.5 0.9 convert_add_fusion.2
  440.4 0.9 convert_add_fusion.2
  441.4 0.9 convert_add_fusion.2
  456.1 1.6 multiply_reduce_fusion
  458.8 6.6 %add_convert_fusion = bf16[512,2048]{1,0:T(8,128)(2,1)} fusion(f32[512,2048]{1,0:T(8,128)} %fusion.17, bf16[2048,512]{1,0:T(8,128)(2,1)} %all-gather.8.cloned.1.call-done, f32[64,8,2,128]{3,2,1,0:T(2,128)S(1)} %bitcast.97, f32[64,8,2,128]{3,2,1,0:T(2,128)S(1)} %bitcast.96, bf16[512,2048]{1,0:T(8,128)(2,1)S(1)} %bitcast.90, ...), kind=kOutput, calls=%fused_computation.6 | convolution fusion | flops 1077018624 | bytes 11534336 | tf_op jit(solution)/shard_map/dot_general | solution.py:218
  465.4 30.8 %all_to_all.10 = bf16[4,128,2048]{2,1,0:T(8,128)(2,1)S(1)} all-to-all(bf16[4,128,2048]{2,1,0:T(8,128)(2,1)} %bitcast.91), channel_id=1, replica_groups=mesh['grp'=2,'sp'=64,'tp'=4] {'tp'}, dimensions={0} | all-to-all | bytes 4194304 | tf_op jit(solution)/shard_map/all_to_all | solution.py:84
  496.2 1.3 reduce_sum.42
  (184 shorter events, 48.3 us)
Async XLA Ops:
  6.5 129.3 %all-gather.6.cloned.1.call-start = ((), (), s32[]{:S(2)}) async-start(), calls=%async_computation.2 | async-start | bytes 7454720 | tf_op jit(solution)/shard_map/all_gather | solution.py:32
  11.6 0.6 copy-start.8
  17.1 4.4 copy-start.9
  17.1 4.4 copy-start.10
  17.1 5.3 %copy-start.12 = (f32[512,2]{0,1:T(2,128)S(1)}, f32[512,2]{0,1:T(2,128)}, u32[]{:S(2)}) copy-start(f32[512,2]{0,1:T(2,128)} %param.29) | copy-start | bytes 12292
  17.1 30.0 %all-to-all-start = ((bf16[4,128,2048]{2,1,0:T(8,128)(2,1)}), bf16[4,128,2048]{2,1,0:T(8,128)(2,1)S(1)}, u32[]{:S(2)}, u32[]{:S(2)}) async-start(bf16[4,128,2048]{2,1,0:T(8,128)(2,1)} %broadcast_in_dim.25), calls=%async_computation | async-start | bytes 4194304 | tf_op jit(solution)/shard_map/all_to_all | solution.py:23
  21.5 242.7 %all-gather.8.cloned.1.call-start = ((), (), s32[]{:S(2)}) async-start(), calls=%async_computation.3 | async-start | bytes 2129920 | tf_op jit(solution)/shard_map/all_gather | solution.py:68
  22.3 372.4 %all-gather.10.cloned.1.call-start = ((), (), s32[]{:S(2)}) async-start(), calls=%async_computation.4 | async-start | bytes 4259840 | tf_op jit(solution)/shard_map/all_gather | solution.py:42
  137.9 7.2 %copy-start.5 = (bf16[4,128,2,128]{3,2,1,0:T(2,128)(2,1)}, bf16[4,128,2,128]{3,2,1,0:T(2,128)(2,1)S(1)}, u32[]{:S(2)}) copy-start(bf16[4,128,2,128]{3,2,1,0:T(2,128)(2,1)S(1)} %reshape_reshape.3) | copy-start | bytes 786436
  145.1 0.8 copy-start
  145.1 1.4 copy-start.2
  146.5 8.5 %copy-start.13 = (f32[2]{0:T(128)S(1)}, f32[2]{0:T(128)}, u32[]{:S(2)}) copy-start(f32[2]{0:T(128)} %get-tuple-element.118) | copy-start | bytes 28
  146.5 101.1 %copy-start.11 = (bf16[3,256]{1,0:T(4,128)(2,1)S(1)}, bf16[3,256]{1,0:T(4,128)(2,1)}, u32[]{:S(2)}) copy-start(bf16[3,256]{1,0:T(4,128)(2,1)} %param.26) | copy-start | bytes 4612
  253.7 4.2 copy-start.3
  253.7 4.2 copy-start.4
  255.7 0.8 copy-start.6
  255.7 2.4 copy-start.1
  256.5 7.7 %collective-permute-start = (f32[2,256]{1,0:T(2,128)S(1)}, f32[2,256]{1,0:T(2,128)S(1)}, u32[]{:S(2)}, u32[]{:S(2)}) collective-permute-start(f32[2,256]{1,0:T(2,128)S(1)} %slice.84), channel_id=1, source_target_pairs={{0,4},{4,8},{8,12},{12,16},{16,20},{20,24},{24,28},{28,32},{32,36}... | collective-permute-start | bytes 6152 | tf_op jit(solution)/shard_map/ppermute | solution.py:62
  258.0 6.2 %copy-start.7 = (f32[512,256]{1,0:T(8,128)S(1)}, f32[512,256]{1,0:T(8,128)}, u32[]{:S(2)}) copy-start(f32[512,256]{1,0:T(8,128)} %copy-done.6) | copy-start | bytes 1572868
Sparse Core Ops, SparseCore 0:
  12.4 123.3 all-gather.5
  138.0 126.1 all-gather.7
  266.4 128.3 all-gather.9
where the time goes:
time: 508 us; the launch traced here: 504 us
  waiting for transfers between devices  239 us (47%)
  blocking collectives  123 us (24%)
  other arithmetic  71.5 us (14%)
  matrix products  27.3 us (5%)
  local copies, waits for them, and re-layouts  21.4 us (4%)
  between operations  14.2 us (3%)
  starting transfers between devices  5.79 us (1%)
    all_gather x1, waiting for transfers between devices, prefix_2(): lax.all_gather(a.astype(kind), axis)  125 us
    unnamed x1, blocking collectives  92 us
    all_gather x1, waiting for transfers between devices, sent_together(): lax.all_gather(both, axis, axis=dim, tiled=True)  88.8 us
    add x63, other arithmetic, combine_states(): later[0][:, None, None] * earlier[1] + later[1]  58.7 us
    all_to_all x1, blocking collectives, summed_on_arrival(): blocks = lax.all_to_all(split_up(x, dim, count), axis, 0, 0, tiled=True)  30.8 us
    all_to_all x1, waiting for transfers between devices, from_everyone(): return lax.all_to_all(copies, axis, split_axis=0, concat_axis=0, tiled=True)  21.8 us
    unnamed x42, local copies, waits for them, and re-layouts  13.9 us
  transfers between devices with their start and end apart: 5, of which 4 were waited for; matrix products, arithmetic and copies ran while one was open for 9% of the time, Pallas kernels for 0%

commit v1 on v0

v1 whole, which is shorter than its diff:
```python
import functools

import jax
import jax.numpy as jnp
from jax import lax
from jax.experimental import pallas as pl
from jax.experimental.pallas import tpu as pltpu
from jax.sharding import Mesh, PartitionSpec as P

HEAD = 128
HALF = HEAD // 2
CONV_K = 3
EPSILON = 1e-06
ROTARY_BASE = 10000.0
BLOCK = 256
EXTRA = 16
INTERPRET = False

BF16 = jnp.bfloat16
F32 = jnp.float32
CHIPS = ("za", "zb", "zc")
NEAR = ("zb", "zc")
FAR = ("za", "zb")
PAIR = ("zc", "core")

VMEM = pl.BlockSpec(memory_space=pltpu.VMEM)
SMEM = pl.BlockSpec(memory_space=pltpu.SMEM)


def call(kernel, outs, name, n_scalar=0, scratch=(), flops=0):
    def run(*args):
        return pl.pallas_call(
            kernel,
            out_shape=outs,
            in_specs=[SMEM] * n_scalar + [VMEM] * (len(args) - n_scalar),
            out_specs=jax.tree.map(lambda _: VMEM, outs),
            scratch_shapes=list(scratch),
            interpret=INTERPRET,
            name=name,
            cost_estimate=pl.CostEstimate(flops=flops, bytes_accessed=0, transcendentals=0),
        )(*args)

    return run


def shape(dims, kind):
    return jax.ShapeDtypeStruct(dims, kind)


def dot(a, b, dims):
    return lax.dot_general(a, b, (dims, ((), ())), preferred_element_type=F32)


def pack_kernel(*refs):
    *inputs, out = refs
    for at, ref in enumerate(inputs):
        for core in range(2):
            half = ref[:, core * HEAD : (core + 1) * HEAD]
            for pair in range(2):
                out[2 * pair + core, :, at * HEAD : (at + 1) * HEAD] = half


def norm_kernel(tokens, gain, out):
    values = tokens[...].astype(F32)
    scale = lax.rsqrt(jnp.mean(values * values, axis=-1, keepdims=True) + EPSILON)
    normed = (values * scale * gain[...].astype(F32)).astype(BF16)
    for copy in range(out.shape[0]):
        out[copy] = normed


def rotated(head, cosine, sine):
    wide_cosine = jnp.concatenate([cosine, cosine], axis=-1)
    wide_sine = jnp.concatenate([-sine, sine], axis=-1)
    turned = jnp.concatenate([head[:, HALF:], head[:, :HALF]], axis=-1)
    return head * wide_cosine + turned * wide_sine


def in_three(log_total):
    high = log_total.astype(BF16).astype(F32)
    middle = (log_total - high).astype(BF16).astype(F32)
    low = log_total - high - middle
    row = lax.broadcasted_iota(jnp.int32, (EXTRA, HEAD), 0)
    rows = jnp.where(row == 0, high, jnp.where(row == 1, middle, jnp.where(row == 2, low, 0.0)))
    return rows.astype(BF16)


def from_three(rows):
    rows = rows.astype(F32)
    return rows[0:1] + rows[1:2] + rows[2:3]


def kv_kernel(x, wk, wv, cosine, sine, decay, k_out, v_out, message):
    rows = x.shape[0]
    total = decay[rows - 1 : rows, :]
    weight = jnp.concatenate([wk[...], wv[...]], axis=1)

    def block(i, state):
        at = pl.ds(pl.multiple_of(i * BLOCK, BLOCK), BLOCK)
        both = dot(x[at, :], weight, ((1,), (0,))).astype(BF16)
        key = rotated(both[:, :HEAD].astype(F32), cosine[at, :], sine[at, :]) * HEAD ** (-0.5)
        k_out[at, :] = key.astype(BF16)
        value = both[:, HEAD:]
        v_out[at, :] = value
        faded = (key * jnp.exp(total - decay[at, :])).astype(BF16)
        return state + dot(faded, value, ((0,), (0,)))

    state = lax.fori_loop(0, rows // BLOCK, block, jnp.zeros((HEAD, HEAD), F32))
    extra = in_three(jnp.broadcast_to(total, (1, HEAD)))
    for copy in range(message.shape[0]):
        message[copy, :HEAD, :] = state.astype(BF16)
        message[copy, HEAD:, :] = extra


def near_kernel(place, gathered, message, before, fade, scratch):
    own = place[0]
    run = jnp.zeros((HEAD, HEAD), F32)
    passed = jnp.zeros((1, HEAD), F32)
    kept, kept_passed = run, passed
    for at in range(gathered.shape[0]):
        kept = jnp.where(own == at, run, kept)
        kept_passed = jnp.where(own == at, passed, kept_passed)
        log_total = from_three(gathered[at, HEAD:, :])
        run = jnp.exp(log_total) * run + gathered[at, :HEAD, :].astype(F32)
        passed = passed + log_total
    before[...] = kept
    fade[...] = jnp.broadcast_to(jnp.exp(kept_passed), fade.shape)
    scratch[...] = run
    share = HEAD // gathered.shape[0]
    part = scratch[pl.ds(pl.multiple_of(own * share, share), share), :].astype(BF16)
    extra = in_three(passed)
    for copy in range(message.shape[0]):
        message[copy, :share, :] = part
        message[copy, share:, :] = extra


def far_kernel(place, gathered, message):
    own = place[0]
    share = message.shape[1]
    run = jnp.zeros((share, HEAD), F32)
    kept = run
    for at in range(gathered.shape[0]):
        kept = jnp.where(own == at, run, kept)
        run = jnp.exp(from_three(gathered[at, share:, :])) * run + gathered[at, :share, :].astype(F32)
    for copy in range(message.shape[0]):
        message[copy] = kept.astype(BF16)


def branch_kernel(
    core, x, halo, weights, cosine, sine, decay, decay_row, keys, values, base, before, fade, taps, keep, send
):
    rows = x.shape[0]
    own = core[0]
    share = base.shape[1]
    parts = [base[at].astype(F32) for at in range(base.shape[0])]
    incoming = fade[0:1, :] * jnp.concatenate(parts, axis=0) + before[...]
    weight = weights[:, : 5 * HEAD]
    rim = dot(halo[...], weights[:, HEAD : 3 * HEAD], ((1,), (0,))).astype(BF16).astype(F32)
    tail = (rim[:, :HEAD] * rim[:, HEAD:])[EXTRA - 8 :]
    row = lax.broadcasted_iota(jnp.int32, (BLOCK, HEAD), 0)
    causal = lax.broadcasted_iota(jnp.int32, (BLOCK, BLOCK), 0) >= lax.broadcasted_iota(
        jnp.int32, (BLOCK, BLOCK), 1
    )
    tap = taps[...].astype(F32)
    state = incoming
    start = jnp.zeros((1, 1), F32)
    for i in range(rows // BLOCK):
        at = pl.ds(i * BLOCK, BLOCK)
        projected = dot(x[at, :], weight, ((1,), (0,))).astype(BF16)
        outer = projected[:, :HEAD].astype(F32)
        mixed = projected[:, HEAD : 2 * HEAD].astype(F32) * projected[:, 2 * HEAD : 3 * HEAD].astype(F32)
        one = jnp.where(row == 0, tail[7:8], pltpu.roll(mixed, 1, 0))
        two = jnp.where(row == 0, tail[6:7], jnp.where(row == 1, tail[7:8], pltpu.roll(mixed, 2, 0)))
        conv = tap[0:1] * two + tap[1:2] * one + tap[2:3] * mixed
        tail = mixed[BLOCK - 8 :]
        conv_branch = (outer * conv).astype(BF16)

        query = rotated(projected[:, 3 * HEAD : 4 * HEAD].astype(F32), cosine[at, :], sine[at, :])
        query16 = query.astype(BF16)
        key, value = keys[at, :], values[at, :]
        column = decay[at, :]
        line = decay_row[:, i * BLOCK : (i + 1) * BLOCK]
        spread = jnp.where(causal, column - line, 0.0)
        scores = jnp.where(causal, dot(query16, key, ((1,), (1,))) * jnp.exp(spread), 0.0)
        within = dot(scores.astype(BF16), value, ((1,), (0,)))
        across = dot(query16, state.astype(BF16), ((1,), (0,))) * jnp.exp(column - start)
        retained = within + across
        end = decay[(i + 1) * BLOCK - 1 : (i + 1) * BLOCK, :]
        faded = (key.astype(F32) * jnp.exp(end - column)).astype(BF16)
        state = jnp.exp(end - start) * state + dot(faded, value, ((0,), (0,)))
        start = end
        normed = retained * lax.rsqrt(jnp.mean(retained * retained, axis=-1, keepdims=True) + EPSILON)
        gate = projected[:, 4 * HEAD :].astype(F32)
        ret_branch = (normed * (gate / (1.0 + jnp.exp(-gate)))).astype(BF16)

        half = (i * BLOCK) // (rows // 2)
        place = pl.ds(i * BLOCK - half * (rows // 2), BLOCK)

        @pl.when(own == half)
        def _():
            keep[place, :HEAD] = conv_branch
            keep[place, HEAD:] = ret_branch

        @pl.when(own != half)
        def _():
            send[place, :HEAD] = conv_branch
            send[place, HEAD:] = ret_branch


def out_kernel(mine, theirs, own_weight, other_weight, out):
    parts, rows = out.shape[0], out.shape[1]
    step = 512
    for column in range(0, out.shape[2], step):
        at = pl.ds(column, step)
        total = dot(mine[...], own_weight[at, :], ((1,), (1,))) + dot(theirs[...], other_weight[at, :], ((1,), (1,)))
        total = total.astype(BF16)
        for part in range(parts):
            out[part, :, column : column + step] = total[part * rows : (part + 1) * rows]


def sum_kernel(parts, out):
    total = parts[0].astype(F32)
    for at in range(1, parts.shape[0]):
        total = total + parts[at].astype(F32)
    out[...] = total.astype(BF16)


def exchanged(x, axes):
    return lax.all_to_all(x, axes, 0, 0, tiled=True)


def body(
    tokens,
    norm_gain,
    conv_outer_weight,
    conv_inner_weight,
    conv_input_weight,
    query_matrix,
    key_weight,
    value_weight,
    gate_weight,
    conv_taps,
    conv_out_weight,
    ret_out_weight,
    log_decay,
):
    own_rows, width = tokens.shape
    tp = lax.axis_size("tp")
    chip = lax.axis_index(CHIPS)
    core = lax.axis_index("core")
    chips = lax.axis_size(CHIPS)
    near, far = lax.axis_size(NEAR), lax.axis_size("za")
    rows = 2 * tp * own_rows
    shard = key_weight.shape[0]

    packed = call(pack_kernel, shape((4, shard, 9 * HEAD), BF16), "pack")(
        key_weight,
        value_weight,
        conv_outer_weight,
        conv_inner_weight,
        conv_input_weight,
        query_matrix,
        gate_weight,
        conv_out_weight.T,
        ret_out_weight.T,
    )
    bundle = exchanged(packed, PAIR).reshape(4 * shard, 9 * HEAD)
    rest = lax.all_gather(bundle[:, 2 * HEAD :], FAR, axis=0, tiled=True)
    wk = lax.all_gather(bundle[:, :HEAD], FAR).reshape(width, HEAD)
    wv = lax.all_gather(bundle[:, HEAD : 2 * HEAD], FAR).reshape(width, HEAD)

    normed = call(norm_kernel, shape((2 * tp, own_rows, width), BF16), "norm")(
        tokens, norm_gain.reshape(1, width)
    )
    x = exchanged(normed, ("core", "tp")).reshape(rows, width)
    halo = lax.ppermute(x[rows - EXTRA :], CHIPS, [(i, i + 1) for i in range(chips - 1)])

    logs = exchanged(log_decay.T, "core").reshape(rows // HEAD, HEAD)
    upper = jnp.triu(jnp.ones((HEAD, HEAD), F32))
    inner = jnp.dot(logs, upper, precision=lax.Precision.HIGHEST)
    ends = inner[:, -1]
    lower = jnp.tril(jnp.ones((rows // HEAD, rows // HEAD), F32), -1)
    cumulative = inner + jnp.sum(lower * ends[None, :], axis=1)[:, None]
    decay = cumulative.reshape(rows, 1)
    decay_row = cumulative.reshape(1, rows)

    positions = (chip * rows).astype(F32) + jnp.arange(rows, dtype=F32)
    inv_freq = ROTARY_BASE ** (-jnp.arange(HALF, dtype=F32) / HALF)
    angles = positions[:, None] * inv_freq[None, :]
    cosine, sine = jnp.cos(angles), jnp.sin(angles)

    keys, values, message = call(
        kv_kernel,
        (shape((rows, HEAD), BF16), shape((rows, HEAD), BF16), shape((near, HEAD + EXTRA, HEAD), BF16)),
        "kv",
        flops=4 * rows * width * HEAD,
    )(x, wk, wv, cosine, sine, decay)

    share = HEAD // near
    gathered = exchanged(message, NEAR)
    message, before, fade = call(
        near_kernel,
        (shape((far, share + EXTRA, HEAD), BF16), shape((HEAD, HEAD), F32), shape((8, HEAD), F32)),
        "near",
        n_scalar=1,
        scratch=[pltpu.VMEM((HEAD, HEAD), F32)],
    )(lax.axis_index(NEAR).reshape(1), gathered)
    gathered = exchanged(message, "za")
    message = call(far_kernel, shape((near, share, HEAD), BF16), "far", n_scalar=1)(
        lax.axis_index("za").reshape(1), gathered
    )
    base = exchanged(message, NEAR)

    other_core = [(0, 1), (1, 0)]
    out_own = rest[:, 5 * HEAD :]
    out_other = lax.ppermute(out_own, "core", other_core)
    keep, send = call(
        branch_kernel,
        (shape((rows // 2, 2 * HEAD), BF16), shape((rows // 2, 2 * HEAD), BF16)),
        "branch",
        n_scalar=1,
        flops=10 * rows * width * HEAD,
    )(
        core.reshape(1),
        x,
        halo,
        rest,
        cosine,
        sine,
        decay,
        decay_row,
        keys,
        values,
        base,
        before,
        fade,
        lax.dynamic_slice_in_dim(conv_taps, core * HEAD, HEAD, 1),
    )
    theirs = lax.ppermute(send, "core", other_core)
    partial = call(out_kernel, shape((tp, own_rows, width), BF16), "out", flops=rows * width * 4 * HEAD)(
        keep, theirs, out_own, out_other
    )
    return call(sum_kernel, shape((own_rows, width), BF16), "sum")(exchanged(partial, "tp"))


def solution(mesh):
    groups, stretches, tp = mesh.devices.shape
    chips = stretches // 2
    fine = Mesh(
        mesh.devices.reshape(groups, chips // 4, 2, 2, 2, tp), ("grp", "za", "zb", "zc", "core", "tp")
    )
    sp = ("za", "zb", "zc", "core")
    columns = P(sp, "tp")
    placed = (
        P(("grp", *sp, "tp"), None),
        P(),
        *([columns] * 7),
        P(None, "tp"),
        P("tp", sp),
        P("tp", sp),
        P(("grp", *sp), "tp"),
    )
    return jax.shard_map(
        body, mesh=fine, in_specs=placed, out_specs=P(("grp", *sp, "tp"), None), check_vma=False
    )
```

time: 508 us -> 311 us (0.61)
  the two profiles are of different devices: /device:TPU:2017 before, /device:TPU:33 now
where the time goes in v1:
time: 311 us; the launch traced here: 310 us
  blocking collectives  189 us (61%)
  starting transfers between devices  49.9 us (16%)
  Pallas kernels  31.8 us (10%)
  between operations  13.5 us (4%)
  waiting for transfers between devices  12.8 us (4%)
  local copies, waits for them, and re-layouts  9.53 us (3%)
  other arithmetic  3.33 us (1%)
    all_to_all x3, blocking collectives, exchanged(): return lax.all_to_all(x, axes, 0, 0, tiled=True)  91.5 us
    all_gather x1, blocking collectives, body(): wk = lax.all_gather(bundle[:, :HEAD], FAR).reshape(width, HEAD)  52.7 us
    all_gather x1, blocking collectives, body(): wv = lax.all_gather(bundle[:, HEAD:2 * HEAD], FAR).reshape(width, HEAD)  45 us
    pallas_call x8, Pallas kernels, run(): pl.pallas_call(kernel, out_shape=outs, in_specs=[SMEM] * n_scalar + [VMEM...  31.8 us
    all_to_all x4, starting transfers between devices, exchanged(): return lax.all_to_all(x, axes, 0, 0, tiled=True)  22.4 us
    ppermute x1, starting transfers between devices, body(): theirs = lax.ppermute(send, 'core', other_core)  12.9 us
    ppermute x1, starting transfers between devices, body(): out_other = lax.ppermute(out_own, 'core', other_core)  10.7 us
    all_to_all x4, waiting for transfers between devices, exchanged(): return lax.all_to_all(x, axes, 0, 0, tiled=True)  10.6 us
  transfers between devices with their start and end apart: 8, of which 3 were waited for; matrix products, arithmetic and copies ran while one was open for 3% of the time, Pallas kernels for 7%

profile of v1, /device:TPU:33, one launch (start us, length us, event | category | flops | bytes accessed | tf_op | source)
XLA Modules:
  0.0 310.3 jit_solution(9254079337031111038)
XLA Ops:
  6.5 0.0 copy-start
  6.6 0.0 all-gather.4.cloned.1.call-start
  6.6 1.6 pack.1
  8.2 50.7 %all_to_all.39 = bf16[4,32,1152]{2,1,0:T(8,128)(2,1)S(1)} all-to-all(bf16[4,32,1152]{2,1,0:T(8,128)(2,1)} %pack.1), channel_id=1, replica_groups=mesh['grp'=2,'za'=8,'zb'=2,'zc'=2,'core'=2,'tp'=4] {'zc','core'}, dimensions={0} | all-to-all | bytes 589824 | tf_op jit(solution)/shard_map/all_to_all | solution.py:228
  58.8 0.7 slice.25
  59.5 0.1 all-gather.4.cloned.1.call-update
  59.6 1.3 all_to_all.26
  60.9 3.7 %all-to-all-start.2 = ((f32[2,1,512]{2,1,0:T(1,128)}), f32[2,1,512]{2,1,0:T(1,128)S(1)}, u32[]{:S(2)}, u32[]{:S(2)}) async-start(f32[2,1,512]{2,1,0:T(1,128)} %all_to_all.26), calls=%async_computation.2 | async-start | bytes 8192 | tf_op jit(solution)/shard_map/all_to_all | solution.py:228
  64.6 1.3 reshape.49.gain
  65.9 3.5 %norm.1 = bf16[8,128,2048]{2,1,0:T(8,128)(2,1)} custom-call(bf16[128,2048]{1,0:T(8,128)(2,1)} %tokens.1, bf16[1,2048]{1,0:T(2,128)(2,1)} %reshape.49.gain), custom_call_target="tpu_custom_call" | custom-call | tf_op jit(solution)/shard_map/norm/pallas_call | solution.py:32
  69.4 0.0 all-to-all-done.2
  69.4 4.6 %all-to-all-start = ((bf16[8,128,2048]{2,1,0:T(8,128)(2,1)}), bf16[8,128,2048]{2,1,0:T(8,128)(2,1)}, u32[]{:S(2)}, u32[]{:S(2)}) async-start(bf16[8,128,2048]{2,1,0:T(8,128)(2,1)} %norm.1), calls=%async_computation | async-start | bytes 8388608 | tf_op jit(solution)/shard_map/all_to_all | solution.py:228
  74.0 0.2 convolution_bitcast_fusion
  74.3 0.2 slice_reduce_fusion
  74.5 0.2 multiply_reduce_fusion
  74.6 0.1 broadcast_add_fusion
  74.7 0.0 copy-start.7
  74.7 1.1 copy.19.decay
  75.8 3.0 multiply_sine_fusion
  78.9 52.7 %all-gather.wk = bf16[2048,128]{1,0:T(8,128)(2,1)} all-gather(bf16[128,128]{1,0:T(8,128)(2,1)S(1)} %get-tuple-element.22), channel_id=2, replica_groups=mesh['grp'=2,'za'=8,'zb'=2,'zc'=2,'core'=2,'tp'=4] {'za','zb'}, dimensions={0}, use_global_device_ids=true | all-gather | bytes 557056 | tf_op jit(solution)/shard_map/all_gather | solution.py:268
  131.6 45.0 %all-gather.1.wv = bf16[2048,128]{1,0:T(8,128)(2,1)} all-gather(bf16[128,128]{1,0:T(8,128)(2,1)S(1)} %get-tuple-element.21), channel_id=3, replica_groups=mesh['grp'=2,'za'=8,'zb'=2,'zc'=2,'core'=2,'tp'=4] {'za','zb'}, dimensions={0}, use_global_device_ids=true | all-gather | bytes 557056 | tf_op jit(solution)/shard_map/all_gather | solution.py:269
  176.6 0.0 all-to-all-done
  176.6 6.7 %kv.1 = (bf16[1024,128]{1,0:T(8,128)(2,1)}, bf16[1024,128]{1,0:T(8,128)(2,1)}, bf16[4,144,128]{2,1,0:T(8,128)(2,1)}) custom-call(bf16[1024,2048]{1,0:T(8,128)(2,1)} %bitcast.1.x, bf16[2048,128]{1,0:T(8,128)(2,1)} %all-gather.wk, bf16[2048,128]{1,0:T(8,128)(2,1)} %all-gather.1.wv, f32[1024,64]{1,0:T(8,128)} %get-tuple-element.24.cosine, ...), custom_call_target="tpu_custom_call" | custom-call | flops 1073741824 | tf_op jit(solution)/shard_map/kv/pallas_call | solution.py:32
  183.3 0.0 copy-done.7
  183.3 10.3 %all_to_all.40.gathered = bf16[4,144,128]{2,1,0:T(8,128)(2,1)} all-to-all(bf16[4,144,128]{2,1,0:T(8,128)(2,1)} %get-tuple-element.15), channel_id=1, replica_groups=mesh['grp'=2,'za'=8,'zb'=2,'zc'=2,'core'=2,'tp'=4] {'zb','zc'}, dimensions={0} | all-to-all | bytes 294912 | tf_op jit(solution)/shard_map/all_to_all | solution.py:228
  193.5 1.6 near.1
  195.1 10.6 %all-to-all-start.4 = ((bf16[8,48,128]{2,1,0:T(8,128)(2,1)}), bf16[8,48,128]{2,1,0:T(8,128)(2,1)S(1)}, u32[]{:S(2)}, u32[]{:S(2)}) async-start(bf16[8,48,128]{2,1,0:T(8,128)(2,1)} %get-tuple-element.16), calls=%async_computation.4 | async-start | bytes 196608 | tf_op jit(solution)/shard_map/all_to_all | solution.py:228
  205.7 0.0 all-gather.4.cloned.1.call-done.weights
  205.7 1.3 slice.28.own_weight
  207.0 0.0 copy-start.1
  207.1 10.7 %collective-permute-start.2 = (bf16[2048,256]{1,0:T(8,128)(2,1)S(1)}, bf16[2048,256]{1,0:T(8,128)(2,1)S(1)}, u32[]{:S(2)}, u32[]{:S(2)}) collective-permute-start(bf16[2048,256]{1,0:T(8,128)(2,1)S(1)} %slice.28.own_weight), channel_id=1, source_target_pairs={{0,4},{4,0},{1,5},{5,1},{2,6},{6,2},{3,7},{7,3},{8,12},{12,8},{9,1... | collective-permute-start | bytes 3145736 | tf_op jit(solution)/shard_map/ppermute | solution.py:315
  217.8 10.6 %all-to-all-done.4.gathered = bf16[8,48,128]{2,1,0:T(8,128)(2,1)S(1)} async-done(((bf16[8,48,128]{2,1,0:T(8,128)(2,1)}), bf16[8,48,128]{2,1,0:T(8,128)(2,1)S(1)}, u32[]{:S(2)}, u32[]{:S(2)}) %all-to-all-start.4) | async-done | bytes 98336 | tf_op jit(solution)/shard_map/all_to_all | solution.py:228
  228.4 0.0 copy-start.3
  228.4 0.6 copy-done.3
  229.0 1.5 far.1
  230.5 3.4 %all-to-all-start.5 = ((bf16[4,32,128]{2,1,0:T(8,128)(2,1)}), bf16[4,32,128]{2,1,0:T(8,128)(2,1)S(1)}, u32[]{:S(2)}, u32[]{:S(2)}) async-start(bf16[4,32,128]{2,1,0:T(8,128)(2,1)} %far.1), calls=%async_computation.5 | async-start | bytes 65536 | tf_op jit(solution)/shard_map/all_to_all | solution.py:228
  234.0 0.8 slice.24
  234.8 4.0 %collective-permute-start = (bf16[16,2048]{1,0:T(8,128)(2,1)S(1)}, bf16[16,2048]{1,0:T(8,128)(2,1)S(1)}, u32[]{:S(2)}, u32[]{:S(2)}) collective-permute-start(bf16[16,2048]{1,0:T(8,128)(2,1)S(1)} %slice.24), channel_id=1, source_target_pairs={{0,8},{8,16},{16,24},{24,32},{32,40},{40,48},{48,56},{56,64},{64,7... | collective-permute-start | bytes 196616 | tf_op jit(solution)/shard_map/ppermute | solution.py:275
  238.8 0.0 copy-done
  238.8 0.5 constant_dynamic-slice_fusion.taps
  239.3 0.8 collective-permute-done.halo
  240.1 0.0 copy-start.6
  240.1 0.0 all-to-all-done.5.base
  240.1 0.0 copy-start.5
  240.1 0.6 copy-done.6
  240.7 0.0 copy-done.5
  240.7 9.9 %branch.1 = (bf16[512,256]{1,0:T(8,128)(2,1)}, bf16[512,256]{1,0:T(8,128)(2,1)}) custom-call(s32[1]{0:T(128)} %bitcast.core, bf16[1024,2048]{1,0:T(8,128)(2,1)} %bitcast.1.x, bf16[16,2048]{1,0:T(8,128)(2,1)} %copy-done.6, bf16[2048,896]{1,0:T(8,128)(2,1)} %all-gather.4.cloned.1.call-done.weights, f32[1024,64]{1,0:T(8,128)} %get-tuple-element.24.cosine, ...), custom_call_target="tpu_custom_call" | custom-call | flops 2684354560 | tf_op jit(solution)/shard_map/branch/pallas_call | solution.py:32
  250.7 0.0 copy-done.1
  250.7 12.9 %collective-permute-start.1 = (bf16[512,256]{1,0:T(8,128)(2,1)}, bf16[512,256]{1,0:T(8,128)(2,1)S(1)}, u32[]{:S(2)}, u32[]{:S(2)}) collective-permute-start(bf16[512,256]{1,0:T(8,128)(2,1)} %get-tuple-element.20), channel_id=1, source_target_pairs={{0,4},{4,0},{1,5},{5,1},{2,6},{6,2},{3,7},{7,3},{8,12},{12,8},{9,1... | collective-permute-start | bytes 786440 | tf_op jit(solution)/shard_map/ppermute | solution.py:338
  263.6 1.4 collective-permute-done.1.theirs
  264.9 0.0 copy-start.4
  264.9 0.0 collective-permute-done.2.other_weight
  264.9 0.0 copy-start.2
  264.9 0.7 copy-done.4
  265.6 0.4 copy-done.2
  266.0 4.3 %out.1 = bf16[4,128,2048]{2,1,0:T(8,128)(2,1)} custom-call(bf16[512,256]{1,0:T(8,128)(2,1)} %get-tuple-element.19.mine, bf16[512,256]{1,0:T(8,128)(2,1)} %copy-done.4, bf16[2048,256]{1,0:T(8,128)(2,1)} %copy-done.1, bf16[2048,256]{1,0:T(8,128)(2,1)} %copy-done.2), custom_call_target="tpu_custom_call" | custom-call | flops 1073741824 | tf_op jit(solution)/shard_map/out/pallas_call | solution.py:32
  270.3 30.5 %all_to_all.41.parts = bf16[4,128,2048]{2,1,0:T(8,128)(2,1)} all-to-all(bf16[4,128,2048]{2,1,0:T(8,128)(2,1)} %out.1), channel_id=1, replica_groups=mesh['grp'=2,'za'=8,'zb'=2,'zc'=2,'core'=2,'tp'=4] {'tp'}, dimensions={0} | all-to-all | bytes 4194304 | tf_op jit(solution)/shard_map/all_to_all | solution.py:228
  300.8 2.6 sum.1
  (5 shorter events, 0.0 us)
Async XLA Ops:
  6.5 232.2 %copy-start = (bf16[3,256]{1,0:T(4,128)(2,1)S(1)}, bf16[3,256]{1,0:T(4,128)(2,1)}, u32[]{:S(2)}) copy-start(bf16[3,256]{1,0:T(4,128)(2,1)} %param.22) | copy-start | bytes 4612
  6.6 199.2 %all-gather.4.cloned.1.call-start = ((), (), s32[]{:S(2)}) async-start(), calls=%async_computation.7 | async-start | bytes 3899392 | tf_op jit(solution)/shard_map/all_gather | solution.py:267
  60.9 8.5 %all-to-all-start.2 = ((f32[2,1,512]{2,1,0:T(1,128)}), f32[2,1,512]{2,1,0:T(1,128)S(1)}, u32[]{:S(2)}, u32[]{:S(2)}) async-start(f32[2,1,512]{2,1,0:T(1,128)} %all_to_all.26), calls=%async_computation.2 | async-start | bytes 8192 | tf_op jit(solution)/shard_map/all_to_all | solution.py:228
  69.4 107.2 %all-to-all-start = ((bf16[8,128,2048]{2,1,0:T(8,128)(2,1)}), bf16[8,128,2048]{2,1,0:T(8,128)(2,1)}, u32[]{:S(2)}, u32[]{:S(2)}) async-start(bf16[8,128,2048]{2,1,0:T(8,128)(2,1)} %norm.1), calls=%async_computation | async-start | bytes 8388608 | tf_op jit(solution)/shard_map/all_to_all | solution.py:228
  74.7 108.5 %copy-start.7 = (f32[8,128]{1,0:T(8,128)}, f32[8,128]{1,0:T(8,128)S(1)}, u32[]{:S(2)}) copy-start(f32[8,128]{1,0:T(8,128)S(1)} %broadcast_add_fusion) | copy-start | bytes 12292
  195.1 33.2 %all-to-all-start.4 = ((bf16[8,48,128]{2,1,0:T(8,128)(2,1)}), bf16[8,48,128]{2,1,0:T(8,128)(2,1)S(1)}, u32[]{:S(2)}, u32[]{:S(2)}) async-start(bf16[8,48,128]{2,1,0:T(8,128)(2,1)} %get-tuple-element.16), calls=%async_computation.4 | async-start | bytes 196608 | tf_op jit(solution)/shard_map/all_to_all | solution.py:228
  207.0 43.6 %copy-start.1 = (bf16[2048,256]{1,0:T(8,128)(2,1)}, bf16[2048,256]{1,0:T(8,128)(2,1)S(1)}, u32[]{:S(2)}) copy-start(bf16[2048,256]{1,0:T(8,128)(2,1)S(1)} %slice.28.own_weight) | copy-start | bytes 3145732
  207.1 57.9 %collective-permute-start.2 = (bf16[2048,256]{1,0:T(8,128)(2,1)S(1)}, bf16[2048,256]{1,0:T(8,128)(2,1)S(1)}, u32[]{:S(2)}, u32[]{:S(2)}) collective-permute-start(bf16[2048,256]{1,0:T(8,128)(2,1)S(1)} %slice.28.own_weight), channel_id=1, source_target_pairs={{0,4},{4,0},{1,5},{5,1},{2,6},{6,2},{3,7},{7,3},{8,12},{12,8},{9,1... | collective-permute-start | bytes 3145736 | tf_op jit(solution)/shard_map/ppermute | solution.py:315
  228.4 0.6 copy-start.3
  230.5 9.6 %all-to-all-start.5 = ((bf16[4,32,128]{2,1,0:T(8,128)(2,1)}), bf16[4,32,128]{2,1,0:T(8,128)(2,1)S(1)}, u32[]{:S(2)}, u32[]{:S(2)}) async-start(bf16[4,32,128]{2,1,0:T(8,128)(2,1)} %far.1), calls=%async_computation.5 | async-start | bytes 65536 | tf_op jit(solution)/shard_map/all_to_all | solution.py:228
  234.8 5.3 %collective-permute-start = (bf16[16,2048]{1,0:T(8,128)(2,1)S(1)}, bf16[16,2048]{1,0:T(8,128)(2,1)S(1)}, u32[]{:S(2)}, u32[]{:S(2)}) collective-permute-start(bf16[16,2048]{1,0:T(8,128)(2,1)S(1)} %slice.24), channel_id=1, source_target_pairs={{0,8},{8,16},{16,24},{24,32},{32,40},{40,48},{48,56},{56,64},{64,7... | collective-permute-start | bytes 196616 | tf_op jit(solution)/shard_map/ppermute | solution.py:275
  240.1 0.6 copy-start.6
  240.1 0.6 copy-start.5
  250.7 14.2 %collective-permute-start.1 = (bf16[512,256]{1,0:T(8,128)(2,1)}, bf16[512,256]{1,0:T(8,128)(2,1)S(1)}, u32[]{:S(2)}, u32[]{:S(2)}) collective-permute-start(bf16[512,256]{1,0:T(8,128)(2,1)} %get-tuple-element.20), channel_id=1, source_target_pairs={{0,4},{4,0},{1,5},{5,1},{2,6},{6,2},{3,7},{7,3},{8,12},{12,8},{9,1... | collective-permute-start | bytes 786440 | tf_op jit(solution)/shard_map/ppermute | solution.py:338
  264.9 0.7 copy-start.4
  264.9 1.1 copy-start.2
Sparse Core Ops, SparseCore 0:
  59.7 112.2 all-gather.3

commit v2 on v1

v2 whole, which is shorter than its diff:
```python
import jax
import jax.numpy as jnp
from jax import lax
from jax.experimental import pallas as pl
from jax.experimental.pallas import tpu as pltpu
from jax.sharding import Mesh, PartitionSpec as P

HEAD = 128
HALF = HEAD // 2
CONV_K = 3
EPSILON = 1e-06
ROTARY_BASE = 10000.0
BLOCK = 256
EXTRA = 16
PROJECTED = 5 * HEAD
COLUMNS = 7 * HEAD
INTERPRET = False

BF16 = jnp.bfloat16
F32 = jnp.float32
CHIPS = ("za", "zb", "zc")
STRETCHES = ("za", "zb", "zc", "core")
NEAR = ("zb", "zc")
FAR = ("za", "zb")

VMEM = pl.BlockSpec(memory_space=pltpu.VMEM)
PLAIN = pl.BlockSpec(memory_space=pltpu.VMEM)
SMEM = pl.BlockSpec(memory_space=pltpu.SMEM)
ANY = pl.BlockSpec(memory_space=pl.ANY)


def call(kernel, outs, name, specs=None, scratch=(), flops=0, limit=16):
    def run(*args):
        in_specs = specs if specs is not None else [VMEM] * len(args)
        placed = [placed_for(arg, spec) for arg, spec in zip(args, in_specs)]
        return pl.pallas_call(
            kernel,
            out_shape=[o[0] for o in outs],
            in_specs=in_specs,
            out_specs=[o[1] for o in outs],
            scratch_shapes=list(scratch),
            interpret=INTERPRET,
            name=name,
            compiler_params=pltpu.CompilerParams(vmem_limit_bytes=limit << 20 if limit else None),
            cost_estimate=pl.CostEstimate(flops=flops, bytes_accessed=0, transcendentals=0),
        )(*placed)

    return run


def placed_for(arg, spec):
    if INTERPRET or all(spec is not kind for kind in (VMEM, ANY)):
        return arg
    return pltpu.with_memory_space_constraint(arg, pltpu.VMEM if spec is VMEM else pltpu.HBM)


def fast(dims, kind):
    return (jax.ShapeDtypeStruct(dims, kind) if INTERPRET else pltpu.VMEM(dims, kind), VMEM)


def slow(dims, kind):
    return (jax.ShapeDtypeStruct(dims, kind), VMEM)


def dot(a, b, dims):
    return lax.dot_general(a, b, (dims, ((), ())), preferred_element_type=F32)


def pack_kernel(key, value, *refs):
    *inputs, logs, rest, message = refs
    for at, ref in enumerate(inputs):
        for core in range(2):
            to = core * COLUMNS + at * HEAD
            rest[:, to : to + HEAD] = ref[:, core * HEAD : (core + 1) * HEAD]
    shard = key.shape[0]
    for core in range(2):
        message[core, :shard, :HEAD] = key[:, core * HEAD : (core + 1) * HEAD]
        message[core, :shard, HEAD:] = value[:, core * HEAD : (core + 1) * HEAD]
        lines = [logs[core : core + 1, at : at + 2 * HEAD] for at in range(0, logs.shape[1], 2 * HEAD)]
        line = jnp.concatenate(lines, axis=0)
        high = line.astype(BF16).astype(F32)
        middle = (line - high).astype(BF16).astype(F32)
        low = line - high - middle
        filler = jnp.zeros((EXTRA - 3 * len(lines), 2 * HEAD), F32)
        message[core, shard:, :] = jnp.concatenate([high, middle, low, filler], axis=0).astype(BF16)


def logs_of(rows, lines):
    rows = rows.astype(F32)
    return rows[:lines] + rows[lines : 2 * lines] + rows[2 * lines : 3 * lines]


def norm_kernel(tokens, gain, out):
    values = tokens[...].astype(F32)
    scale = lax.rsqrt(jnp.mean(values * values, axis=-1, keepdims=True) + EPSILON)
    normed = (values * scale * gain[...].astype(F32)).astype(BF16)
    for copy in range(out.shape[0]):
        out[copy] = normed


def rotated(head, cosine, sine):
    return head * cosine + pltpu.roll(head, HALF, 1) * sine


def kv_kernel(
    x, gathered, own, cos_far, sin_far, cos_near, sin_near, k_out, v_out, cosine, sine, decay, column, totals, message, weight
):
    rows, width = x.shape[0] * x.shape[1], x.shape[2]
    pairs, fars = gathered.shape[:2]
    shard = own.shape[1] - EXTRA
    lines = rows // 2 // (2 * HEAD)

    pieces = []
    for core in range(2):
        logs = logs_of(own[core, shard:, :], lines)
        for line in range(lines):
            pieces += [logs[line : line + 1, :HEAD], logs[line : line + 1, HEAD:]]
    logs = jnp.concatenate(pieces, axis=0)
    upper = lax.broadcasted_iota(jnp.int32, (HEAD, HEAD), 0) <= lax.broadcasted_iota(jnp.int32, (HEAD, HEAD), 1)
    inner = lax.dot_general(
        logs,
        upper.astype(F32),
        (((1,), (0,)), ((), ())),
        precision=lax.Precision.HIGHEST,
        preferred_element_type=F32,
    )
    before = jnp.zeros((1, 1), F32)
    added = []
    for at in range(len(pieces)):
        added.append(inner[at : at + 1] + before)
        before = before + inner[at : at + 1, HEAD - 1 :]
    cumulative = jnp.concatenate(added, axis=0)
    decay[...] = cumulative
    filler = jnp.zeros((HEAD - len(pieces), HEAD), F32)
    column[...] = jnp.concatenate([cumulative, filler], axis=0).T
    total = before

    for far in range(fars):
        for pair in range(pairs):
            chip = far * pairs + pair
            log_total = jnp.zeros((1, 1), F32)
            for core in range(2):
                at = core * (shard + EXTRA)
                weight[(2 * chip + core) * shard : (2 * chip + core + 1) * shard, :] = gathered[
                    pair, far, at : at + shard, :
                ]
                logs = logs_of(gathered[pair, far, at + shard : at + shard + EXTRA, :], lines)
                log_total = log_total + jnp.sum(logs, axis=(0, 1), keepdims=True)
            totals[chip : chip + 1, :] = jnp.broadcast_to(log_total, (1, HEAD))

    state = jnp.zeros((HEAD, HEAD), F32)
    for i in range(rows // BLOCK):
        at = pl.ds(i * BLOCK, BLOCK)
        cos_at = cos_far[i : i + 1, :] * cos_near[...] - sin_far[i : i + 1, :] * sin_near[...]
        sin_at = sin_far[i : i + 1, :] * cos_near[...] + cos_far[i : i + 1, :] * sin_near[...]
        first = lax.broadcasted_iota(jnp.int32, sin_at.shape, 1) < HALF
        sin_at = jnp.where(first, -sin_at, sin_at)
        cosine[at, :] = cos_at
        sine[at, :] = sin_at
        both = dot(block_rows(x, i), weight[...], ((1,), (0,))).astype(BF16)
        key = rotated(both[:, :HEAD].astype(F32), cos_at, sin_at) * HEAD ** (-0.5)
        k_out[at, :] = key.astype(BF16)
        value = both[:, HEAD:]
        v_out[at, :] = value
        here = block_column(column, i)
        faded = (key * jnp.exp(total - here)).astype(BF16)
        state = state + dot(faded, value, ((0,), (0,)))
    for copy in range(message.shape[0]):
        message[copy] = state.astype(BF16)


def block_rows(x, i):
    per = BLOCK // x.shape[1]
    return x[i * per : (i + 1) * per].reshape(BLOCK, x.shape[2])


def block_column(column, i):
    per = BLOCK // HEAD
    return jnp.concatenate([column[:, per * i + j : per * i + j + 1] for j in range(per)], axis=0)


def near_kernel(place, block, totals, gathered, message, before, fade, scratch):
    own = place[0]
    near = gathered.shape[0]
    run = jnp.zeros((HEAD, HEAD), F32)
    passed = jnp.zeros((1, HEAD), F32)
    kept, kept_passed = run, passed
    for at in range(near):
        kept = jnp.where(own == at, run, kept)
        kept_passed = jnp.where(own == at, passed, kept_passed)
        log_total = totals[pl.ds(block[0] * near + at, 1), :]
        run = jnp.exp(log_total) * run + gathered[at].astype(F32)
        passed = passed + log_total
    before[...] = kept
    fade[...] = jnp.broadcast_to(jnp.exp(kept_passed), fade.shape)
    scratch[...] = run
    share = HEAD // near
    part = scratch[pl.ds(pl.multiple_of(own * share, share), share), :].astype(BF16)
    for copy in range(message.shape[0]):
        message[copy] = part


def far_kernel(place, totals, gathered, message):
    own = place[0]
    near, share = message.shape[:2]
    run = jnp.zeros((share, HEAD), F32)
    kept = run
    for at in range(gathered.shape[0]):
        kept = jnp.where(own == at, run, kept)
        log_total = jnp.sum(totals[at * near : (at + 1) * near, :], axis=0, keepdims=True)
        run = jnp.exp(log_total) * run + gathered[at].astype(F32)
    for copy in range(near):
        message[copy] = kept.astype(BF16)


def branch_kernel(
    core,
    weights,
    x,
    halo,
    cosine,
    sine,
    decay,
    column,
    keys,
    values,
    base,
    before,
    fade,
    taps,
    keep,
    send,
    out_weight,
    weight,
    semaphores,
):
    rows = x.shape[0] * x.shape[1]
    own = core[0]
    start_at = pl.multiple_of(own * COLUMNS, HEAD)
    other_at = pl.multiple_of((1 - own) * COLUMNS, HEAD)
    copies = [
        pltpu.make_async_copy(weights.at[:, pl.ds(start_at, PROJECTED)], weight, semaphores.at[0]),
        pltpu.make_async_copy(
            weights.at[:, pl.ds(start_at + PROJECTED, 2 * HEAD)], out_weight.at[0], semaphores.at[1]
        ),
        pltpu.make_async_copy(
            weights.at[:, pl.ds(other_at + PROJECTED, 2 * HEAD)], out_weight.at[1], semaphores.at[2]
        ),
    ]
    for copy in copies:
        copy.start()
    incoming = jnp.concatenate([base[at].astype(F32) for at in range(base.shape[0])], axis=0)
    state = fade[0:1, :] * incoming + before[...]
    row = lax.broadcasted_iota(jnp.int32, (BLOCK, HEAD), 0)
    causal = lax.broadcasted_iota(jnp.int32, (BLOCK, BLOCK), 0) >= lax.broadcasted_iota(
        jnp.int32, (BLOCK, BLOCK), 1
    )
    tap = jnp.where(own == 0, taps[:, :HEAD].astype(F32), taps[:, HEAD:].astype(F32))
    start = jnp.zeros((1, 1), F32)
    per = BLOCK // HEAD
    copies[0].wait()
    rim = dot(halo[...], weight[:, HEAD : 3 * HEAD], ((1,), (0,))).astype(BF16).astype(F32)
    tail = (rim[:, :HEAD] * rim[:, HEAD:])[EXTRA - 8 :]
    for i in range(rows // BLOCK):
        at = pl.ds(i * BLOCK, BLOCK)
        projected = dot(block_rows(x, i), weight[...], ((1,), (0,))).astype(BF16)
        outer = projected[:, :HEAD].astype(F32)
        mixed = projected[:, HEAD : 2 * HEAD].astype(F32) * projected[:, 2 * HEAD : 3 * HEAD].astype(F32)
        one = jnp.where(row == 0, tail[7:8], pltpu.roll(mixed, 1, 0))
        two = jnp.where(row == 0, tail[6:7], jnp.where(row == 1, tail[7:8], pltpu.roll(mixed, 2, 0)))
        conv = tap[0:1] * two + tap[1:2] * one + tap[2:3] * mixed
        tail = mixed[BLOCK - 8 :]
        conv_branch = (outer * conv).astype(BF16)

        query = rotated(projected[:, 3 * HEAD : 4 * HEAD].astype(F32), cosine[at, :], sine[at, :])
        query = query.astype(BF16)
        key, value = keys[at, :], values[at, :]
        here = block_column(column, i)
        line = jnp.concatenate([decay[per * i + j : per * i + j + 1, :] for j in range(per)], axis=1)
        spread = jnp.where(causal, here - line, 0.0)
        scores = jnp.where(causal, dot(query, key, ((1,), (1,))) * jnp.exp(spread), 0.0)
        within = dot(scores.astype(BF16), value, ((1,), (0,)))
        across = dot(query, state.astype(BF16), ((1,), (0,))) * jnp.exp(here - start)
        retained = within + across
        end = line[:, BLOCK - 1 :]
        faded = (key.astype(F32) * jnp.exp(end - here)).astype(BF16)
        state = jnp.exp(end - start) * state + dot(faded, value, ((0,), (0,)))
        start = end
        normed = retained * lax.rsqrt(jnp.mean(retained * retained, axis=-1, keepdims=True) + EPSILON)
        gate = projected[:, 4 * HEAD :].astype(F32)
        ret_branch = (normed * (gate / (1.0 + jnp.exp(-gate)))).astype(BF16)

        half = (i * BLOCK) // (rows // 2)
        place = pl.ds(i * BLOCK - half * (rows // 2), BLOCK)

        @pl.when(own == half)
        def _():
            keep[place, :HEAD] = conv_branch
            keep[place, HEAD:] = ret_branch

        @pl.when(own != half)
        def _():
            send[place, :HEAD] = conv_branch
            send[place, HEAD:] = ret_branch

    copies[1].wait()
    copies[2].wait()


def out_kernel(mine, theirs, weight, out):
    parts, rows = out.shape[0], out.shape[1]
    step = 512
    for column in range(0, out.shape[2], step):
        at = pl.ds(column, step)
        total = dot(mine[...], weight[0, at, :], ((1,), (1,))) + dot(theirs[...], weight[1, at, :], ((1,), (1,)))
        total = total.astype(BF16)
        for part in range(parts):
            out[part, :, column : column + step] = total[part * rows : (part + 1) * rows]


def sum_kernel(parts, out):
    total = parts[0].astype(F32)
    for at in range(1, parts.shape[0]):
        total = total + parts[at].astype(F32)
    out[...] = total.astype(BF16)


def exchanged(x, axes):
    return lax.all_to_all(x, axes, 0, 0, tiled=True)


def body(
    tokens,
    norm_gain,
    conv_outer_weight,
    conv_inner_weight,
    conv_input_weight,
    query_matrix,
    key_weight,
    value_weight,
    gate_weight,
    conv_taps,
    conv_out_weight,
    ret_out_weight,
    log_decay,
):
    own_rows, width = tokens.shape
    tp = lax.axis_size("tp")
    chip = lax.axis_index(CHIPS)
    core = lax.axis_index("core")
    chips = lax.axis_size(CHIPS)
    near, far = lax.axis_size(NEAR), lax.axis_size("za")
    rows = 2 * tp * own_rows
    shard = key_weight.shape[0]

    rest, message = call(
        pack_kernel,
        [slow((shard, 2 * COLUMNS), BF16), fast((2, shard + EXTRA, 2 * HEAD), BF16)],
        "pack",
        specs=[PLAIN] * 10,
        limit=None,
    )(
        key_weight,
        value_weight,
        conv_outer_weight,
        conv_inner_weight,
        conv_input_weight,
        query_matrix,
        gate_weight,
        conv_out_weight.T,
        ret_out_weight.T,
        log_decay.T,
    )
    weights = lax.all_gather(rest, STRETCHES, axis=0, tiled=True)

    own = exchanged(message, "core")
    every_second = lax.all_gather(own.reshape(2 * (shard + EXTRA), 2 * HEAD), FAR)
    pairs = lax.axis_size("zc")
    gathered = exchanged(jnp.broadcast_to(every_second, (pairs, *every_second.shape)), "zc")

    (normed,) = call(norm_kernel, [slow((2 * tp, own_rows, width), BF16)], "norm", specs=[PLAIN] * 2, limit=None)(
        tokens, norm_gain.reshape(1, width)
    )
    x = exchanged(normed, ("core", "tp"))
    halo = lax.ppermute(x[-1, own_rows - EXTRA :], CHIPS, [(i, i + 1) for i in range(chips - 1)])

    inv_freq = ROTARY_BASE ** (-jnp.arange(HALF, dtype=F32) / HALF)
    inv_freq = jnp.concatenate([inv_freq, inv_freq])[None, :]
    far_angle = ((chip * rows).astype(F32) + BLOCK * jnp.arange(8, dtype=F32))[:, None] * inv_freq
    near_angle = jnp.arange(BLOCK, dtype=F32)[:, None] * inv_freq

    keys, values, cosine, sine, decay, column, totals, message = call(
        kv_kernel,
        [
            fast((rows, HEAD), BF16),
            fast((rows, HEAD), BF16),
            fast((rows, HEAD), F32),
            fast((rows, HEAD), F32),
            fast((rows // HEAD, HEAD), F32),
            fast((HEAD, HEAD), F32),
            fast((chips, HEAD), F32),
            fast((near, HEAD, HEAD), BF16),
        ],
        "kv",
        scratch=[pltpu.VMEM((width, 2 * HEAD), BF16)],
        flops=4 * rows * width * HEAD,
    )(x, gathered, own, jnp.cos(far_angle), jnp.sin(far_angle), jnp.cos(near_angle), jnp.sin(near_angle))

    share = HEAD // near
    block = lax.axis_index("za").reshape(1)
    message, before, fade = call(
        near_kernel,
        [fast((far, share, HEAD), BF16), fast((HEAD, HEAD), F32), fast((8, HEAD), F32)],
        "near",
        specs=[SMEM, SMEM, VMEM, VMEM],
        scratch=[pltpu.VMEM((HEAD, HEAD), F32)],
    )(lax.axis_index(NEAR).reshape(1), block, totals, exchanged(message, NEAR))
    (message,) = call(far_kernel, [fast((near, share, HEAD), BF16)], "far", specs=[SMEM, VMEM, VMEM])(
        block, totals, exchanged(message, "za")
    )
    base = exchanged(message, NEAR)

    keep, send, out_weight = call(
        branch_kernel,
        [fast((rows // 2, 2 * HEAD), BF16), fast((rows // 2, 2 * HEAD), BF16), fast((2, width, 2 * HEAD), BF16)],
        "branch",
        specs=[SMEM, ANY] + [VMEM] * 12,
        scratch=[pltpu.VMEM((width, PROJECTED), BF16), pltpu.SemaphoreType.DMA((3,))],
        flops=10 * rows * width * HEAD,
    )(
        core.reshape(1),
        weights,
        x,
        halo,
        cosine,
        sine,
        decay,
        column,
        keys,
        values,
        base,
        before,
        fade,
        conv_taps,
    )
    theirs = lax.ppermute(send, "core", [(0, 1), (1, 0)])
    (partial,) = call(out_kernel, [fast((tp, own_rows, width), BF16)], "out", flops=rows * width * 4 * HEAD)(
        keep, theirs, out_weight
    )
    (mixed,) = call(sum_kernel, [slow((own_rows, width), BF16)], "sum")(exchanged(partial, "tp"))
    return mixed


def solution(mesh):
    groups, stretches, tp = mesh.devices.shape
    chips = stretches // 2
    fine = Mesh(
        mesh.devices.reshape(groups, chips // 4, 2, 2, 2, tp), ("grp", "za", "zb", "zc", "core", "tp")
    )
    columns = P(STRETCHES, "tp")
    placed = (
        P(("grp", *STRETCHES, "tp"), None),
        P(),
        *([columns] * 7),
        P(None, "tp"),
        P("tp", STRETCHES),
        P("tp", STRETCHES),
        P(("grp", *STRETCHES), "tp"),
    )
    return jax.shard_map(
        body, mesh=fine, in_specs=placed, out_specs=P(("grp", *STRETCHES, "tp"), None), check_vma=False
    )
```

time: 311 us -> 252 us (0.81)
  blocking collectives: 189 us -> 106 us
  waiting for transfers between devices: 12.8 us -> 39.3 us
  starting transfers between devices: 49.9 us -> 66.2 us
  Pallas kernels: 31.8 us -> 22.4 us
  local copies, waits for them, and re-layouts: 9.53 us -> 3.59 us
    all_gather x2 -> x1, blocking collectives: 97.7 us -> 40.1 us  [body(): lax.all_gather(own.reshape(2 * (shard + EXTRA), 2 * HEAD), FAR)]
    all_to_all x4, starting transfers between devices: 22.4 us -> 56.4 us  [exchanged(): return lax.all_to_all(x, axes, 0, 0, tiled=True)]
    all_to_all x4, waiting for transfers between devices: 10.6 us -> 36.7 us  [exchanged(): return lax.all_to_all(x, axes, 0, 0, tiled=True)]
    all_to_all x3, blocking collectives: 91.5 us -> 65.4 us  [exchanged(): return lax.all_to_all(x, axes, 0, 0, tiled=True)]
    ppermute x3 -> x2, starting transfers between devices: 27.6 us -> 9.8 us  [the longest x1 6.48 us: body(): theirs = lax.ppermute(send, 'core', [(0, 1), (1, 0)])]
    pallas_call x8, Pallas kernels: 31.8 us -> 22.4 us  [run(): pl.pallas_call(kernel, out_shape=[o[0] for o in outs], in_specs=in_specs,...]
  transfers between devices with their start and end apart: 8 -> 7, of which waited for: 3 -> 4; matrix products, arithmetic and copies ran while one was open for 3% -> 2% of each run, Pallas kernels for 7% -> 4%
where the time goes in v2:
time: 252 us; the launch traced here: 251 us
  blocking collectives  106 us (42%)
  starting transfers between devices  66.2 us (26%)
  waiting for transfers between devices  39.3 us (16%)
  Pallas kernels  22.4 us (9%)
  between operations  13.5 us (5%)
  local copies, waits for them, and re-layouts  3.59 us (1%)
    all_to_all x3, blocking collectives, exchanged(): return lax.all_to_all(x, axes, 0, 0, tiled=True)  65.4 us
    all_to_all x4, starting transfers between devices, exchanged(): return lax.all_to_all(x, axes, 0, 0, tiled=True)  56.4 us
    all_gather x1, blocking collectives, body(): lax.all_gather(own.reshape(2 * (shard + EXTRA), 2 * HEAD), FAR)  40.1 us
    all_to_all x4, waiting for transfers between devices, exchanged(): return lax.all_to_all(x, axes, 0, 0, tiled=True)  36.7 us
    pallas_call x8, Pallas kernels, run(): pl.pallas_call(kernel, out_shape=[o[0] for o in outs], in_specs=in_specs,...  22.4 us
    ppermute x1, starting transfers between devices, body(): theirs = lax.ppermute(send, 'core', [(0, 1), (1, 0)])  6.48 us
  transfers between devices with their start and end apart: 7, of which 4 were waited for; matrix products, arithmetic and copies ran while one was open for 2% of the time, Pallas kernels for 4%

profile of v2, /device:TPU:33, one launch (start us, length us, event | category | flops | bytes accessed | tf_op | source)
XLA Modules:
  0.0 251.1 jit_solution(4622863805009996267)
XLA Ops:
  6.5 0.0 all-gather.2.cloned.1.call-start
  6.6 1.5 pack.1
  8.1 0.1 all-gather.2.cloned.1.call-update
  8.2 44.7 %all-to-all-start.1 = ((bf16[2,48,256]{2,1,0:T(8,128)(2,1)}), bf16[2,48,256]{2,1,0:T(8,128)(2,1)S(1)}, u32[]{:S(2)}, u32[]{:S(2)}) async-start(bf16[2,48,256]{2,1,0:T(8,128)(2,1)} %get-tuple-element.22), calls=%async_computation.1 | async-start | bytes 98304 | tf_op jit(solution)/shard_map/all_to_all | solution.py:329
  52.9 1.3 reshape.19.gain
  54.2 3.5 %norm.1 = bf16[8,128,2048]{2,1,0:T(8,128)(2,1)} custom-call(bf16[128,2048]{1,0:T(8,128)(2,1)} %tokens.1, bf16[1,2048]{1,0:T(2,128)(2,1)} %reshape.19.gain), custom_call_target="tpu_custom_call" | custom-call | tf_op jit(solution)/shard_map/norm/pallas_call | solution.py:36
  57.7 0.0 all-to-all-done.1.own
  57.7 4.6 %all-to-all-start = ((bf16[8,128,2048]{2,1,0:T(8,128)(2,1)}), bf16[8,128,2048]{2,1,0:T(8,128)(2,1)}, u32[]{:S(2)}, u32[]{:S(2)}) async-start(bf16[8,128,2048]{2,1,0:T(8,128)(2,1)} %norm.1), calls=%async_computation | async-start | bytes 8388608 | tf_op jit(solution)/shard_map/all_to_all | solution.py:329
  62.3 40.1 %all_gather.7 = bf16[16,96,256]{2,1,0:T(8,128)(2,1)S(1)} all-gather(bf16[1,96,256]{2,1,0:T(8,128)(2,1)S(1)} %bitcast.9), channel_id=1, replica_groups=mesh['grp'=2,'za'=8,'zb'=2,'zc'=2,'core'=2,'tp'=4] {'za','zb'}, dimensions={0}, use_global_device_ids=true | all-gather | bytes 835584 | tf_op jit(solution)/shard_map/all_gather | solution.py:377
  102.4 8.7 %all-to-all-done.x = bf16[8,128,2048]{2,1,0:T(8,128)(2,1)} async-done(((bf16[8,128,2048]{2,1,0:T(8,128)(2,1)}), bf16[8,128,2048]{2,1,0:T(8,128)(2,1)}, u32[]{:S(2)}, u32[]{:S(2)}) %all-to-all-start) | async-done | bytes 4194336 | tf_op jit(solution)/shard_map/all_to_all | solution.py:329
  111.1 1.5 broadcast_in_dim.2
  112.5 3.7 %all-to-all-start.2 = ((bf16[2,16,96,256]{3,2,1,0:T(8,128)(2,1)}), bf16[2,16,96,256]{3,2,1,0:T(8,128)(2,1)S(1)}, u32[]{:S(2)}, u32[]{:S(2)}) async-start(bf16[2,16,96,256]{3,2,1,0:T(8,128)(2,1)} %broadcast_in_dim.2), calls=%async_computation.2 | async-start | bytes 3145728 | tf_op jit(solution)/shard_map/all_to_all | solution.py:329
  116.3 0.1 pad_maximum_fusion
  116.3 0.1 multiply_sine_fusion
  116.5 0.5 fusion
  117.0 28.1 %all-to-all-done.2.gathered = bf16[2,16,96,256]{3,2,1,0:T(8,128)(2,1)S(1)} async-done(((bf16[2,16,96,256]{3,2,1,0:T(8,128)(2,1)}), bf16[2,16,96,256]{3,2,1,0:T(8,128)(2,1)S(1)}, u32[]{:S(2)}, u32[]{:S(2)}) %all-to-all-start.2) | async-done | bytes 1572896 | tf_op jit(solution)/shard_map/all_to_all | solution.py:329
  145.1 0.0 copy-start
  145.1 5.0 %kv.1 = (bf16[1024,128]{1,0:T(8,128)(2,1)S(1)}, bf16[1024,128]{1,0:T(8,128)(2,1)S(1)}, f32[1024,128]{1,0:T(8,128)S(1)}, f32[1024,128]{1,0:T(8,128)S(1)}, f32[8,1...) custom-call(bf16[8,128,2048]{2,1,0:T(8,128)(2,1)} %all-to-all-done.x, ...), custom_call_target="tpu_custom_call" | custom-call | flops 1073741824 | tf_op jit(solution)/shard_map/kv/pallas_call | solution.py:36
  150.1 7.7 %all_to_all.35.gathered = bf16[4,128,128]{2,1,0:T(8,128)(2,1)S(1)} all-to-all(bf16[4,128,128]{2,1,0:T(8,128)(2,1)S(1)} %get-tuple-element.30), channel_id=1, replica_groups=mesh['grp'=2,'za'=8,'zb'=2,'zc'=2,'core'=2,'tp'=4] {'zb','zc'}, dimensions={0} | all-to-all | bytes 262144 | tf_op jit(solution)/shard_map/all_to_all | solution.py:329
  157.8 29.3 %all_to_all.36.gathered = bf16[8,32,128]{2,1,0:T(8,128)(2,1)S(1)} all-to-all(bf16[8,32,128]{2,1,0:T(8,128)(2,1)S(1)} %get-tuple-element.31), channel_id=1, replica_groups=mesh['grp'=2,'za'=8,'zb'=2,'zc'=2,'core'=2,'tp'=4] {'za'}, dimensions={0} | all-to-all | bytes 131072 | tf_op jit(solution)/shard_map/all_to_all | solution.py:329
  187.1 0.6 far.1
  187.7 3.4 %all-to-all-start.5 = ((bf16[4,32,128]{2,1,0:T(8,128)(2,1)}), bf16[4,32,128]{2,1,0:T(8,128)(2,1)S(1)}, u32[]{:S(2)}, u32[]{:S(2)}) async-start(bf16[4,32,128]{2,1,0:T(8,128)(2,1)} %far.1), calls=%async_computation.5 | async-start | bytes 65536 | tf_op jit(solution)/shard_map/all_to_all | solution.py:329
  191.1 0.8 slice_bitcast_fusion
  191.9 3.3 %collective-permute-start = (bf16[16,2048]{1,0:T(8,128)(2,1)S(1)}, bf16[16,2048]{1,0:T(8,128)(2,1)S(1)}, u32[]{:S(2)}, u32[]{:S(2)}) collective-permute-start(bf16[16,2048]{1,0:T(8,128)(2,1)S(1)} %slice_bitcast_fusion), channel_id=1, source_target_pairs={{0,8},{8,16},{16,24},{24,32},{32,40},{40,48},{48,56},{56,64},{64,7... | collective-permute-start | bytes 196616 | tf_op jit(solution)/shard_map/ppermute | solution.py:385
  195.3 1.3 collective-permute-done.halo
  196.6 0.0 all-to-all-done.5.base
  196.6 0.0 all-gather.2.cloned.1.call-done.weights
  196.6 0.0 copy-done
  196.6 9.3 %branch.1 = (bf16[512,256]{1,0:T(8,128)(2,1)S(1)}, bf16[512,256]{1,0:T(8,128)(2,1)S(1)}, bf16[2,2048,256]{2,1,0:T(8,128)(2,1)S(1)}) custom-call(s32[1]{0:T(128)} %bitcast.core, bf16[2048,1792]{1,0:T(8,128)(2,1)} %all-gather.2.cloned.1.call-done.weights, bf16[8,128,2048]{2,1,0:T(8,128)(2,1)} %all-to-all-done.x, ...), custom_call_target="tpu_custom_call" | custom-call | flops 2684354560 | tf_op jit(solution)/shard_map/branch/pallas_call | solution.py:36
  205.9 6.5 %collective-permute-start.1 = (bf16[512,256]{1,0:T(8,128)(2,1)S(1)}, bf16[512,256]{1,0:T(8,128)(2,1)S(1)}, u32[]{:S(2)}, u32[]{:S(2)}) collective-permute-start(bf16[512,256]{1,0:T(8,128)(2,1)S(1)} %get-tuple-element.35), channel_id=1, source_target_pairs={{0,4},{4,0},{1,5},{5,1},{2,6},{6,2},{3,7},{7,3},{8,12},{12,8},{9,1... | collective-permute-start | bytes 786440 | tf_op jit(solution)/shard_map/ppermute | solution.py:446
  212.4 1.1 collective-permute-done.1.theirs
  213.5 1.3 out.1
  214.8 28.4 %all_to_all.37.parts = bf16[4,128,2048]{2,1,0:T(8,128)(2,1)S(1)} all-to-all(bf16[4,128,2048]{2,1,0:T(8,128)(2,1)S(1)} %out.1), channel_id=1, replica_groups=mesh['grp'=2,'za'=8,'zb'=2,'zc'=2,'core'=2,'tp'=4] {'tp'}, dimensions={0} | all-to-all | bytes 4194304 | tf_op jit(solution)/shard_map/all_to_all | solution.py:329
  243.2 1.0 sum.1
  (3 shorter events, 0.1 us)
Async XLA Ops:
  6.5 190.1 %all-gather.2.cloned.1.call-start = ((), (), s32[]{:S(2)}) async-start(), calls=%async_computation.7 | async-start | bytes 7454720 | tf_op jit(solution)/shard_map/all_gather | solution.py:374
  8.2 49.5 %all-to-all-start.1 = ((bf16[2,48,256]{2,1,0:T(8,128)(2,1)}), bf16[2,48,256]{2,1,0:T(8,128)(2,1)S(1)}, u32[]{:S(2)}, u32[]{:S(2)}) async-start(bf16[2,48,256]{2,1,0:T(8,128)(2,1)} %get-tuple-element.22), calls=%async_computation.1 | async-start | bytes 98304 | tf_op jit(solution)/shard_map/all_to_all | solution.py:329
  57.7 53.4 %all-to-all-start = ((bf16[8,128,2048]{2,1,0:T(8,128)(2,1)}), bf16[8,128,2048]{2,1,0:T(8,128)(2,1)}, u32[]{:S(2)}, u32[]{:S(2)}) async-start(bf16[8,128,2048]{2,1,0:T(8,128)(2,1)} %norm.1), calls=%async_computation | async-start | bytes 8388608 | tf_op jit(solution)/shard_map/all_to_all | solution.py:329
  112.5 32.5 %all-to-all-start.2 = ((bf16[2,16,96,256]{3,2,1,0:T(8,128)(2,1)}), bf16[2,16,96,256]{3,2,1,0:T(8,128)(2,1)S(1)}, u32[]{:S(2)}, u32[]{:S(2)}) async-start(bf16[2,16,96,256]{3,2,1,0:T(8,128)(2,1)} %broadcast_in_dim.2), calls=%async_computation.2 | async-start | bytes 3145728 | tf_op jit(solution)/shard_map/all_to_all | solution.py:329
  145.1 51.5 %copy-start = (bf16[3,256]{1,0:T(4,128)(2,1)S(1)}, bf16[3,256]{1,0:T(4,128)(2,1)}, u32[]{:S(2)}) copy-start(bf16[3,256]{1,0:T(4,128)(2,1)} %taps.1) | copy-start | bytes 4612
  187.7 8.9 %all-to-all-start.5 = ((bf16[4,32,128]{2,1,0:T(8,128)(2,1)}), bf16[4,32,128]{2,1,0:T(8,128)(2,1)S(1)}, u32[]{:S(2)}, u32[]{:S(2)}) async-start(bf16[4,32,128]{2,1,0:T(8,128)(2,1)} %far.1), calls=%async_computation.5 | async-start | bytes 65536 | tf_op jit(solution)/shard_map/all_to_all | solution.py:329
  191.9 4.6 %collective-permute-start = (bf16[16,2048]{1,0:T(8,128)(2,1)S(1)}, bf16[16,2048]{1,0:T(8,128)(2,1)S(1)}, u32[]{:S(2)}, u32[]{:S(2)}) collective-permute-start(bf16[16,2048]{1,0:T(8,128)(2,1)S(1)} %slice_bitcast_fusion), channel_id=1, source_target_pairs={{0,8},{8,16},{16,24},{24,32},{32,40},{40,48},{48,56},{56,64},{64,7... | collective-permute-start | bytes 196616 | tf_op jit(solution)/shard_map/ppermute | solution.py:385
  205.9 7.6 %collective-permute-start.1 = (bf16[512,256]{1,0:T(8,128)(2,1)S(1)}, bf16[512,256]{1,0:T(8,128)(2,1)S(1)}, u32[]{:S(2)}, u32[]{:S(2)}) collective-permute-start(bf16[512,256]{1,0:T(8,128)(2,1)S(1)} %get-tuple-element.35), channel_id=1, source_target_pairs={{0,4},{4,0},{1,5},{5,1},{2,6},{6,2},{3,7},{7,3},{8,12},{12,8},{9,1... | collective-permute-start | bytes 786440 | tf_op jit(solution)/shard_map/ppermute | solution.py:446
Sparse Core Ops, SparseCore 0:
  9.5 171.4 all-gather.1

commit v3 on v2

--- a/solution.py
+++ b/solution.py
@@ -11,9 +11,9 @@
 EPSILON = 1e-06
 ROTARY_BASE = 10000.0
 BLOCK = 256
-EXTRA = 16
+EXTRA = 8
+RIM = 16
 PROJECTED = 5 * HEAD
-COLUMNS = 7 * HEAD
 INTERPRET = False
 
 BF16 = jnp.bfloat16
@@ -66,16 +66,14 @@
     return lax.dot_general(a, b, (dims, ((), ())), preferred_element_type=F32)
 
 
-def pack_kernel(key, value, *refs):
-    *inputs, logs, rest, message = refs
-    for at, ref in enumerate(inputs):
-        for core in range(2):
-            to = core * COLUMNS + at * HEAD
-            rest[:, to : to + HEAD] = ref[:, core * HEAD : (core + 1) * HEAD]
+def pack_kernel(key, value, conv_out, ret_out, logs, message, outs):
     shard = key.shape[0]
+    parts = []
     for core in range(2):
-        message[core, :shard, :HEAD] = key[:, core * HEAD : (core + 1) * HEAD]
-        message[core, :shard, HEAD:] = value[:, core * HEAD : (core + 1) * HEAD]
+        half = slice(core * HEAD, (core + 1) * HEAD)
+        parts += [conv_out[:, half], ret_out[:, half]]
+        message[core, :shard, :HEAD] = key[:, half]
+        message[core, :shard, HEAD:] = value[:, half]
         lines = [logs[core : core + 1, at : at + 2 * HEAD] for at in range(0, logs.shape[1], 2 * HEAD)]
         line = jnp.concatenate(lines, axis=0)
         high = line.astype(BF16).astype(F32)
@@ -83,6 +81,21 @@
         low = line - high - middle
         filler = jnp.zeros((EXTRA - 3 * len(lines), 2 * HEAD), F32)
         message[core, shard:, :] = jnp.concatenate([high, middle, low, filler], axis=0).astype(BF16)
+    both = jnp.concatenate(parts, axis=1)
+    for copy in range(outs.shape[0]):
+        outs[copy] = both
+
+
+def join_kernel(*refs):
+    *inputs, outs, rest = refs
+    for at, ref in enumerate(inputs):
+        for core in range(2):
+            to = core * PROJECTED + at * HEAD
+            rest[:, to : to + HEAD] = ref[:, core * HEAD : (core + 1) * HEAD]
+    each = outs.shape[2]
+    for part in range(outs.shape[0]):
+        to = 2 * PROJECTED + part * each
+        rest[:, to : to + each] = outs[part]
 
 
 def logs_of(rows, lines):
@@ -93,7 +106,7 @@
 def norm_kernel(tokens, gain, out):
     values = tokens[...].astype(F32)
     scale = lax.rsqrt(jnp.mean(values * values, axis=-1, keepdims=True) + EPSILON)
-    normed = (values * scale * gain[...].astype(F32)).astype(BF16)
+    normed = (values * scale * gain[...].astype(F32)[None, :]).astype(BF16)
     for copy in range(out.shape[0]):
         out[copy] = normed
 
@@ -103,10 +116,10 @@
 
 
 def kv_kernel(
-    x, gathered, own, cos_far, sin_far, cos_near, sin_near, k_out, v_out, cosine, sine, decay, column, totals, message, weight
+    pair, x, same, other, own, cos_far, sin_far, cos_near, sin_near, k_out, v_out, cosine, sine, decay, column, totals, message, weight
 ):
     rows, width = x.shape[0] * x.shape[1], x.shape[2]
-    pairs, fars = gathered.shape[:2]
+    fars = same.shape[0]
     shard = own.shape[1] - EXTRA
     lines = rows // 2 // (2 * HEAD)
 
@@ -135,18 +148,17 @@
     column[...] = jnp.concatenate([cumulative, filler], axis=0).T
     total = before
 
-    for far in range(fars):
-        for pair in range(pairs):
-            chip = far * pairs + pair
+    for source, place in ((same, pair[0]), (other, 1 - pair[0])):
+        for far in range(fars):
+            chip = 2 * far + place
             log_total = jnp.zeros((1, 1), F32)
             for core in range(2):
                 at = core * (shard + EXTRA)
-                weight[(2 * chip + core) * shard : (2 * chip + core + 1) * shard, :] = gathered[
-                    pair, far, at : at + shard, :
-                ]
-                logs = logs_of(gathered[pair, far, at + shard : at + shard + EXTRA, :], lines)
+                to = pl.multiple_of((2 * chip + core) * shard, shard)
+                weight[pl.ds(to, shard), :] = source[far, at : at + shard, :]
+                logs = logs_of(source[far, at + shard : at + shard + EXTRA, :], lines)
                 log_total = log_total + jnp.sum(logs, axis=(0, 1), keepdims=True)
-            totals[chip : chip + 1, :] = jnp.broadcast_to(log_total, (1, HEAD))
+            totals[pl.ds(chip, 1), :] = jnp.broadcast_to(log_total, (1, HEAD))
 
     state = jnp.zeros((HEAD, HEAD), F32)
     for i in range(rows // BLOCK):
@@ -228,23 +240,18 @@
     before,
     fade,
     taps,
-    keep,
-    send,
+    branches,
     out_weight,
     weight,
     semaphores,
 ):
     rows = x.shape[0] * x.shape[1]
     own = core[0]
-    start_at = pl.multiple_of(own * COLUMNS, HEAD)
-    other_at = pl.multiple_of((1 - own) * COLUMNS, HEAD)
+    start_at = pl.multiple_of(own * PROJECTED, HEAD)
     copies = [
         pltpu.make_async_copy(weights.at[:, pl.ds(start_at, PROJECTED)], weight, semaphores.at[0]),
         pltpu.make_async_copy(
-            weights.at[:, pl.ds(start_at + PROJECTED, 2 * HEAD)], out_weight.at[0], semaphores.at[1]
-        ),
-        pltpu.make_async_copy(
-            weights.at[:, pl.ds(other_at + PROJECTED, 2 * HEAD)], out_weight.at[1], semaphores.at[2]
+            weights.at[:, pl.ds(2 * PROJECTED, out_weight.shape[1])], out_weight, semaphores.at[1]
         ),
     ]
     for copy in copies:
@@ -260,7 +267,7 @@
     per = BLOCK // HEAD
     copies[0].wait()
     rim = dot(halo[...], weight[:, HEAD : 3 * HEAD], ((1,), (0,))).astype(BF16).astype(F32)
-    tail = (rim[:, :HEAD] * rim[:, HEAD:])[EXTRA - 8 :]
+    tail = (rim[:, :HEAD] * rim[:, HEAD:])[RIM - 8 :]
     for i in range(rows // BLOCK):
         at = pl.ds(i * BLOCK, BLOCK)
         projected = dot(block_rows(x, i), weight[...], ((1,), (0,))).astype(BF16)
@@ -290,39 +297,22 @@
         gate = projected[:, 4 * HEAD :].astype(F32)
         ret_branch = (normed * (gate / (1.0 + jnp.exp(-gate)))).astype(BF16)
 
-        half = (i * BLOCK) // (rows // 2)
-        place = pl.ds(i * BLOCK - half * (rows // 2), BLOCK)
-
-        @pl.when(own == half)
-        def _():
-            keep[place, :HEAD] = conv_branch
-            keep[place, HEAD:] = ret_branch
-
-        @pl.when(own != half)
-        def _():
-            send[place, :HEAD] = conv_branch
-            send[place, HEAD:] = ret_branch
+        per_part = branches.shape[1]
+        for part in range(BLOCK // per_part):
+            rows_at = slice(part * per_part, (part + 1) * per_part)
+            branches[i * BLOCK // per_part + part, :, :HEAD] = conv_branch[rows_at]
+            branches[i * BLOCK // per_part + part, :, HEAD:] = ret_branch[rows_at]
 
     copies[1].wait()
-    copies[2].wait()
-
-
-def out_kernel(mine, theirs, weight, out):
-    parts, rows = out.shape[0], out.shape[1]
+
+
+def out_kernel(branches, weight, out):
+    parts = branches.shape[0] // 2
+    order = [branches[core * parts + part] for part in range(parts) for core in range(2)]
+    rows = jnp.concatenate(order, axis=1)
     step = 512
-    for column in range(0, out.shape[2], step):
-        at = pl.ds(column, step)
-        total = dot(mine[...], weight[0, at, :], ((1,), (1,))) + dot(theirs[...], weight[1, at, :], ((1,), (1,)))
-        total = total.astype(BF16)
-        for part in range(parts):
-            out[part, :, column : column + step] = total[part * rows : (part + 1) * rows]
-
-
-def sum_kernel(parts, out):
-    total = parts[0].astype(F32)
-    for at in range(1, parts.shape[0]):
-        total = total + parts[at].astype(F32)
-    out[...] = total.astype(BF16)
+    for column in range(0, out.shape[1], step):
+        out[:, column : column + step] = dot(rows, weight[column : column + step, :], ((1,), (1,))).astype(BF16)
 
 
 def exchanged(x, axes):
@@ -353,36 +343,28 @@
     rows = 2 * tp * own_rows
     shard = key_weight.shape[0]
 
-    rest, message = call(
+    message, outs = call(
         pack_kernel,
-        [slow((shard, 2 * COLUMNS), BF16), fast((2, shard + EXTRA, 2 * HEAD), BF16)],
+        [fast((2, shard + EXTRA, 2 * HEAD), BF16), fast((tp, shard, 4 * HEAD), BF16)],
         "pack",
-        specs=[PLAIN] * 10,
+        specs=[PLAIN] * 5,
         limit=None,
-    )(
-        key_weight,
-        value_weight,
-        conv_outer_weight,
-        conv_inner_weight,
-        conv_input_weight,
-        query_matrix,
-        gate_weight,
-        conv_out_weight.T,
-        ret_out_weight.T,
-        log_decay.T,
-    )
+    )(key_weight, value_weight, conv_out_weight.T, ret_out_weight.T, log_decay.T)
+    inputs = (conv_outer_weight, conv_inner_weight, conv_input_weight, query_matrix, gate_weight)
+    (rest,) = call(
+        join_kernel, [slow((shard, 2 * PROJECTED + 4 * HEAD * tp), BF16)], "join", specs=[PLAIN] * 6, limit=None
+    )(*inputs, exchanged(outs, "tp"))
     weights = lax.all_gather(rest, STRETCHES, axis=0, tiled=True)
 
     own = exchanged(message, "core")
-    every_second = lax.all_gather(own.reshape(2 * (shard + EXTRA), 2 * HEAD), FAR)
-    pairs = lax.axis_size("zc")
-    gathered = exchanged(jnp.broadcast_to(every_second, (pairs, *every_second.shape)), "zc")
+    same = lax.all_gather(own.reshape(2 * (shard + EXTRA), 2 * HEAD), FAR)
+    other = lax.ppermute(same, "zc", [(0, 1), (1, 0)])
 
     (normed,) = call(norm_kernel, [slow((2 * tp, own_rows, width), BF16)], "norm", specs=[PLAIN] * 2, limit=None)(
-        tokens, norm_gain.reshape(1, width)
+        tokens, norm_gain
     )
     x = exchanged(normed, ("core", "tp"))
-    halo = lax.ppermute(x[-1, own_rows - EXTRA :], CHIPS, [(i, i + 1) for i in range(chips - 1)])
+    halo = lax.ppermute(x[-1, own_rows - RIM :], CHIPS, [(i, i + 1) for i in range(chips - 1)])
 
     inv_freq = ROTARY_BASE ** (-jnp.arange(HALF, dtype=F32) / HALF)
     inv_freq = jnp.concatenate([inv_freq, inv_freq])[None, :]
@@ -402,9 +384,10 @@
             fast((near, HEAD, HEAD), BF16),
         ],
         "kv",
+        specs=[SMEM] + [VMEM] * 8,
         scratch=[pltpu.VMEM((width, 2 * HEAD), BF16)],
         flops=4 * rows * width * HEAD,
-    )(x, gathered, own, jnp.cos(far_angle), jnp.sin(far_angle), jnp.cos(near_angle), jnp.sin(near_angle))
+    )(lax.axis_index("zc").reshape(1), x, same, other, own, jnp.cos(far_angle), jnp.sin(far_angle), jnp.cos(near_angle), jnp.sin(near_angle))
 
     share = HEAD // near
     block = lax.axis_index("za").reshape(1)
@@ -420,12 +403,13 @@
     )
     base = exchanged(message, NEAR)
 
-    keep, send, out_weight = call(
+    parts = 2 * tp
+    branches, out_weight = call(
         branch_kernel,
-        [fast((rows // 2, 2 * HEAD), BF16), fast((rows // 2, 2 * HEAD), BF16), fast((2, width, 2 * HEAD), BF16)],
+        [fast((parts, own_rows, 2 * HEAD), BF16), fast((width, 2 * HEAD * parts), BF16)],
         "branch",
         specs=[SMEM, ANY] + [VMEM] * 12,
-        scratch=[pltpu.VMEM((width, PROJECTED), BF16), pltpu.SemaphoreType.DMA((3,))],
+        scratch=[pltpu.VMEM((width, PROJECTED), BF16), pltpu.SemaphoreType.DMA((2,))],
         flops=10 * rows * width * HEAD,
     )(
         core.reshape(1),
@@ -443,11 +427,9 @@
         fade,
         conv_taps,
     )
-    theirs = lax.ppermute(send, "core", [(0, 1), (1, 0)])
-    (partial,) = call(out_kernel, [fast((tp, own_rows, width), BF16)], "out", flops=rows * width * 4 * HEAD)(
-        keep, theirs, out_weight
-    )
-    (mixed,) = call(sum_kernel, [slow((own_rows, width), BF16)], "sum")(exchanged(partial, "tp"))
+    (mixed,) = call(out_kernel, [slow((own_rows, width), BF16)], "out", flops=rows * width * 4 * HEAD)(
+        exchanged(branches, ("core", "tp")), out_weight
+    )
     return mixed
 
 

time: 252 us -> 242 us (0.960)
  waiting for transfers between devices: 39.3 us -> 30.4 us
  starting transfers between devices: 66.2 us -> 59.3 us
  blocking collectives: 106 us -> 112 us
  local copies, waits for them, and re-layouts: 3.59 us -> 0.85 us
    all_to_all x4 -> x3, waiting for transfers between devices: 36.7 us -> 0.01 us  [exchanged(): return lax.all_to_all(x, axes, 0, 0, tiled=True)]
    ppermute x2, waiting for transfers between devices: 2.45 us -> 24.6 us  [the longest x1 23.1 us: body(): other = lax.ppermute(same, 'zc', [(0, 1), (1, 0)])]
    all_to_all x3 -> x4, blocking collectives: 65.4 us -> 72.8 us  [exchanged(): return lax.all_to_all(x, axes, 0, 0, tiled=True)]
    all_gather x1, waiting for transfers between devices: 0.01 us -> 5.8 us  [body(): weights = lax.all_gather(rest, STRETCHES, axis=0, tiled=True)]
    all_to_all x4 -> x3, starting transfers between devices: 56.4 us -> 51.9 us  [exchanged(): return lax.all_to_all(x, axes, 0, 0, tiled=True)]
  transfers between devices with their start and end apart: 7 -> 6, of which waited for: 4 -> 3; matrix products, arithmetic and copies ran while one was open for 2% -> 1% of each run, Pallas kernels for 4% -> 4%
where the time goes in v3:
time: 242 us; the launch traced here: 241 us
  blocking collectives  112 us (46%)
  starting transfers between devices  59.3 us (25%)
  waiting for transfers between devices  30.4 us (13%)
  Pallas kernels  24.3 us (10%)
  between operations  13.5 us (6%)
    all_to_all x4, blocking collectives, exchanged(): return lax.all_to_all(x, axes, 0, 0, tiled=True)  72.8 us
    all_to_all x3, starting transfers between devices, exchanged(): return lax.all_to_all(x, axes, 0, 0, tiled=True)  51.9 us
    all_gather x1, blocking collectives, body(): same = lax.all_gather(own.reshape(2 * (shard + EXTRA), 2 * HEAD), FAR)  38.9 us
    pallas_call x8, Pallas kernels, run(): pl.pallas_call(kernel, out_shape=[o[0] for o in outs], in_specs=in_specs,...  24.3 us
    ppermute x1, waiting for transfers between devices, body(): other = lax.ppermute(same, 'zc', [(0, 1), (1, 0)])  23.1 us
    all_gather x1, waiting for transfers between devices, body(): weights = lax.all_gather(rest, STRETCHES, axis=0, tiled=True)  5.8 us
  transfers between devices with their start and end apart: 6, of which 3 were waited for; matrix products, arithmetic and copies ran while one was open for 1% of the time, Pallas kernels for 4%

profile of v3, /device:TPU:33, one launch (start us, length us, event | category | flops | bytes accessed | tf_op | source)
XLA Modules:
  0.0 240.8 jit_solution(9965318915159827697)
XLA Ops:
  6.5 0.0 all-gather.2.cloned.1.call-start
  6.6 1.4 pack.1
  8.0 9.8 %all_to_all.35.refs_5_ = bf16[4,32,512]{2,1,0:T(8,128)(2,1)} all-to-all(bf16[4,32,512]{2,1,0:T(8,128)(2,1)S(1)} %get-tuple-element.20), channel_id=1, replica_groups=mesh['grp'=2,'za'=8,'zb'=2,'zc'=2,'core'=2,'tp'=4] {'tp'}, dimensions={0} | all-to-all | bytes 262144 | tf_op jit(solution)/shard_map/all_to_all | solution.py:319
  17.8 1.7 join.1
  19.5 0.1 all-gather.2.cloned.1.call-update
  19.6 43.9 %all-to-all-start.2 = ((bf16[2,40,256]{2,1,0:T(8,128)(2,1)}), bf16[2,40,256]{2,1,0:T(8,128)(2,1)S(1)}, u32[]{:S(2)}, u32[]{:S(2)}) async-start(bf16[2,40,256]{2,1,0:T(8,128)(2,1)} %get-tuple-element.21), calls=%async_computation.2 | async-start | bytes 81920 | tf_op jit(solution)/shard_map/all_to_all | solution.py:319
  63.5 3.5 %norm.1 = bf16[8,128,2048]{2,1,0:T(8,128)(2,1)} custom-call(bf16[128,2048]{1,0:T(8,128)(2,1)} %tokens.1, bf16[2048]{0:T(1024)(128)(2,1)} %gain.1), custom_call_target="tpu_custom_call" | custom-call | tf_op jit(solution)/shard_map/norm/pallas_call | solution.py:36
  67.0 0.0 all-to-all-done.2.own
  67.0 4.6 %all-to-all-start.1 = ((bf16[8,128,2048]{2,1,0:T(8,128)(2,1)}), bf16[8,128,2048]{2,1,0:T(8,128)(2,1)}, u32[]{:S(2)}, u32[]{:S(2)}) async-start(bf16[8,128,2048]{2,1,0:T(8,128)(2,1)} %norm.1), calls=%async_computation.1 | async-start | bytes 8388608 | tf_op jit(solution)/shard_map/all_to_all | solution.py:319
  71.6 0.0 copy-start
  71.6 38.9 %all_gather.7.same = bf16[16,80,256]{2,1,0:T(8,128)(2,1)S(1)} all-gather(bf16[1,80,256]{2,1,0:T(8,128)(2,1)S(1)} %bitcast.10), channel_id=1, replica_groups=mesh['grp'=2,'za'=8,'zb'=2,'zc'=2,'core'=2,'tp'=4] {'za','zb'}, dimensions={0}, use_global_device_ids=true | all-gather | bytes 696320 | tf_op jit(solution)/shard_map/all_gather | solution.py:360
  110.6 3.7 %collective-permute-start.1 = (bf16[16,80,256]{2,1,0:T(8,128)(2,1)S(1)}, bf16[16,80,256]{2,1,0:T(8,128)(2,1)S(1)}, u32[]{:S(2)}, u32[]{:S(2)}) collective-permute-start(bf16[16,80,256]{2,1,0:T(8,128)(2,1)S(1)} %all_gather.7.same), channel_id=1, source_target_pairs={{0,8},{8,0},{1,9},{9,1},{2,10},{10,2},{3,11},{11,3},{4,12},{12,4},... | collective-permute-start | bytes 1966088 | tf_op jit(solution)/shard_map/ppermute | solution.py:361
  114.3 0.1 pad_maximum_fusion
  114.4 0.1 multiply_sine_fusion
  114.5 0.5 fusion
  115.0 23.1 %collective-permute-done.1.other = bf16[16,80,256]{2,1,0:T(8,128)(2,1)S(1)} collective-permute-done((bf16[16,80,256]{2,1,0:T(8,128)(2,1)S(1)}, bf16[16,80,256]{2,1,0:T(8,128)(2,1)S(1)}, u32[]{:S(2)}, u32[]{:S(2)}) %collective-permute-start.1) | collective-permute-done | bytes 655392 | tf_op jit(solution)/shard_map/ppermute | solution.py:361
  138.1 0.0 all-to-all-done.1.x
  138.1 5.0 %kv.1 = (bf16[1024,128]{1,0:T(8,128)(2,1)S(1)}, bf16[1024,128]{1,0:T(8,128)(2,1)S(1)}, f32[1024,128]{1,0:T(8,128)S(1)}, f32[1024,128]{1,0:T(8,128)S(1)}, f32[8,1...) custom-call(s32[1]{0:T(128)} %bitcast.5.pair, ...), custom_call_target="tpu_custom_call" | custom-call | flops 1073741824 | tf_op jit(solution)/shard_map/kv/pallas_call | solution.py:36
  143.1 13.7 %all_to_all.36.gathered = bf16[4,128,128]{2,1,0:T(8,128)(2,1)S(1)} all-to-all(bf16[4,128,128]{2,1,0:T(8,128)(2,1)S(1)} %get-tuple-element.29), channel_id=1, replica_groups=mesh['grp'=2,'za'=8,'zb'=2,'zc'=2,'core'=2,'tp'=4] {'zb','zc'}, dimensions={0} | all-to-all | bytes 262144 | tf_op jit(solution)/shard_map/all_to_all | solution.py:319
  156.8 31.4 %all_to_all.37.gathered = bf16[8,32,128]{2,1,0:T(8,128)(2,1)S(1)} all-to-all(bf16[8,32,128]{2,1,0:T(8,128)(2,1)S(1)} %get-tuple-element.30), channel_id=1, replica_groups=mesh['grp'=2,'za'=8,'zb'=2,'zc'=2,'core'=2,'tp'=4] {'za'}, dimensions={0} | all-to-all | bytes 131072 | tf_op jit(solution)/shard_map/all_to_all | solution.py:319
  188.2 0.6 far.1
  188.9 3.4 %all-to-all-start.5 = ((bf16[4,32,128]{2,1,0:T(8,128)(2,1)}), bf16[4,32,128]{2,1,0:T(8,128)(2,1)S(1)}, u32[]{:S(2)}, u32[]{:S(2)}) async-start(bf16[4,32,128]{2,1,0:T(8,128)(2,1)} %far.1), calls=%async_computation.5 | async-start | bytes 65536 | tf_op jit(solution)/shard_map/all_to_all | solution.py:319
  192.2 0.8 slice_bitcast_fusion
  193.1 3.7 %collective-permute-start = (bf16[16,2048]{1,0:T(8,128)(2,1)S(1)}, bf16[16,2048]{1,0:T(8,128)(2,1)S(1)}, u32[]{:S(2)}, u32[]{:S(2)}) collective-permute-start(bf16[16,2048]{1,0:T(8,128)(2,1)S(1)} %slice_bitcast_fusion), channel_id=1, source_target_pairs={{0,8},{8,16},{16,24},{24,32},{32,40},{40,48},{48,56},{56,64},{64,7... | collective-permute-start | bytes 196616 | tf_op jit(solution)/shard_map/ppermute | solution.py:367
  196.7 1.5 collective-permute-done.halo
  198.2 0.0 all-to-all-done.5.base
  198.2 5.8 %all-gather.2.cloned.1.call-done.weights = bf16[2048,3328]{1,0:T(8,128)(2,1)} async-done(((bf16[32,3328]{1,0:T(8,128)(2,1)}), bf16[2048,3328]{1,0:T(8,128)(2,1)}) %all-gather.2.cloned.1.call-update) | async-done | bytes 13631504 | tf_op jit(solution)/shard_map/all_gather | solution.py:357
  204.0 0.0 copy-done
  204.0 8.4 %branch.1 = (bf16[8,128,256]{2,1,0:T(8,128)(2,1)S(1)}, bf16[2048,2048]{1,0:T(8,128)(2,1)S(1)}) custom-call(s32[1]{0:T(128)} %bitcast.core, bf16[2048,3328]{1,0:T(8,128)(2,1)} %all-gather.2.cloned.1.call-done.weights, bf16[8,128,2048]{2,1,0:T(8,128)(2,1)} %all-to-all-done.1.x, bf16[16,2048]{1,0:T(8,128)(2,1)S(1)} %collective-permute-done.halo, ...), custom_call_target="tpu_custom_call" | custom-call | flops 2684354560 | tf_op jit(solution)/shard_map/branch/pallas_call | solution.py:36
  212.4 17.9 %all_to_all.38.branches = bf16[8,128,256]{2,1,0:T(8,128)(2,1)S(1)} all-to-all(bf16[8,128,256]{2,1,0:T(8,128)(2,1)S(1)} %get-tuple-element.33), channel_id=1, replica_groups=mesh['grp'=2,'za'=8,'zb'=2,'zc'=2,'core'=2,'tp'=4] {'core','tp'}, dimensions={0} | all-to-all | bytes 1048576 | tf_op jit(solution)/shard_map/all_to_all | solution.py:319
  230.4 3.6 %out.1 = bf16[128,2048]{1,0:T(8,128)(2,1)} custom-call(bf16[8,128,256]{2,1,0:T(8,128)(2,1)S(1)} %all_to_all.38.branches, bf16[2048,2048]{1,0:T(8,128)(2,1)S(1)} %get-tuple-element.34.weight), custom_call_target="tpu_custom_call" | custom-call | flops 1073741824 | tf_op jit(solution)/shard_map/out/pallas_call | solution.py:36
  (3 shorter events, 0.1 us)
Async XLA Ops:
  6.5 197.5 %all-gather.2.cloned.1.call-start = ((), (), s32[]{:S(2)}) async-start(), calls=%async_computation.7 | async-start | bytes 13844480 | tf_op jit(solution)/shard_map/all_gather | solution.py:357
  19.6 47.4 %all-to-all-start.2 = ((bf16[2,40,256]{2,1,0:T(8,128)(2,1)}), bf16[2,40,256]{2,1,0:T(8,128)(2,1)S(1)}, u32[]{:S(2)}, u32[]{:S(2)}) async-start(bf16[2,40,256]{2,1,0:T(8,128)(2,1)} %get-tuple-element.21), calls=%async_computation.2 | async-start | bytes 81920 | tf_op jit(solution)/shard_map/all_to_all | solution.py:319
  67.0 71.2 %all-to-all-start.1 = ((bf16[8,128,2048]{2,1,0:T(8,128)(2,1)}), bf16[8,128,2048]{2,1,0:T(8,128)(2,1)}, u32[]{:S(2)}, u32[]{:S(2)}) async-start(bf16[8,128,2048]{2,1,0:T(8,128)(2,1)} %norm.1), calls=%async_computation.1 | async-start | bytes 8388608 | tf_op jit(solution)/shard_map/all_to_all | solution.py:319
  71.6 132.4 %copy-start = (bf16[3,256]{1,0:T(4,128)(2,1)S(1)}, bf16[3,256]{1,0:T(4,128)(2,1)}, u32[]{:S(2)}) copy-start(bf16[3,256]{1,0:T(4,128)(2,1)} %taps.1) | copy-start | bytes 4612
  110.6 27.6 %collective-permute-start.1 = (bf16[16,80,256]{2,1,0:T(8,128)(2,1)S(1)}, bf16[16,80,256]{2,1,0:T(8,128)(2,1)S(1)}, u32[]{:S(2)}, u32[]{:S(2)}) collective-permute-start(bf16[16,80,256]{2,1,0:T(8,128)(2,1)S(1)} %all_gather.7.same), channel_id=1, source_target_pairs={{0,8},{8,0},{1,9},{9,1},{2,10},{10,2},{3,11},{11,3},{4,12},{12,4},... | collective-permute-start | bytes 1966088 | tf_op jit(solution)/shard_map/ppermute | solution.py:361
  188.9 9.4 %all-to-all-start.5 = ((bf16[4,32,128]{2,1,0:T(8,128)(2,1)}), bf16[4,32,128]{2,1,0:T(8,128)(2,1)S(1)}, u32[]{:S(2)}, u32[]{:S(2)}) async-start(bf16[4,32,128]{2,1,0:T(8,128)(2,1)} %far.1), calls=%async_computation.5 | async-start | bytes 65536 | tf_op jit(solution)/shard_map/all_to_all | solution.py:319
  193.1 5.1 %collective-permute-start = (bf16[16,2048]{1,0:T(8,128)(2,1)S(1)}, bf16[16,2048]{1,0:T(8,128)(2,1)S(1)}, u32[]{:S(2)}, u32[]{:S(2)}) collective-permute-start(bf16[16,2048]{1,0:T(8,128)(2,1)S(1)} %slice_bitcast_fusion), channel_id=1, source_target_pairs={{0,8},{8,16},{16,24},{24,32},{32,40},{40,48},{48,56},{56,64},{64,7... | collective-permute-start | bytes 196616 | tf_op jit(solution)/shard_map/ppermute | solution.py:367
Sparse Core Ops, SparseCore 0:
  19.7 184.2 all-gather.1

commit v4 on v2

--- a/solution.py
+++ b/solution.py
@@ -11,7 +11,8 @@
 EPSILON = 1e-06
 ROTARY_BASE = 10000.0
 BLOCK = 256
-EXTRA = 16
+EXTRA = 8
+RIM = 16
 PROJECTED = 5 * HEAD
 COLUMNS = 7 * HEAD
 INTERPRET = False
@@ -93,7 +94,7 @@
 def norm_kernel(tokens, gain, out):
     values = tokens[...].astype(F32)
     scale = lax.rsqrt(jnp.mean(values * values, axis=-1, keepdims=True) + EPSILON)
-    normed = (values * scale * gain[...].astype(F32)).astype(BF16)
+    normed = (values * scale * gain[...].astype(F32)[None, :]).astype(BF16)
     for copy in range(out.shape[0]):
         out[copy] = normed
 
@@ -103,10 +104,10 @@
 
 
 def kv_kernel(
-    x, gathered, own, cos_far, sin_far, cos_near, sin_near, k_out, v_out, cosine, sine, decay, column, totals, message, weight
+    pair, x, same, low, high, own, cos_far, sin_far, cos_near, sin_near, k_out, v_out, cosine, sine, decay, column, totals, message, weight
 ):
     rows, width = x.shape[0] * x.shape[1], x.shape[2]
-    pairs, fars = gathered.shape[:2]
+    half = low.shape[0]
     shard = own.shape[1] - EXTRA
     lines = rows // 2 // (2 * HEAD)
 
@@ -135,18 +136,18 @@
     column[...] = jnp.concatenate([cumulative, filler], axis=0).T
     total = before
 
-    for far in range(fars):
-        for pair in range(pairs):
-            chip = far * pairs + pair
+    mine, others = pair[0], 1 - pair[0]
+    for source, first, place in ((same, 0, mine), (low, 0, others), (high, half, others)):
+        for at_far in range(source.shape[0]):
+            chip = 2 * (first + at_far) + place
             log_total = jnp.zeros((1, 1), F32)
             for core in range(2):
                 at = core * (shard + EXTRA)
-                weight[(2 * chip + core) * shard : (2 * chip + core + 1) * shard, :] = gathered[
-                    pair, far, at : at + shard, :
-                ]
-                logs = logs_of(gathered[pair, far, at + shard : at + shard + EXTRA, :], lines)
+                to = pl.multiple_of((2 * chip + core) * shard, shard)
+                weight[pl.ds(to, shard), :] = source[at_far, at : at + shard, :]
+                logs = logs_of(source[at_far, at + shard : at + shard + EXTRA, :], lines)
                 log_total = log_total + jnp.sum(logs, axis=(0, 1), keepdims=True)
-            totals[chip : chip + 1, :] = jnp.broadcast_to(log_total, (1, HEAD))
+            totals[pl.ds(chip, 1), :] = jnp.broadcast_to(log_total, (1, HEAD))
 
     state = jnp.zeros((HEAD, HEAD), F32)
     for i in range(rows // BLOCK):
@@ -213,6 +214,19 @@
         message[copy] = kept.astype(BF16)
 
 
+def store(own, i, rows, keep, send, channel, branch):
+    half = (i * BLOCK) // (rows // 2)
+    place = slice(i * BLOCK - half * (rows // 2), (i + 1) * BLOCK - half * (rows // 2))
+
+    @pl.when(own == half)
+    def _():
+        keep[place, channel : channel + HEAD] = branch
+
+    @pl.when(own != half)
+    def _():
+        send[place, channel : channel + HEAD] = branch
+
+
 def branch_kernel(
     core,
     weights,
@@ -231,7 +245,8 @@
     keep,
     send,
     out_weight,
-    weight,
+    conv_weight,
+    ret_weight,
     semaphores,
 ):
     rows = x.shape[0] * x.shape[1]
@@ -239,12 +254,15 @@
     start_at = pl.multiple_of(own * COLUMNS, HEAD)
     other_at = pl.multiple_of((1 - own) * COLUMNS, HEAD)
     copies = [
-        pltpu.make_async_copy(weights.at[:, pl.ds(start_at, PROJECTED)], weight, semaphores.at[0]),
+        pltpu.make_async_copy(weights.at[:, pl.ds(start_at, 3 * HEAD)], conv_weight, semaphores.at[0]),
         pltpu.make_async_copy(
-            weights.at[:, pl.ds(start_at + PROJECTED, 2 * HEAD)], out_weight.at[0], semaphores.at[1]
+            weights.at[:, pl.ds(start_at + 3 * HEAD, 2 * HEAD)], ret_weight, semaphores.at[1]
         ),
         pltpu.make_async_copy(
-            weights.at[:, pl.ds(other_at + PROJECTED, 2 * HEAD)], out_weight.at[1], semaphores.at[2]
+            weights.at[:, pl.ds(start_at + PROJECTED, 2 * HEAD)], out_weight.at[0], semaphores.at[2]
+        ),
+        pltpu.make_async_copy(
+            weights.at[:, pl.ds(other_at + PROJECTED, 2 * HEAD)], out_weight.at[1], semaphores.at[3]
         ),
     ]
     for copy in copies:
@@ -259,20 +277,23 @@
     start = jnp.zeros((1, 1), F32)
     per = BLOCK // HEAD
     copies[0].wait()
-    rim = dot(halo[...], weight[:, HEAD : 3 * HEAD], ((1,), (0,))).astype(BF16).astype(F32)
-    tail = (rim[:, :HEAD] * rim[:, HEAD:])[EXTRA - 8 :]
+    rim = dot(halo[...], conv_weight[:, HEAD:], ((1,), (0,))).astype(BF16).astype(F32)
+    tail = (rim[:, :HEAD] * rim[:, HEAD:])[RIM - 8 :]
     for i in range(rows // BLOCK):
-        at = pl.ds(i * BLOCK, BLOCK)
-        projected = dot(block_rows(x, i), weight[...], ((1,), (0,))).astype(BF16)
+        projected = dot(block_rows(x, i), conv_weight[...], ((1,), (0,))).astype(BF16)
         outer = projected[:, :HEAD].astype(F32)
-        mixed = projected[:, HEAD : 2 * HEAD].astype(F32) * projected[:, 2 * HEAD : 3 * HEAD].astype(F32)
+        mixed = projected[:, HEAD : 2 * HEAD].astype(F32) * projected[:, 2 * HEAD :].astype(F32)
         one = jnp.where(row == 0, tail[7:8], pltpu.roll(mixed, 1, 0))
         two = jnp.where(row == 0, tail[6:7], jnp.where(row == 1, tail[7:8], pltpu.roll(mixed, 2, 0)))
         conv = tap[0:1] * two + tap[1:2] * one + tap[2:3] * mixed
         tail = mixed[BLOCK - 8 :]
-        conv_branch = (outer * conv).astype(BF16)
-
-        query = rotated(projected[:, 3 * HEAD : 4 * HEAD].astype(F32), cosine[at, :], sine[at, :])
+        store(own, i, rows, keep, send, 0, (outer * conv).astype(BF16))
+
+    copies[1].wait()
+    for i in range(rows // BLOCK):
+        at = pl.ds(i * BLOCK, BLOCK)
+        projected = dot(block_rows(x, i), ret_weight[...], ((1,), (0,))).astype(BF16)
+        query = rotated(projected[:, :HEAD].astype(F32), cosine[at, :], sine[at, :])
         query = query.astype(BF16)
         key, value = keys[at, :], values[at, :]
         here = block_column(column, i)
@@ -287,24 +308,13 @@
         state = jnp.exp(end - start) * state + dot(faded, value, ((0,), (0,)))
         start = end
         normed = retained * lax.rsqrt(jnp.mean(retained * retained, axis=-1, keepdims=True) + EPSILON)
-        gate = projected[:, 4 * HEAD :].astype(F32)
+        gate = projected[:, HEAD:].astype(F32)
         ret_branch = (normed * (gate / (1.0 + jnp.exp(-gate)))).astype(BF16)
 
-        half = (i * BLOCK) // (rows // 2)
-        place = pl.ds(i * BLOCK - half * (rows // 2), BLOCK)
-
-        @pl.when(own == half)
-        def _():
-            keep[place, :HEAD] = conv_branch
-            keep[place, HEAD:] = ret_branch
-
-        @pl.when(own != half)
-        def _():
-            send[place, :HEAD] = conv_branch
-            send[place, HEAD:] = ret_branch
-
-    copies[1].wait()
+        store(own, i, rows, keep, send, HEAD, ret_branch)
+
     copies[2].wait()
+    copies[3].wait()
 
 
 def out_kernel(mine, theirs, weight, out):
@@ -374,15 +384,16 @@
     weights = lax.all_gather(rest, STRETCHES, axis=0, tiled=True)
 
     own = exchanged(message, "core")
-    every_second = lax.all_gather(own.reshape(2 * (shard + EXTRA), 2 * HEAD), FAR)
-    pairs = lax.axis_size("zc")
-    gathered = exchanged(jnp.broadcast_to(every_second, (pairs, *every_second.shape)), "zc")
+    same = lax.all_gather(own.reshape(2 * (shard + EXTRA), 2 * HEAD), FAR)
+    half = same.shape[0] // 2
+    low = lax.ppermute(same[:half], CHIPS, [(i, (i - 1) % chips) for i in range(chips)])
+    high = lax.ppermute(same[half:], CHIPS, [(i, (i + 1) % chips) for i in range(chips)])
 
     (normed,) = call(norm_kernel, [slow((2 * tp, own_rows, width), BF16)], "norm", specs=[PLAIN] * 2, limit=None)(
-        tokens, norm_gain.reshape(1, width)
+        tokens, norm_gain
     )
     x = exchanged(normed, ("core", "tp"))
-    halo = lax.ppermute(x[-1, own_rows - EXTRA :], CHIPS, [(i, i + 1) for i in range(chips - 1)])
+    halo = lax.ppermute(x[-1, own_rows - RIM :], CHIPS, [(i, i + 1) for i in range(chips - 1)])
 
     inv_freq = ROTARY_BASE ** (-jnp.arange(HALF, dtype=F32) / HALF)
     inv_freq = jnp.concatenate([inv_freq, inv_freq])[None, :]
@@ -402,9 +413,10 @@
             fast((near, HEAD, HEAD), BF16),
         ],
         "kv",
+        specs=[SMEM] + [VMEM] * 9,
         scratch=[pltpu.VMEM((width, 2 * HEAD), BF16)],
         flops=4 * rows * width * HEAD,
-    )(x, gathered, own, jnp.cos(far_angle), jnp.sin(far_angle), jnp.cos(near_angle), jnp.sin(near_angle))
+    )(lax.axis_index("zc").reshape(1), x, same, low, high, own, jnp.cos(far_angle), jnp.sin(far_angle), jnp.cos(near_angle), jnp.sin(near_angle))
 
     share = HEAD // near
     block = lax.axis_index("za").reshape(1)
@@ -425,7 +437,11 @@
         [fast((rows // 2, 2 * HEAD), BF16), fast((rows // 2, 2 * HEAD), BF16), fast((2, width, 2 * HEAD), BF16)],
         "branch",
         specs=[SMEM, ANY] + [VMEM] * 12,
-        scratch=[pltpu.VMEM((width, PROJECTED), BF16), pltpu.SemaphoreType.DMA((3,))],
+        scratch=[
+            pltpu.VMEM((width, 3 * HEAD), BF16),
+            pltpu.VMEM((width, 2 * HEAD), BF16),
+            pltpu.SemaphoreType.DMA((4,)),
+        ],
         flops=10 * rows * width * HEAD,
     )(
         core.reshape(1),

time: 252 us -> 234 us (0.929)
  waiting for transfers between devices: 39.3 us -> 24.8 us
  local copies, waits for them, and re-layouts: 3.59 us -> 0.89 us
    all_to_all x4 -> x3, waiting for transfers between devices: 36.7 us -> 0.01 us  [exchanged(): return lax.all_to_all(x, axes, 0, 0, tiled=True)]
    all_gather x1, waiting for transfers between devices: 0.01 us -> 13.9 us  [body(): weights = lax.all_gather(rest, STRETCHES, axis=0, tiled=True)]
    ppermute x1 -> x3, waiting for transfers between devices: 1.31 us -> 9.61 us  [the longest x1 4.8 us: body(): lax.ppermute(same[:half], CHIPS, [(i, (i - 1) % chips) for i in range(chi...]
    ppermute x1 -> x3, starting transfers between devices: 3.33 us -> 10.4 us  [the longest x1 4.12 us: body(): lax.ppermute(same[:half], CHIPS, [(i, (i - 1) % chips) for i in range(chi...]
    all_gather x1, blocking collectives: 40.1 us -> 35.1 us  [body(): same = lax.all_gather(own.reshape(2 * (shard + EXTRA), 2 * HEAD), FAR)]
    ppermute x1, starting transfers between devices: 6.48 us -> 2.23 us  [body(): theirs = lax.ppermute(send, 'core', [(0, 1), (1, 0)])]
    all_to_all x4 -> x3, starting transfers between devices: 56.4 us -> 52.8 us  [exchanged(): return lax.all_to_all(x, axes, 0, 0, tiled=True)]
    all_to_all x3, blocking collectives: 65.4 us -> 68.9 us  [exchanged(): return lax.all_to_all(x, axes, 0, 0, tiled=True)]
  transfers between devices with their start and end apart: 7 -> 8, of which waited for: 4 -> 5; matrix products, arithmetic and copies ran while one was open for 2% -> 1% of each run, Pallas kernels for 4% -> 4%
where the time goes in v4:
time: 234 us
  blocking collectives  104 us (44%)
  starting transfers between devices  65.3 us (28%)
  waiting for transfers between devices  24.8 us (11%)
  Pallas kernels  24.5 us (10%)
  between operations  13.5 us (6%)
    all_to_all x3, blocking collectives, exchanged(): return lax.all_to_all(x, axes, 0, 0, tiled=True)  68.9 us
    all_to_all x3, starting transfers between devices, exchanged(): return lax.all_to_all(x, axes, 0, 0, tiled=True)  52.8 us
    all_gather x1, blocking collectives, body(): same = lax.all_gather(own.reshape(2 * (shard + EXTRA), 2 * HEAD), FAR)  35.1 us
    pallas_call x8, Pallas kernels, run(): pl.pallas_call(kernel, out_shape=[o[0] for o in outs], in_specs=in_specs,...  24.5 us
    all_gather x1, waiting for transfers between devices, body(): weights = lax.all_gather(rest, STRETCHES, axis=0, tiled=True)  13.9 us
    ppermute x1, waiting for transfers between devices, body(): lax.ppermute(same[:half], CHIPS, [(i, (i - 1) % chips) for i in range(chi...  4.8 us
  transfers between devices with their start and end apart: 8, of which 5 were waited for; matrix products, arithmetic and copies ran while one was open for 1% of the time, Pallas kernels for 4%

profile of v4, /device:TPU:33, one launch (start us, length us, event | category | flops | bytes accessed | tf_op | source)
XLA Modules:
  0.0 233.7 jit_solution(1577649684346382850)
XLA Ops:
  6.5 0.0 all-gather.2.cloned.1.call-start
  6.6 1.5 pack.1
  8.1 0.1 all-gather.2.cloned.1.call-update
  8.2 44.7 %all-to-all-start.1 = ((bf16[2,40,256]{2,1,0:T(8,128)(2,1)}), bf16[2,40,256]{2,1,0:T(8,128)(2,1)S(1)}, u32[]{:S(2)}, u32[]{:S(2)}) async-start(bf16[2,40,256]{2,1,0:T(8,128)(2,1)} %get-tuple-element.22), calls=%async_computation.1 | async-start | bytes 81920 | tf_op jit(solution)/shard_map/all_to_all | solution.py:339
  52.9 3.5 %norm.1 = bf16[8,128,2048]{2,1,0:T(8,128)(2,1)} custom-call(bf16[128,2048]{1,0:T(8,128)(2,1)} %tokens.1, bf16[2048]{0:T(1024)(128)(2,1)} %gain.1), custom_call_target="tpu_custom_call" | custom-call | tf_op jit(solution)/shard_map/norm/pallas_call | solution.py:37
  56.4 0.0 all-to-all-done.1.own
  56.4 4.6 %all-to-all-start = ((bf16[8,128,2048]{2,1,0:T(8,128)(2,1)}), bf16[8,128,2048]{2,1,0:T(8,128)(2,1)}, u32[]{:S(2)}, u32[]{:S(2)}) async-start(bf16[8,128,2048]{2,1,0:T(8,128)(2,1)} %norm.1), calls=%async_computation | async-start | bytes 8388608 | tf_op jit(solution)/shard_map/all_to_all | solution.py:339
  61.0 35.1 %all_gather.7.same = bf16[16,80,256]{2,1,0:T(8,128)(2,1)S(1)} all-gather(bf16[1,80,256]{2,1,0:T(8,128)(2,1)S(1)} %bitcast.10), channel_id=1, replica_groups=mesh['grp'=2,'za'=8,'zb'=2,'zc'=2,'core'=2,'tp'=4] {'za','zb'}, dimensions={0}, use_global_device_ids=true | all-gather | bytes 696320 | tf_op jit(solution)/shard_map/all_gather | solution.py:387
  96.1 0.0 copy-start
  96.1 4.1 %collective-permute-start.1 = (bf16[8,80,256]{2,1,0:T(8,128)(2,1)S(1)}, bf16[8,80,256]{2,1,0:T(8,128)(2,1)S(1)}, u32[]{:S(2)}, u32[]{:S(2)}) collective-permute-start(bf16[8,80,256]{2,1,0:T(8,128)(2,1)S(1)} %get-tuple-element.38), channel_id=1, source_target_pairs={{0,248},{8,0},{16,8},{24,16},{32,24},{40,32},{48,40},{56,48},{64,5... | collective-permute-start | bytes 983048 | tf_op jit(solution)/shard_map/ppermute | solution.py:389
  100.3 2.6 %collective-permute-start.2 = (bf16[8,80,256]{2,1,0:T(8,128)(2,1)S(1)}, bf16[8,80,256]{2,1,0:T(8,128)(2,1)S(1)}, u32[]{:S(2)}, u32[]{:S(2)}) collective-permute-start(bf16[8,80,256]{2,1,0:T(8,128)(2,1)S(1)} %get-tuple-element.37), channel_id=1, source_target_pairs={{0,8},{8,16},{16,24},{24,32},{32,40},{40,48},{48,56},{56,64},{64,7... | collective-permute-start | bytes 983048 | tf_op jit(solution)/shard_map/ppermute | solution.py:390
  102.9 0.1 pad_maximum_fusion
  103.0 0.1 multiply_sine_fusion
  103.1 0.5 fusion
  103.6 4.8 %collective-permute-done.1.low = bf16[8,80,256]{2,1,0:T(8,128)(2,1)S(1)} collective-permute-done((bf16[8,80,256]{2,1,0:T(8,128)(2,1)S(1)}, bf16[8,80,256]{2,1,0:T(8,128)(2,1)S(1)}, u32[]{:S(2)}, u32[]{:S(2)}) %collective-permute-start.1) | collective-permute-done | bytes 327712 | tf_op jit(solution)/shard_map/ppermute | solution.py:389
  108.4 3.5 %collective-permute-done.2.high = bf16[8,80,256]{2,1,0:T(8,128)(2,1)S(1)} collective-permute-done((bf16[8,80,256]{2,1,0:T(8,128)(2,1)S(1)}, bf16[8,80,256]{2,1,0:T(8,128)(2,1)S(1)}, u32[]{:S(2)}, u32[]{:S(2)}) %collective-permute-start.2) | collective-permute-done | bytes 327712 | tf_op jit(solution)/shard_map/ppermute | solution.py:390
  111.9 0.0 all-to-all-done.x
  111.9 5.0 %kv.1 = (bf16[1024,128]{1,0:T(8,128)(2,1)S(1)}, bf16[1024,128]{1,0:T(8,128)(2,1)S(1)}, f32[1024,128]{1,0:T(8,128)S(1)}, f32[1024,128]{1,0:T(8,128)S(1)}, f32[8,1...) custom-call(s32[1]{0:T(128)} %bitcast.5.pair, ...), custom_call_target="tpu_custom_call" | custom-call | flops 1073741824 | tf_op jit(solution)/shard_map/kv/pallas_call | solution.py:37
  116.9 7.9 %all_to_all.30.gathered = bf16[4,128,128]{2,1,0:T(8,128)(2,1)S(1)} all-to-all(bf16[4,128,128]{2,1,0:T(8,128)(2,1)S(1)} %get-tuple-element.30), channel_id=1, replica_groups=mesh['grp'=2,'za'=8,'zb'=2,'zc'=2,'core'=2,'tp'=4] {'zb','zc'}, dimensions={0} | all-to-all | bytes 262144 | tf_op jit(solution)/shard_map/all_to_all | solution.py:339
  124.8 0.1 near.1
  124.8 32.1 %all_to_all.31.gathered = bf16[8,32,128]{2,1,0:T(8,128)(2,1)S(1)} all-to-all(bf16[8,32,128]{2,1,0:T(8,128)(2,1)S(1)} %get-tuple-element.31), channel_id=1, replica_groups=mesh['grp'=2,'za'=8,'zb'=2,'zc'=2,'core'=2,'tp'=4] {'za'}, dimensions={0} | all-to-all | bytes 131072 | tf_op jit(solution)/shard_map/all_to_all | solution.py:339
  156.9 0.6 far.1
  157.5 3.4 %all-to-all-start.4 = ((bf16[4,32,128]{2,1,0:T(8,128)(2,1)}), bf16[4,32,128]{2,1,0:T(8,128)(2,1)S(1)}, u32[]{:S(2)}, u32[]{:S(2)}) async-start(bf16[4,32,128]{2,1,0:T(8,128)(2,1)} %far.1), calls=%async_computation.4 | async-start | bytes 65536 | tf_op jit(solution)/shard_map/all_to_all | solution.py:339
  161.0 0.8 slice_bitcast_fusion
  161.8 3.7 %collective-permute-start = (bf16[16,2048]{1,0:T(8,128)(2,1)S(1)}, bf16[16,2048]{1,0:T(8,128)(2,1)S(1)}, u32[]{:S(2)}, u32[]{:S(2)}) collective-permute-start(bf16[16,2048]{1,0:T(8,128)(2,1)S(1)} %slice_bitcast_fusion), channel_id=1, source_target_pairs={{0,8},{8,16},{16,24},{24,32},{32,40},{40,48},{48,56},{56,64},{64,7... | collective-permute-start | bytes 196616 | tf_op jit(solution)/shard_map/ppermute | solution.py:396
  165.5 1.3 collective-permute-done.halo
  166.8 0.0 all-to-all-done.4.base
  166.8 13.9 %all-gather.2.cloned.1.call-done.weights = bf16[2048,1792]{1,0:T(8,128)(2,1)} async-done(((bf16[32,1792]{1,0:T(8,128)(2,1)}), bf16[2048,1792]{1,0:T(8,128)(2,1)}) %all-gather.2.cloned.1.call-update) | async-done | bytes 7340048 | tf_op jit(solution)/shard_map/all_gather | solution.py:384
  180.7 0.0 copy-done
  180.7 11.4 %branch.1 = (bf16[512,256]{1,0:T(8,128)(2,1)S(1)}, bf16[512,256]{1,0:T(8,128)(2,1)S(1)}, bf16[2,2048,256]{2,1,0:T(8,128)(2,1)S(1)}) custom-call(s32[1]{0:T(128)} %bitcast.core, bf16[2048,1792]{1,0:T(8,128)(2,1)} %all-gather.2.cloned.1.call-done.weights, bf16[8,128,2048]{2,1,0:T(8,128)(2,1)} %all-to-all-done.x, ...), custom_call_target="tpu_custom_call" | custom-call | flops 2684354560 | tf_op jit(solution)/shard_map/branch/pallas_call | solution.py:37
  192.1 2.2 collective-permute-start.3
  194.4 1.2 collective-permute-done.3.theirs
  195.6 1.3 out.1
  196.9 28.9 %all_to_all.32.parts = bf16[4,128,2048]{2,1,0:T(8,128)(2,1)S(1)} all-to-all(bf16[4,128,2048]{2,1,0:T(8,128)(2,1)S(1)} %out.1), channel_id=1, replica_groups=mesh['grp'=2,'za'=8,'zb'=2,'zc'=2,'core'=2,'tp'=4] {'tp'}, dimensions={0} | all-to-all | bytes 4194304 | tf_op jit(solution)/shard_map/all_to_all | solution.py:339
  225.8 1.0 sum.1
  (3 shorter events, 0.1 us)
Async XLA Ops:
  6.5 174.2 %all-gather.2.cloned.1.call-start = ((), (), s32[]{:S(2)}) async-start(), calls=%async_computation.6 | async-start | bytes 7454720 | tf_op jit(solution)/shard_map/all_gather | solution.py:384
  8.2 48.3 %all-to-all-start.1 = ((bf16[2,40,256]{2,1,0:T(8,128)(2,1)}), bf16[2,40,256]{2,1,0:T(8,128)(2,1)S(1)}, u32[]{:S(2)}, u32[]{:S(2)}) async-start(bf16[2,40,256]{2,1,0:T(8,128)(2,1)} %get-tuple-element.22), calls=%async_computation.1 | async-start | bytes 81920 | tf_op jit(solution)/shard_map/all_to_all | solution.py:339
  56.4 55.5 %all-to-all-start = ((bf16[8,128,2048]{2,1,0:T(8,128)(2,1)}), bf16[8,128,2048]{2,1,0:T(8,128)(2,1)}, u32[]{:S(2)}, u32[]{:S(2)}) async-start(bf16[8,128,2048]{2,1,0:T(8,128)(2,1)} %norm.1), calls=%async_computation | async-start | bytes 8388608 | tf_op jit(solution)/shard_map/all_to_all | solution.py:339
  96.1 84.6 %copy-start = (bf16[3,256]{1,0:T(4,128)(2,1)S(1)}, bf16[3,256]{1,0:T(4,128)(2,1)}, u32[]{:S(2)}) copy-start(bf16[3,256]{1,0:T(4,128)(2,1)} %taps.1) | copy-start | bytes 4612
  96.1 12.2 %collective-permute-start.1 = (bf16[8,80,256]{2,1,0:T(8,128)(2,1)S(1)}, bf16[8,80,256]{2,1,0:T(8,128)(2,1)S(1)}, u32[]{:S(2)}, u32[]{:S(2)}) collective-permute-start(bf16[8,80,256]{2,1,0:T(8,128)(2,1)S(1)} %get-tuple-element.38), channel_id=1, source_target_pairs={{0,248},{8,0},{16,8},{24,16},{32,24},{40,32},{48,40},{56,48},{64,5... | collective-permute-start | bytes 983048 | tf_op jit(solution)/shard_map/ppermute | solution.py:389
  100.3 11.6 %collective-permute-start.2 = (bf16[8,80,256]{2,1,0:T(8,128)(2,1)S(1)}, bf16[8,80,256]{2,1,0:T(8,128)(2,1)S(1)}, u32[]{:S(2)}, u32[]{:S(2)}) collective-permute-start(bf16[8,80,256]{2,1,0:T(8,128)(2,1)S(1)} %get-tuple-element.37), channel_id=1, source_target_pairs={{0,8},{8,16},{16,24},{24,32},{32,40},{40,48},{48,56},{56,64},{64,7... | collective-permute-start | bytes 983048 | tf_op jit(solution)/shard_map/ppermute | solution.py:390
  157.5 9.3 %all-to-all-start.4 = ((bf16[4,32,128]{2,1,0:T(8,128)(2,1)}), bf16[4,32,128]{2,1,0:T(8,128)(2,1)S(1)}, u32[]{:S(2)}, u32[]{:S(2)}) async-start(bf16[4,32,128]{2,1,0:T(8,128)(2,1)} %far.1), calls=%async_computation.4 | async-start | bytes 65536 | tf_op jit(solution)/shard_map/all_to_all | solution.py:339
  161.8 5.0 %collective-permute-start = (bf16[16,2048]{1,0:T(8,128)(2,1)S(1)}, bf16[16,2048]{1,0:T(8,128)(2,1)S(1)}, u32[]{:S(2)}, u32[]{:S(2)}) collective-permute-start(bf16[16,2048]{1,0:T(8,128)(2,1)S(1)} %slice_bitcast_fusion), channel_id=1, source_target_pairs={{0,8},{8,16},{16,24},{24,32},{32,40},{40,48},{48,56},{56,64},{64,7... | collective-permute-start | bytes 196616 | tf_op jit(solution)/shard_map/ppermute | solution.py:396
  192.1 3.5 %collective-permute-start.3 = (bf16[512,256]{1,0:T(8,128)(2,1)S(1)}, bf16[512,256]{1,0:T(8,128)(2,1)S(1)}, u32[]{:S(2)}, u32[]{:S(2)}) collective-permute-start(bf16[512,256]{1,0:T(8,128)(2,1)S(1)} %get-tuple-element.35), channel_id=1, source_target_pairs={{0,4},{4,0},{1,5},{5,1},{2,6},{6,2},{3,7},{7,3},{8,12},{12,8},{9,1... | collective-permute-start | bytes 786440 | tf_op jit(solution)/shard_map/ppermute | solution.py:462
Sparse Core Ops, SparseCore 0:
  9.5 171.1 all-gather.1

commit v5 on v4

--- a/solution.py
+++ b/solution.py
@@ -14,6 +14,7 @@
 EXTRA = 8
 RIM = 16
 PROJECTED = 5 * HEAD
+PIECES = 4
 COLUMNS = 7 * HEAD
 INTERPRET = False
 
@@ -214,19 +215,6 @@
         message[copy] = kept.astype(BF16)
 
 
-def store(own, i, rows, keep, send, channel, branch):
-    half = (i * BLOCK) // (rows // 2)
-    place = slice(i * BLOCK - half * (rows // 2), (i + 1) * BLOCK - half * (rows // 2))
-
-    @pl.when(own == half)
-    def _():
-        keep[place, channel : channel + HEAD] = branch
-
-    @pl.when(own != half)
-    def _():
-        send[place, channel : channel + HEAD] = branch
-
-
 def branch_kernel(
     core,
     weights,
@@ -242,27 +230,30 @@
     before,
     fade,
     taps,
-    keep,
-    send,
+    branches,
     out_weight,
-    conv_weight,
-    ret_weight,
+    weight,
     semaphores,
 ):
     rows = x.shape[0] * x.shape[1]
     own = core[0]
     start_at = pl.multiple_of(own * COLUMNS, HEAD)
     other_at = pl.multiple_of((1 - own) * COLUMNS, HEAD)
+    piece = weight.shape[0] // PIECES
     copies = [
-        pltpu.make_async_copy(weights.at[:, pl.ds(start_at, 3 * HEAD)], conv_weight, semaphores.at[0]),
-        pltpu.make_async_copy(
-            weights.at[:, pl.ds(start_at + 3 * HEAD, 2 * HEAD)], ret_weight, semaphores.at[1]
+        *(
+            pltpu.make_async_copy(
+                weights.at[pl.ds(at, piece), pl.ds(start_at, PROJECTED)],
+                weight.at[pl.ds(at, piece), :],
+                semaphores.at[2 + at // piece],
+            )
+            for at in range(0, weight.shape[0], piece)
         ),
         pltpu.make_async_copy(
-            weights.at[:, pl.ds(start_at + PROJECTED, 2 * HEAD)], out_weight.at[0], semaphores.at[2]
+            weights.at[:, pl.ds(start_at + PROJECTED, 2 * HEAD)], out_weight.at[0], semaphores.at[0]
         ),
         pltpu.make_async_copy(
-            weights.at[:, pl.ds(other_at + PROJECTED, 2 * HEAD)], out_weight.at[1], semaphores.at[3]
+            weights.at[:, pl.ds(other_at + PROJECTED, 2 * HEAD)], out_weight.at[1], semaphores.at[1]
         ),
     ]
     for copy in copies:
@@ -276,24 +267,28 @@
     tap = jnp.where(own == 0, taps[:, :HEAD].astype(F32), taps[:, HEAD:].astype(F32))
     start = jnp.zeros((1, 1), F32)
     per = BLOCK // HEAD
-    copies[0].wait()
-    rim = dot(halo[...], conv_weight[:, HEAD:], ((1,), (0,))).astype(BF16).astype(F32)
+    first = jnp.zeros((BLOCK, PROJECTED), F32)
+    for at in range(PIECES):
+        copies[at].wait()
+        cut = slice(at * piece, (at + 1) * piece)
+        first = first + dot(block_rows(x, 0)[:, cut], weight[cut, :], ((1,), (0,)))
+    rim = dot(halo[...], weight[:, HEAD : 3 * HEAD], ((1,), (0,))).astype(BF16).astype(F32)
     tail = (rim[:, :HEAD] * rim[:, HEAD:])[RIM - 8 :]
     for i in range(rows // BLOCK):
-        projected = dot(block_rows(x, i), conv_weight[...], ((1,), (0,))).astype(BF16)
+        at = pl.ds(i * BLOCK, BLOCK)
+        half = (i * BLOCK) // (rows // 2)
+        place = slice(i * BLOCK - half * (rows // 2), (i + 1) * BLOCK - half * (rows // 2))
+        slot = jnp.where(own == half, 0, 1)
+        projected = (dot(block_rows(x, i), weight[...], ((1,), (0,))) if i else first).astype(BF16)
         outer = projected[:, :HEAD].astype(F32)
-        mixed = projected[:, HEAD : 2 * HEAD].astype(F32) * projected[:, 2 * HEAD :].astype(F32)
+        mixed = projected[:, HEAD : 2 * HEAD].astype(F32) * projected[:, 2 * HEAD : 3 * HEAD].astype(F32)
         one = jnp.where(row == 0, tail[7:8], pltpu.roll(mixed, 1, 0))
         two = jnp.where(row == 0, tail[6:7], jnp.where(row == 1, tail[7:8], pltpu.roll(mixed, 2, 0)))
         conv = tap[0:1] * two + tap[1:2] * one + tap[2:3] * mixed
         tail = mixed[BLOCK - 8 :]
-        store(own, i, rows, keep, send, 0, (outer * conv).astype(BF16))
-
-    copies[1].wait()
-    for i in range(rows // BLOCK):
-        at = pl.ds(i * BLOCK, BLOCK)
-        projected = dot(block_rows(x, i), ret_weight[...], ((1,), (0,))).astype(BF16)
-        query = rotated(projected[:, :HEAD].astype(F32), cosine[at, :], sine[at, :])
+        branches[slot, place, :HEAD] = (outer * conv).astype(BF16)
+
+        query = rotated(projected[:, 3 * HEAD : 4 * HEAD].astype(F32), cosine[at, :], sine[at, :])
         query = query.astype(BF16)
         key, value = keys[at, :], values[at, :]
         here = block_column(column, i)
@@ -308,13 +303,13 @@
         state = jnp.exp(end - start) * state + dot(faded, value, ((0,), (0,)))
         start = end
         normed = retained * lax.rsqrt(jnp.mean(retained * retained, axis=-1, keepdims=True) + EPSILON)
-        gate = projected[:, HEAD:].astype(F32)
+        gate = projected[:, 4 * HEAD :].astype(F32)
         ret_branch = (normed * (gate / (1.0 + jnp.exp(-gate)))).astype(BF16)
 
-        store(own, i, rows, keep, send, HEAD, ret_branch)
-
-    copies[2].wait()
-    copies[3].wait()
+        branches[slot, place, HEAD:] = ret_branch
+
+    copies[PIECES].wait()
+    copies[PIECES + 1].wait()
 
 
 def out_kernel(mine, theirs, weight, out):
@@ -322,17 +317,10 @@
     step = 512
     for column in range(0, out.shape[2], step):
         at = pl.ds(column, step)
-        total = dot(mine[...], weight[0, at, :], ((1,), (1,))) + dot(theirs[...], weight[1, at, :], ((1,), (1,)))
+        total = dot(mine[0], weight[0, at, :], ((1,), (1,))) + dot(theirs[1], weight[1, at, :], ((1,), (1,)))
         total = total.astype(BF16)
         for part in range(parts):
             out[part, :, column : column + step] = total[part * rows : (part + 1) * rows]
-
-
-def sum_kernel(parts, out):
-    total = parts[0].astype(F32)
-    for at in range(1, parts.shape[0]):
-        total = total + parts[at].astype(F32)
-    out[...] = total.astype(BF16)
 
 
 def exchanged(x, axes):
@@ -432,16 +420,12 @@
     )
     base = exchanged(message, NEAR)
 
-    keep, send, out_weight = call(
+    branches, out_weight = call(
         branch_kernel,
-        [fast((rows // 2, 2 * HEAD), BF16), fast((rows // 2, 2 * HEAD), BF16), fast((2, width, 2 * HEAD), BF16)],
+        [fast((2, rows // 2, 2 * HEAD), BF16), fast((2, width, 2 * HEAD), BF16)],
         "branch",
         specs=[SMEM, ANY] + [VMEM] * 12,
-        scratch=[
-            pltpu.VMEM((width, 3 * HEAD), BF16),
-            pltpu.VMEM((width, 2 * HEAD), BF16),
-            pltpu.SemaphoreType.DMA((4,)),
-        ],
+        scratch=[pltpu.VMEM((width, PROJECTED), BF16), pltpu.SemaphoreType.DMA((PIECES + 2,))],
         flops=10 * rows * width * HEAD,
     )(
         core.reshape(1),
@@ -459,12 +443,11 @@
         fade,
         conv_taps,
     )
-    theirs = lax.ppermute(send, "core", [(0, 1), (1, 0)])
-    (partial,) = call(out_kernel, [fast((tp, own_rows, width), BF16)], "out", flops=rows * width * 4 * HEAD)(
-        keep, theirs, out_weight
-    )
-    (mixed,) = call(sum_kernel, [slow((own_rows, width), BF16)], "sum")(exchanged(partial, "tp"))
-    return mixed
+    theirs = lax.ppermute(branches, "core", [(0, 1), (1, 0)])
+    (partial,) = call(out_kernel, [slow((tp, own_rows, width), BF16)], "out", flops=rows * width * 4 * HEAD)(
+        branches, theirs, out_weight
+    )
+    return lax.psum_scatter(partial.reshape(tp * own_rows, width), "tp", scatter_dimension=0, tiled=True)
 
 
 def solution(mesh):

time: 234 us -> 240 us (1.026)
  waiting for transfers between devices: 24.8 us -> 57.6 us
  blocking collectives: 104 us -> 79.2 us
  Pallas kernels: 24.5 us -> 21.9 us
    reduce_scatter x0 -> x1, waiting for transfers between devices: none -> 36.7 us  [body(): lax.psum_scatter(partial.reshape(tp * own_rows, width), 'tp', scatter_dim...]
    all_to_all x3 -> x2, blocking collectives: 68.9 us -> 44.4 us  [exchanged(): return lax.all_to_all(x, axes, 0, 0, tiled=True)]
    all_gather x1, waiting for transfers between devices: 13.9 us -> 10.4 us  [body(): weights = lax.all_gather(rest, STRETCHES, axis=0, tiled=True)]
    pallas_call x8 -> x7, Pallas kernels: 24.5 us -> 21.9 us  [run(): pl.pallas_call(kernel, out_shape=[o[0] for o in outs], in_specs=in_specs,...]
  transfers between devices with their start and end apart: 8 -> 9, of which waited for: 5 -> 6; matrix products, arithmetic and copies ran while one was open for 1% -> 1% of each run, Pallas kernels for 4% -> 4%
where the time goes in v5:
time: 240 us
  blocking collectives  79.2 us (33%)
  starting transfers between devices  65.8 us (27%)
  waiting for transfers between devices  57.6 us (24%)
  Pallas kernels  21.9 us (9%)
  between operations  13.5 us (6%)
    all_to_all x3, starting transfers between devices, exchanged(): return lax.all_to_all(x, axes, 0, 0, tiled=True)  52.7 us
    all_to_all x2, blocking collectives, exchanged(): return lax.all_to_all(x, axes, 0, 0, tiled=True)  44.4 us
    reduce_scatter x1, waiting for transfers between devices, body(): lax.psum_scatter(partial.reshape(tp * own_rows, width), 'tp', scatter_dim...  36.7 us
    all_gather x1, blocking collectives, body(): same = lax.all_gather(own.reshape(2 * (shard + EXTRA), 2 * HEAD), FAR)  34.8 us
    pallas_call x7, Pallas kernels, run(): pl.pallas_call(kernel, out_shape=[o[0] for o in outs], in_specs=in_specs,...  21.9 us
    all_gather x1, waiting for transfers between devices, body(): weights = lax.all_gather(rest, STRETCHES, axis=0, tiled=True)  10.4 us
  transfers between devices with their start and end apart: 9, of which 6 were waited for; matrix products, arithmetic and copies ran while one was open for 1% of the time, Pallas kernels for 4%

profile of v5, /device:TPU:33, one launch (start us, length us, event | category | flops | bytes accessed | tf_op | source)
XLA Modules:
  0.0 239.6 jit_solution(828282163452861797)
XLA Ops:
  6.5 0.0 all-gather.2.cloned.1.call-start
  6.6 1.5 pack.1
  8.1 0.1 all-gather.2.cloned.1.call-update
  8.2 44.7 %all-to-all-start.1 = ((bf16[2,40,256]{2,1,0:T(8,128)(2,1)}), bf16[2,40,256]{2,1,0:T(8,128)(2,1)S(1)}, u32[]{:S(2)}, u32[]{:S(2)}) async-start(bf16[2,40,256]{2,1,0:T(8,128)(2,1)} %get-tuple-element.21), calls=%async_computation.1 | async-start | bytes 81920 | tf_op jit(solution)/shard_map/all_to_all | solution.py:327
  52.9 3.5 %norm.1 = bf16[8,128,2048]{2,1,0:T(8,128)(2,1)} custom-call(bf16[128,2048]{1,0:T(8,128)(2,1)} %tokens.1, bf16[2048]{0:T(1024)(128)(2,1)} %gain.1), custom_call_target="tpu_custom_call" | custom-call | tf_op jit(solution)/shard_map/norm/pallas_call | solution.py:38
  56.4 0.0 all-to-all-done.1.own
  56.4 4.6 %all-to-all-start = ((bf16[8,128,2048]{2,1,0:T(8,128)(2,1)}), bf16[8,128,2048]{2,1,0:T(8,128)(2,1)}, u32[]{:S(2)}, u32[]{:S(2)}) async-start(bf16[8,128,2048]{2,1,0:T(8,128)(2,1)} %norm.1), calls=%async_computation | async-start | bytes 8388608 | tf_op jit(solution)/shard_map/all_to_all | solution.py:327
  61.0 34.8 %all_gather.7.same = bf16[16,80,256]{2,1,0:T(8,128)(2,1)S(1)} all-gather(bf16[1,80,256]{2,1,0:T(8,128)(2,1)S(1)} %bitcast.11), channel_id=1, replica_groups=mesh['grp'=2,'za'=8,'zb'=2,'zc'=2,'core'=2,'tp'=4] {'za','zb'}, dimensions={0}, use_global_device_ids=true | all-gather | bytes 696320 | tf_op jit(solution)/shard_map/all_gather | solution.py:375
  95.8 0.0 copy-start
  95.9 4.1 %collective-permute-start.1 = (bf16[8,80,256]{2,1,0:T(8,128)(2,1)S(1)}, bf16[8,80,256]{2,1,0:T(8,128)(2,1)S(1)}, u32[]{:S(2)}, u32[]{:S(2)}) collective-permute-start(bf16[8,80,256]{2,1,0:T(8,128)(2,1)S(1)} %get-tuple-element.36), channel_id=1, source_target_pairs={{0,248},{8,0},{16,8},{24,16},{32,24},{40,32},{48,40},{56,48},{64,5... | collective-permute-start | bytes 983048 | tf_op jit(solution)/shard_map/ppermute | solution.py:377
  100.0 3.0 %collective-permute-start.2 = (bf16[8,80,256]{2,1,0:T(8,128)(2,1)S(1)}, bf16[8,80,256]{2,1,0:T(8,128)(2,1)S(1)}, u32[]{:S(2)}, u32[]{:S(2)}) collective-permute-start(bf16[8,80,256]{2,1,0:T(8,128)(2,1)S(1)} %get-tuple-element.35), channel_id=1, source_target_pairs={{0,8},{8,16},{16,24},{24,32},{32,40},{40,48},{48,56},{56,64},{64,7... | collective-permute-start | bytes 983048 | tf_op jit(solution)/shard_map/ppermute | solution.py:378
  103.1 0.1 pad_maximum_fusion
  103.1 0.1 multiply_sine_fusion
  103.3 0.5 fusion
  103.8 4.4 %collective-permute-done.1.low = bf16[8,80,256]{2,1,0:T(8,128)(2,1)S(1)} collective-permute-done((bf16[8,80,256]{2,1,0:T(8,128)(2,1)S(1)}, bf16[8,80,256]{2,1,0:T(8,128)(2,1)S(1)}, u32[]{:S(2)}, u32[]{:S(2)}) %collective-permute-start.1) | collective-permute-done | bytes 327712 | tf_op jit(solution)/shard_map/ppermute | solution.py:377
  108.1 3.1 %collective-permute-done.2.high = bf16[8,80,256]{2,1,0:T(8,128)(2,1)S(1)} collective-permute-done((bf16[8,80,256]{2,1,0:T(8,128)(2,1)S(1)}, bf16[8,80,256]{2,1,0:T(8,128)(2,1)S(1)}, u32[]{:S(2)}, u32[]{:S(2)}) %collective-permute-start.2) | collective-permute-done | bytes 327712 | tf_op jit(solution)/shard_map/ppermute | solution.py:378
  111.2 0.0 all-to-all-done.x
  111.2 5.0 %kv.1 = (bf16[1024,128]{1,0:T(8,128)(2,1)S(1)}, bf16[1024,128]{1,0:T(8,128)(2,1)S(1)}, f32[1024,128]{1,0:T(8,128)S(1)}, f32[1024,128]{1,0:T(8,128)S(1)}, f32[8,1...) custom-call(s32[1]{0:T(128)} %bitcast.5.pair, ...), custom_call_target="tpu_custom_call" | custom-call | flops 1073741824 | tf_op jit(solution)/shard_map/kv/pallas_call | solution.py:38
  116.2 9.3 %all_to_all.25.gathered = bf16[4,128,128]{2,1,0:T(8,128)(2,1)S(1)} all-to-all(bf16[4,128,128]{2,1,0:T(8,128)(2,1)S(1)} %get-tuple-element.29), channel_id=1, replica_groups=mesh['grp'=2,'za'=8,'zb'=2,'zc'=2,'core'=2,'tp'=4] {'zb','zc'}, dimensions={0} | all-to-all | bytes 262144 | tf_op jit(solution)/shard_map/all_to_all | solution.py:327
  125.5 35.2 %all_to_all.26.gathered = bf16[8,32,128]{2,1,0:T(8,128)(2,1)S(1)} all-to-all(bf16[8,32,128]{2,1,0:T(8,128)(2,1)S(1)} %get-tuple-element.30), channel_id=1, replica_groups=mesh['grp'=2,'za'=8,'zb'=2,'zc'=2,'core'=2,'tp'=4] {'za'}, dimensions={0} | all-to-all | bytes 131072 | tf_op jit(solution)/shard_map/all_to_all | solution.py:327
  160.7 0.6 far.1
  161.3 3.4 %all-to-all-start.4 = ((bf16[4,32,128]{2,1,0:T(8,128)(2,1)}), bf16[4,32,128]{2,1,0:T(8,128)(2,1)S(1)}, u32[]{:S(2)}, u32[]{:S(2)}) async-start(bf16[4,32,128]{2,1,0:T(8,128)(2,1)} %far.1), calls=%async_computation.4 | async-start | bytes 65536 | tf_op jit(solution)/shard_map/all_to_all | solution.py:327
  164.7 0.1 reduce-scatter.2.cloned.1.call-start
  164.7 0.8 slice_bitcast_fusion
  165.6 3.7 %collective-permute-start = (bf16[16,2048]{1,0:T(8,128)(2,1)S(1)}, bf16[16,2048]{1,0:T(8,128)(2,1)S(1)}, u32[]{:S(2)}, u32[]{:S(2)}) collective-permute-start(bf16[16,2048]{1,0:T(8,128)(2,1)S(1)} %slice_bitcast_fusion), channel_id=1, source_target_pairs={{0,8},{8,16},{16,24},{24,32},{32,40},{40,48},{48,56},{56,64},{64,7... | collective-permute-start | bytes 196616 | tf_op jit(solution)/shard_map/ppermute | solution.py:384
  169.3 1.3 collective-permute-done.halo
  170.6 0.0 all-to-all-done.4.base
  170.6 10.4 %all-gather.2.cloned.1.call-done.weights = bf16[2048,1792]{1,0:T(8,128)(2,1)} async-done(((bf16[32,1792]{1,0:T(8,128)(2,1)}), bf16[2048,1792]{1,0:T(8,128)(2,1)}) %all-gather.2.cloned.1.call-update) | async-done | bytes 7340048 | tf_op jit(solution)/shard_map/all_gather | solution.py:372
  181.0 0.0 copy-done
  181.0 8.5 %branch.1 = (bf16[2,512,256]{2,1,0:T(8,128)(2,1)S(1)}, bf16[2,2048,256]{2,1,0:T(8,128)(2,1)S(1)}) custom-call(s32[1]{0:T(128)} %bitcast.core, bf16[2048,1792]{1,0:T(8,128)(2,1)} %all-gather.2.cloned.1.call-done.weights, bf16[8,128,2048]{2,1,0:T(8,128)(2,1)} %all-to-all-done.x, bf16[16,2048]{1,0:T(8,128)(2,1)S(1)} %collective-permute-done.halo, ...), custom_call_target="tpu_custom_call" | custom-call | flops 2684354560 | tf_op jit(solution)/shard_map/branch/pallas_call | solution.py:38
  189.5 2.2 collective-permute-start.3
  191.8 1.6 collective-permute-done.3.theirs
  193.4 2.6 %out.1 = bf16[4,128,2048]{2,1,0:T(8,128)(2,1)} custom-call(bf16[2,512,256]{2,1,0:T(8,128)(2,1)S(1)} %get-tuple-element.33.mine, bf16[2,512,256]{2,1,0:T(8,128)(2,1)S(1)} %collective-permute-done.3.theirs, bf16[2,2048,256]{2,1,0:T(8,128)(2,1)S(1)} %get-tuple-element.34.weight), custom_call_target="tpu_custom_call" | custom-call | flops 1073741824 | tf_op jit(solution)/shard_map/out/pallas_call | solution.py:38
  196.0 0.1 reduce-scatter.2.cloned.1.call-update
  196.1 36.7 %reduce-scatter.2.cloned.1.call-done = bf16[128,2048]{1,0:T(8,128)(2,1)} async-done(((bf16[512,2048]{1,0:T(8,128)(2,1)}), bf16[128,2048]{1,0:T(8,128)(2,1)}) %reduce-scatter.2.cloned.1.call-update) | async-done | bytes 524304 | tf_op jit(solution)/shard_map/reduce_scatter | solution.py:450
  (4 shorter events, 0.1 us)
Async XLA Ops:
  6.5 174.5 %all-gather.2.cloned.1.call-start = ((), (), s32[]{:S(2)}) async-start(), calls=%async_computation.6 | async-start | bytes 7454720 | tf_op jit(solution)/shard_map/all_gather | solution.py:372
  8.2 48.2 %all-to-all-start.1 = ((bf16[2,40,256]{2,1,0:T(8,128)(2,1)}), bf16[2,40,256]{2,1,0:T(8,128)(2,1)S(1)}, u32[]{:S(2)}, u32[]{:S(2)}) async-start(bf16[2,40,256]{2,1,0:T(8,128)(2,1)} %get-tuple-element.21), calls=%async_computation.1 | async-start | bytes 81920 | tf_op jit(solution)/shard_map/all_to_all | solution.py:327
  56.4 54.8 %all-to-all-start = ((bf16[8,128,2048]{2,1,0:T(8,128)(2,1)}), bf16[8,128,2048]{2,1,0:T(8,128)(2,1)}, u32[]{:S(2)}, u32[]{:S(2)}) async-start(bf16[8,128,2048]{2,1,0:T(8,128)(2,1)} %norm.1), calls=%async_computation | async-start | bytes 8388608 | tf_op jit(solution)/shard_map/all_to_all | solution.py:327
  95.8 85.2 %copy-start = (bf16[3,256]{1,0:T(4,128)(2,1)S(1)}, bf16[3,256]{1,0:T(4,128)(2,1)}, u32[]{:S(2)}) copy-start(bf16[3,256]{1,0:T(4,128)(2,1)} %taps.1) | copy-start | bytes 4612
  95.9 12.3 %collective-permute-start.1 = (bf16[8,80,256]{2,1,0:T(8,128)(2,1)S(1)}, bf16[8,80,256]{2,1,0:T(8,128)(2,1)S(1)}, u32[]{:S(2)}, u32[]{:S(2)}) collective-permute-start(bf16[8,80,256]{2,1,0:T(8,128)(2,1)S(1)} %get-tuple-element.36), channel_id=1, source_target_pairs={{0,248},{8,0},{16,8},{24,16},{32,24},{40,32},{48,40},{56,48},{64,5... | collective-permute-start | bytes 983048 | tf_op jit(solution)/shard_map/ppermute | solution.py:377
  100.0 11.2 %collective-permute-start.2 = (bf16[8,80,256]{2,1,0:T(8,128)(2,1)S(1)}, bf16[8,80,256]{2,1,0:T(8,128)(2,1)S(1)}, u32[]{:S(2)}, u32[]{:S(2)}) collective-permute-start(bf16[8,80,256]{2,1,0:T(8,128)(2,1)S(1)} %get-tuple-element.35), channel_id=1, source_target_pairs={{0,8},{8,16},{16,24},{24,32},{32,40},{40,48},{48,56},{56,64},{64,7... | collective-permute-start | bytes 983048 | tf_op jit(solution)/shard_map/ppermute | solution.py:378
  161.3 9.3 %all-to-all-start.4 = ((bf16[4,32,128]{2,1,0:T(8,128)(2,1)}), bf16[4,32,128]{2,1,0:T(8,128)(2,1)S(1)}, u32[]{:S(2)}, u32[]{:S(2)}) async-start(bf16[4,32,128]{2,1,0:T(8,128)(2,1)} %far.1), calls=%async_computation.4 | async-start | bytes 65536 | tf_op jit(solution)/shard_map/all_to_all | solution.py:327
  164.7 68.1 %reduce-scatter.2.cloned.1.call-start = ((), (), s32[]{:S(2)}) async-start(), calls=%async_computation.7 | async-start | bytes 2621440 | tf_op jit(solution)/shard_map/reduce_scatter | solution.py:450
  165.6 5.0 %collective-permute-start = (bf16[16,2048]{1,0:T(8,128)(2,1)S(1)}, bf16[16,2048]{1,0:T(8,128)(2,1)S(1)}, u32[]{:S(2)}, u32[]{:S(2)}) collective-permute-start(bf16[16,2048]{1,0:T(8,128)(2,1)S(1)} %slice_bitcast_fusion), channel_id=1, source_target_pairs={{0,8},{8,16},{16,24},{24,32},{32,40},{40,48},{48,56},{56,64},{64,7... | collective-permute-start | bytes 196616 | tf_op jit(solution)/shard_map/ppermute | solution.py:384
  189.5 3.8 %collective-permute-start.3 = (bf16[2,512,256]{2,1,0:T(8,128)(2,1)S(1)}, bf16[2,512,256]{2,1,0:T(8,128)(2,1)S(1)}, u32[]{:S(2)}, u32[]{:S(2)}) collective-permute-start(bf16[2,512,256]{2,1,0:T(8,128)(2,1)S(1)} %get-tuple-element.33.mine), channel_id=1, source_target_pairs={{0,4},{4,0},{1,5},{5,1},{2,6},{6,2},{3,7},{7,3},{8,12},{12,8},{9,1... | collective-permute-start | bytes 1572872 | tf_op jit(solution)/shard_map/ppermute | solution.py:446
Sparse Core Ops, SparseCore 0:
  9.5 171.4 all-gather.1
  196.2 36.5 reduce-scatter.1

commit v6 on v5

--- a/solution.py
+++ b/solution.py
@@ -105,8 +105,15 @@
 
 
 def kv_kernel(
-    pair, x, same, low, high, own, cos_far, sin_far, cos_near, sin_near, k_out, v_out, cosine, sine, decay, column, totals, message, weight
+    pair, x, same, low, high, own, cos_far, sin_far, cos_near, sin_near, k_out, v_out, cosine, sine, decay, column, totals, message, last, x_kept, weight, semaphores
 ):
+    per = BLOCK // x.shape[1]
+    copies = [
+        pltpu.make_async_copy(x.at[pl.ds(i * per, per)], x_kept.at[pl.ds(i * per, per)], semaphores.at[i])
+        for i in range(x.shape[0] // per)
+    ]
+    for copy in copies:
+        copy.start()
     rows, width = x.shape[0] * x.shape[1], x.shape[2]
     half = low.shape[0]
     shard = own.shape[1] - EXTRA
@@ -159,7 +166,8 @@
         sin_at = jnp.where(first, -sin_at, sin_at)
         cosine[at, :] = cos_at
         sine[at, :] = sin_at
-        both = dot(block_rows(x, i), weight[...], ((1,), (0,))).astype(BF16)
+        copies[i].wait()
+        both = dot(block_rows(x_kept, i), weight[...], ((1,), (0,))).astype(BF16)
         key = rotated(both[:, :HEAD].astype(F32), cos_at, sin_at) * HEAD ** (-0.5)
         k_out[at, :] = key.astype(BF16)
         value = both[:, HEAD:]
@@ -169,6 +177,7 @@
         state = state + dot(faded, value, ((0,), (0,)))
     for copy in range(message.shape[0]):
         message[copy] = state.astype(BF16)
+    last[...] = x_kept[x.shape[0] - 1, x.shape[1] - RIM :, :]
 
 
 def block_rows(x, i):
@@ -218,7 +227,7 @@
 def branch_kernel(
     core,
     weights,
-    x,
+    x_far,
     halo,
     cosine,
     sine,
@@ -232,10 +241,12 @@
     taps,
     branches,
     out_weight,
+    x,
     weight,
     semaphores,
 ):
     rows = x.shape[0] * x.shape[1]
+    blocks = rows // BLOCK
     own = core[0]
     start_at = pl.multiple_of(own * COLUMNS, HEAD)
     other_at = pl.multiple_of((1 - own) * COLUMNS, HEAD)
@@ -256,7 +267,19 @@
             weights.at[:, pl.ds(other_at + PROJECTED, 2 * HEAD)], out_weight.at[1], semaphores.at[1]
         ),
     ]
-    for copy in copies:
+    per_block = x.shape[0] // blocks
+    x_copies = [
+        pltpu.make_async_copy(
+            x_far.at[pl.ds(i * per_block, per_block)],
+            x.at[pl.ds(i * per_block, per_block)],
+            semaphores.at[PIECES + 2 + i],
+        )
+        for i in range(blocks)
+    ]
+    x_copies[0].start()
+    for copy in copies[:PIECES]:
+        copy.start()
+    for copy in x_copies[1:]:
         copy.start()
     incoming = jnp.concatenate([base[at].astype(F32) for at in range(base.shape[0])], axis=0)
     state = fade[0:1, :] * incoming + before[...]
@@ -268,10 +291,13 @@
     start = jnp.zeros((1, 1), F32)
     per = BLOCK // HEAD
     first = jnp.zeros((BLOCK, PROJECTED), F32)
+    x_copies[0].wait()
     for at in range(PIECES):
         copies[at].wait()
         cut = slice(at * piece, (at + 1) * piece)
         first = first + dot(block_rows(x, 0)[:, cut], weight[cut, :], ((1,), (0,)))
+    for copy in copies[PIECES:]:
+        copy.start()
     rim = dot(halo[...], weight[:, HEAD : 3 * HEAD], ((1,), (0,))).astype(BF16).astype(F32)
     tail = (rim[:, :HEAD] * rim[:, HEAD:])[RIM - 8 :]
     for i in range(rows // BLOCK):
@@ -279,6 +305,8 @@
         half = (i * BLOCK) // (rows // 2)
         place = slice(i * BLOCK - half * (rows // 2), (i + 1) * BLOCK - half * (rows // 2))
         slot = jnp.where(own == half, 0, 1)
+        if i:
+            x_copies[i].wait()
         projected = (dot(block_rows(x, i), weight[...], ((1,), (0,))) if i else first).astype(BF16)
         outer = projected[:, :HEAD].astype(F32)
         mixed = projected[:, HEAD : 2 * HEAD].astype(F32) * projected[:, 2 * HEAD : 3 * HEAD].astype(F32)
@@ -321,6 +349,13 @@
         total = total.astype(BF16)
         for part in range(parts):
             out[part, :, column : column + step] = total[part * rows : (part + 1) * rows]
+
+
+def sum_kernel(parts, out):
+    total = parts[0].astype(F32)
+    for at in range(1, parts.shape[0]):
+        total = total + parts[at].astype(F32)
+    out[...] = total.astype(BF16)
 
 
 def exchanged(x, axes):
@@ -381,14 +416,13 @@
         tokens, norm_gain
     )
     x = exchanged(normed, ("core", "tp"))
-    halo = lax.ppermute(x[-1, own_rows - RIM :], CHIPS, [(i, i + 1) for i in range(chips - 1)])
 
     inv_freq = ROTARY_BASE ** (-jnp.arange(HALF, dtype=F32) / HALF)
     inv_freq = jnp.concatenate([inv_freq, inv_freq])[None, :]
     far_angle = ((chip * rows).astype(F32) + BLOCK * jnp.arange(8, dtype=F32))[:, None] * inv_freq
     near_angle = jnp.arange(BLOCK, dtype=F32)[:, None] * inv_freq
 
-    keys, values, cosine, sine, decay, column, totals, message = call(
+    keys, values, cosine, sine, decay, column, totals, message, last = call(
         kv_kernel,
         [
             fast((rows, HEAD), BF16),
@@ -399,12 +433,19 @@
             fast((HEAD, HEAD), F32),
             fast((chips, HEAD), F32),
             fast((near, HEAD, HEAD), BF16),
+            fast((RIM, width), BF16),
         ],
         "kv",
-        specs=[SMEM] + [VMEM] * 9,
-        scratch=[pltpu.VMEM((width, 2 * HEAD), BF16)],
+        specs=[SMEM, ANY] + [VMEM] * 8,
+        scratch=[
+            pltpu.VMEM(x.shape, BF16),
+            pltpu.VMEM((width, 2 * HEAD), BF16),
+            pltpu.SemaphoreType.DMA((rows // BLOCK,)),
+        ],
         flops=4 * rows * width * HEAD,
     )(lax.axis_index("zc").reshape(1), x, same, low, high, own, jnp.cos(far_angle), jnp.sin(far_angle), jnp.cos(near_angle), jnp.sin(near_angle))
+
+    halo = lax.ppermute(last, CHIPS, [(i, i + 1) for i in range(chips - 1)])
 
     share = HEAD // near
     block = lax.axis_index("za").reshape(1)
@@ -424,8 +465,12 @@
         branch_kernel,
         [fast((2, rows // 2, 2 * HEAD), BF16), fast((2, width, 2 * HEAD), BF16)],
         "branch",
-        specs=[SMEM, ANY] + [VMEM] * 12,
-        scratch=[pltpu.VMEM((width, PROJECTED), BF16), pltpu.SemaphoreType.DMA((PIECES + 2,))],
+        specs=[SMEM, ANY, ANY] + [VMEM] * 11,
+        scratch=[
+            pltpu.VMEM(x.shape, BF16),
+            pltpu.VMEM((width, PROJECTED), BF16),
+            pltpu.SemaphoreType.DMA((PIECES + 2 + rows // BLOCK,)),
+        ],
         flops=10 * rows * width * HEAD,
     )(
         core.reshape(1),
@@ -444,10 +489,11 @@
         conv_taps,
     )
     theirs = lax.ppermute(branches, "core", [(0, 1), (1, 0)])
-    (partial,) = call(out_kernel, [slow((tp, own_rows, width), BF16)], "out", flops=rows * width * 4 * HEAD)(
+    (partial,) = call(out_kernel, [fast((tp, own_rows, width), BF16)], "out", flops=rows * width * 4 * HEAD)(
         branches, theirs, out_weight
     )
-    return lax.psum_scatter(partial.reshape(tp * own_rows, width), "tp", scatter_dimension=0, tiled=True)
+    (mixed,) = call(sum_kernel, [slow((own_rows, width), BF16)], "sum")(exchanged(partial, "tp"))
+    return mixed
 
 
 def solution(mesh):

time: 240 us -> 231 us (0.963)
  waiting for transfers between devices: 57.6 us -> 25.4 us
  blocking collectives: 79.2 us -> 105 us
    reduce_scatter x1 -> x0, waiting for transfers between devices: 36.7 us -> none  [body(): lax.psum_scatter(partial.reshape(tp * own_rows, width), 'tp', scatter_dim...]
    all_to_all x2 -> x3, blocking collectives: 44.4 us -> 70 us  [exchanged(): return lax.all_to_all(x, axes, 0, 0, tiled=True)]
    all_gather x1, waiting for transfers between devices: 10.4 us -> 14.1 us  [body(): weights = lax.all_gather(rest, STRETCHES, axis=0, tiled=True)]
    pallas_call x7 -> x8, Pallas kernels: 21.9 us -> 20.8 us  [run(): pl.pallas_call(kernel, out_shape=[o[0] for o in outs], in_specs=in_specs,...]
  transfers between devices with their start and end apart: 9 -> 8, of which waited for: 6 -> 5; matrix products, arithmetic and copies ran while one was open for 1% -> 0% of each run, Pallas kernels for 4% -> 4%
where the time goes in v6:
time: 231 us
  blocking collectives  105 us (45%)
  starting transfers between devices  65.3 us (28%)
  waiting for transfers between devices  25.4 us (11%)
  Pallas kernels  20.8 us (9%)
  between operations  13.5 us (6%)
    all_to_all x3, blocking collectives, exchanged(): return lax.all_to_all(x, axes, 0, 0, tiled=True)  70 us
    all_to_all x3, starting transfers between devices, exchanged(): return lax.all_to_all(x, axes, 0, 0, tiled=True)  52.8 us
    all_gather x1, blocking collectives, body(): same = lax.all_gather(own.reshape(2 * (shard + EXTRA), 2 * HEAD), FAR)  35.1 us
    pallas_call x8, Pallas kernels, run(): pl.pallas_call(kernel, out_shape=[o[0] for o in outs], in_specs=in_specs,...  20.8 us
    all_gather x1, waiting for transfers between devices, body(): weights = lax.all_gather(rest, STRETCHES, axis=0, tiled=True)  14.1 us
    ppermute x1, waiting for transfers between devices, body(): lax.ppermute(same[:half], CHIPS, [(i, (i - 1) % chips) for i in range(chi...  4.8 us
  transfers between devices with their start and end apart: 8, of which 5 were waited for; matrix products, arithmetic and copies ran while one was open for 0% of the time, Pallas kernels for 4%

profile of v6, /device:TPU:33, one launch (start us, length us, event | category | flops | bytes accessed | tf_op | source)
XLA Modules:
  0.0 230.8 jit_solution(6063028344646398081)
XLA Ops:
  6.5 0.0 all-gather.2.cloned.1.call-start
  6.6 1.5 pack.1
  8.1 0.1 all-gather.2.cloned.1.call-update
  8.2 44.7 %all-to-all-start.1 = ((bf16[2,40,256]{2,1,0:T(8,128)(2,1)}), bf16[2,40,256]{2,1,0:T(8,128)(2,1)S(1)}, u32[]{:S(2)}, u32[]{:S(2)}) async-start(bf16[2,40,256]{2,1,0:T(8,128)(2,1)} %get-tuple-element.22), calls=%async_computation.1 | async-start | bytes 81920 | tf_op jit(solution)/shard_map/all_to_all | solution.py:362
  52.9 3.5 %norm.1 = bf16[8,128,2048]{2,1,0:T(8,128)(2,1)} custom-call(bf16[128,2048]{1,0:T(8,128)(2,1)} %tokens.1, bf16[2048]{0:T(1024)(128)(2,1)} %gain.1), custom_call_target="tpu_custom_call" | custom-call | tf_op jit(solution)/shard_map/norm/pallas_call | solution.py:38
  56.4 0.0 all-to-all-done.1.own
  56.4 4.6 %all-to-all-start = ((bf16[8,128,2048]{2,1,0:T(8,128)(2,1)}), bf16[8,128,2048]{2,1,0:T(8,128)(2,1)}, u32[]{:S(2)}, u32[]{:S(2)}) async-start(bf16[8,128,2048]{2,1,0:T(8,128)(2,1)} %norm.1), calls=%async_computation | async-start | bytes 8388608 | tf_op jit(solution)/shard_map/all_to_all | solution.py:362
  61.0 35.1 %all_gather.7.same = bf16[16,80,256]{2,1,0:T(8,128)(2,1)S(1)} all-gather(bf16[1,80,256]{2,1,0:T(8,128)(2,1)S(1)} %bitcast.8), channel_id=1, replica_groups=mesh['grp'=2,'za'=8,'zb'=2,'zc'=2,'core'=2,'tp'=4] {'za','zb'}, dimensions={0}, use_global_device_ids=true | all-gather | bytes 696320 | tf_op jit(solution)/shard_map/all_gather | solution.py:410
  96.1 0.0 copy-start
  96.1 4.1 %collective-permute-start = (bf16[8,80,256]{2,1,0:T(8,128)(2,1)S(1)}, bf16[8,80,256]{2,1,0:T(8,128)(2,1)S(1)}, u32[]{:S(2)}, u32[]{:S(2)}) collective-permute-start(bf16[8,80,256]{2,1,0:T(8,128)(2,1)S(1)} %get-tuple-element.38), channel_id=1, source_target_pairs={{0,248},{8,0},{16,8},{24,16},{32,24},{40,32},{48,40},{56,48},{64,5... | collective-permute-start | bytes 983048 | tf_op jit(solution)/shard_map/ppermute | solution.py:412
  100.3 2.6 %collective-permute-start.1 = (bf16[8,80,256]{2,1,0:T(8,128)(2,1)S(1)}, bf16[8,80,256]{2,1,0:T(8,128)(2,1)S(1)}, u32[]{:S(2)}, u32[]{:S(2)}) collective-permute-start(bf16[8,80,256]{2,1,0:T(8,128)(2,1)S(1)} %get-tuple-element.37), channel_id=1, source_target_pairs={{0,8},{8,16},{16,24},{24,32},{32,40},{40,48},{48,56},{56,64},{64,7... | collective-permute-start | bytes 983048 | tf_op jit(solution)/shard_map/ppermute | solution.py:413
  102.9 0.1 pad_maximum_fusion
  103.0 0.1 multiply_sine_fusion
  103.1 0.5 fusion
  103.6 4.8 %collective-permute-done.low = bf16[8,80,256]{2,1,0:T(8,128)(2,1)S(1)} collective-permute-done((bf16[8,80,256]{2,1,0:T(8,128)(2,1)S(1)}, bf16[8,80,256]{2,1,0:T(8,128)(2,1)S(1)}, u32[]{:S(2)}, u32[]{:S(2)}) %collective-permute-start) | collective-permute-done | bytes 327712 | tf_op jit(solution)/shard_map/ppermute | solution.py:412
  108.4 3.5 %collective-permute-done.1.high = bf16[8,80,256]{2,1,0:T(8,128)(2,1)S(1)} collective-permute-done((bf16[8,80,256]{2,1,0:T(8,128)(2,1)S(1)}, bf16[8,80,256]{2,1,0:T(8,128)(2,1)S(1)}, u32[]{:S(2)}, u32[]{:S(2)}) %collective-permute-start.1) | collective-permute-done | bytes 327712 | tf_op jit(solution)/shard_map/ppermute | solution.py:413
  111.9 0.0 all-to-all-done.x.x_far
  111.9 5.4 %kv.1 = (bf16[1024,128]{1,0:T(8,128)(2,1)S(1)}, bf16[1024,128]{1,0:T(8,128)(2,1)S(1)}, f32[1024,128]{1,0:T(8,128)S(1)}, f32[1024,128]{1,0:T(8,128)S(1)}, f32[8,1...) custom-call(s32[1]{0:T(128)} %bitcast.4.pair, ...), custom_call_target="tpu_custom_call" | custom-call | flops 1073741824 | tf_op jit(solution)/shard_map/kv/pallas_call | solution.py:38
  117.3 8.4 %all_to_all.30.gathered = bf16[4,128,128]{2,1,0:T(8,128)(2,1)S(1)} all-to-all(bf16[4,128,128]{2,1,0:T(8,128)(2,1)S(1)} %get-tuple-element.31), channel_id=1, replica_groups=mesh['grp'=2,'za'=8,'zb'=2,'zc'=2,'core'=2,'tp'=4] {'zb','zc'}, dimensions={0} | all-to-all | bytes 262144 | tf_op jit(solution)/shard_map/all_to_all | solution.py:362
  125.7 0.1 near.1
  125.7 31.7 %all_to_all.31.gathered = bf16[8,32,128]{2,1,0:T(8,128)(2,1)S(1)} all-to-all(bf16[8,32,128]{2,1,0:T(8,128)(2,1)S(1)} %get-tuple-element.32), channel_id=1, replica_groups=mesh['grp'=2,'za'=8,'zb'=2,'zc'=2,'core'=2,'tp'=4] {'za'}, dimensions={0} | all-to-all | bytes 131072 | tf_op jit(solution)/shard_map/all_to_all | solution.py:362
  157.4 0.6 far.1
  158.0 3.5 %all-to-all-start.4 = ((bf16[4,32,128]{2,1,0:T(8,128)(2,1)}), bf16[4,32,128]{2,1,0:T(8,128)(2,1)S(1)}, u32[]{:S(2)}, u32[]{:S(2)}) async-start(bf16[4,32,128]{2,1,0:T(8,128)(2,1)} %far.1), calls=%async_computation.4 | async-start | bytes 65536 | tf_op jit(solution)/shard_map/all_to_all | solution.py:362
  161.6 3.5 %collective-permute-start.2 = (bf16[16,2048]{1,0:T(8,128)(2,1)S(1)}, bf16[16,2048]{1,0:T(8,128)(2,1)S(1)}, u32[]{:S(2)}, u32[]{:S(2)}) collective-permute-start(bf16[16,2048]{1,0:T(8,128)(2,1)S(1)} %get-tuple-element.23), channel_id=1, source_target_pairs={{0,8},{8,16},{16,24},{24,32},{32,40},{40,48},{48,56},{56,64},{64,7... | collective-permute-start | bytes 196616 | tf_op jit(solution)/shard_map/ppermute | solution.py:448
  165.1 1.3 collective-permute-done.2.halo
  166.4 0.0 all-to-all-done.4.base
  166.4 14.1 %all-gather.2.cloned.1.call-done.weights = bf16[2048,1792]{1,0:T(8,128)(2,1)} async-done(((bf16[32,1792]{1,0:T(8,128)(2,1)}), bf16[2048,1792]{1,0:T(8,128)(2,1)}) %all-gather.2.cloned.1.call-update) | async-done | bytes 7340048 | tf_op jit(solution)/shard_map/all_gather | solution.py:407
  180.5 0.0 copy-done
  180.5 7.3 %branch.1 = (bf16[2,512,256]{2,1,0:T(8,128)(2,1)S(1)}, bf16[2,2048,256]{2,1,0:T(8,128)(2,1)S(1)}) custom-call(s32[1]{0:T(128)} %bitcast.core, bf16[2048,1792]{1,0:T(8,128)(2,1)} %all-gather.2.cloned.1.call-done.weights, bf16[8,128,2048]{2,1,0:T(8,128)(2,1)} %all-to-all-done.x.x_far, bf16[16,2048]{1,0:T(8,128)(2,1)S(1)} %collective-permute-done.2.halo, ...), custom_call_target="tpu_custom_call" | custom-call | flops 2684354560 | tf_op jit(solution)/shard_map/branch/pallas_call | solution.py:38
  187.9 2.2 collective-permute-start.3
  190.1 1.6 collective-permute-done.3.theirs
  191.7 1.3 out.1
  193.0 29.9 %all_to_all.32.parts = bf16[4,128,2048]{2,1,0:T(8,128)(2,1)S(1)} all-to-all(bf16[4,128,2048]{2,1,0:T(8,128)(2,1)S(1)} %out.1), channel_id=1, replica_groups=mesh['grp'=2,'za'=8,'zb'=2,'zc'=2,'core'=2,'tp'=4] {'tp'}, dimensions={0} | all-to-all | bytes 4194304 | tf_op jit(solution)/shard_map/all_to_all | solution.py:362
  222.9 1.0 sum.1
  (3 shorter events, 0.1 us)
Async XLA Ops:
  6.5 174.0 %all-gather.2.cloned.1.call-start = ((), (), s32[]{:S(2)}) async-start(), calls=%async_computation.6 | async-start | bytes 7454720 | tf_op jit(solution)/shard_map/all_gather | solution.py:407
  8.2 48.3 %all-to-all-start.1 = ((bf16[2,40,256]{2,1,0:T(8,128)(2,1)}), bf16[2,40,256]{2,1,0:T(8,128)(2,1)S(1)}, u32[]{:S(2)}, u32[]{:S(2)}) async-start(bf16[2,40,256]{2,1,0:T(8,128)(2,1)} %get-tuple-element.22), calls=%async_computation.1 | async-start | bytes 81920 | tf_op jit(solution)/shard_map/all_to_all | solution.py:362
  56.4 55.5 %all-to-all-start = ((bf16[8,128,2048]{2,1,0:T(8,128)(2,1)}), bf16[8,128,2048]{2,1,0:T(8,128)(2,1)}, u32[]{:S(2)}, u32[]{:S(2)}) async-start(bf16[8,128,2048]{2,1,0:T(8,128)(2,1)} %norm.1), calls=%async_computation | async-start | bytes 8388608 | tf_op jit(solution)/shard_map/all_to_all | solution.py:362
  96.1 84.5 %copy-start = (bf16[3,256]{1,0:T(4,128)(2,1)S(1)}, bf16[3,256]{1,0:T(4,128)(2,1)}, u32[]{:S(2)}) copy-start(bf16[3,256]{1,0:T(4,128)(2,1)} %taps.1) | copy-start | bytes 4612
  96.1 12.2 %collective-permute-start = (bf16[8,80,256]{2,1,0:T(8,128)(2,1)S(1)}, bf16[8,80,256]{2,1,0:T(8,128)(2,1)S(1)}, u32[]{:S(2)}, u32[]{:S(2)}) collective-permute-start(bf16[8,80,256]{2,1,0:T(8,128)(2,1)S(1)} %get-tuple-element.38), channel_id=1, source_target_pairs={{0,248},{8,0},{16,8},{24,16},{32,24},{40,32},{48,40},{56,48},{64,5... | collective-permute-start | bytes 983048 | tf_op jit(solution)/shard_map/ppermute | solution.py:412
  100.3 11.6 %collective-permute-start.1 = (bf16[8,80,256]{2,1,0:T(8,128)(2,1)S(1)}, bf16[8,80,256]{2,1,0:T(8,128)(2,1)S(1)}, u32[]{:S(2)}, u32[]{:S(2)}) collective-permute-start(bf16[8,80,256]{2,1,0:T(8,128)(2,1)S(1)} %get-tuple-element.37), channel_id=1, source_target_pairs={{0,8},{8,16},{16,24},{24,32},{32,40},{40,48},{48,56},{56,64},{64,7... | collective-permute-start | bytes 983048 | tf_op jit(solution)/shard_map/ppermute | solution.py:413
  158.0 8.4 %all-to-all-start.4 = ((bf16[4,32,128]{2,1,0:T(8,128)(2,1)}), bf16[4,32,128]{2,1,0:T(8,128)(2,1)S(1)}, u32[]{:S(2)}, u32[]{:S(2)}) async-start(bf16[4,32,128]{2,1,0:T(8,128)(2,1)} %far.1), calls=%async_computation.4 | async-start | bytes 65536 | tf_op jit(solution)/shard_map/all_to_all | solution.py:362
  161.6 4.8 %collective-permute-start.2 = (bf16[16,2048]{1,0:T(8,128)(2,1)S(1)}, bf16[16,2048]{1,0:T(8,128)(2,1)S(1)}, u32[]{:S(2)}, u32[]{:S(2)}) collective-permute-start(bf16[16,2048]{1,0:T(8,128)(2,1)S(1)} %get-tuple-element.23), channel_id=1, source_target_pairs={{0,8},{8,16},{16,24},{24,32},{32,40},{40,48},{48,56},{56,64},{64,7... | collective-permute-start | bytes 196616 | tf_op jit(solution)/shard_map/ppermute | solution.py:448
  187.9 3.8 %collective-permute-start.3 = (bf16[2,512,256]{2,1,0:T(8,128)(2,1)S(1)}, bf16[2,512,256]{2,1,0:T(8,128)(2,1)S(1)}, u32[]{:S(2)}, u32[]{:S(2)}) collective-permute-start(bf16[2,512,256]{2,1,0:T(8,128)(2,1)S(1)} %get-tuple-element.35.mine), channel_id=1, source_target_pairs={{0,4},{4,0},{1,5},{5,1},{2,6},{6,2},{3,7},{7,3},{8,12},{12,8},{9,1... | collective-permute-start | bytes 1572872 | tf_op jit(solution)/shard_map/ppermute | solution.py:491
Sparse Core Ops, SparseCore 0:
  9.5 171.0 all-gather.1

commit v7 on v6

--- a/solution.py
+++ b/solution.py
@@ -104,12 +104,24 @@
     return head * cosine + pltpu.roll(head, HALF, 1) * sine
 
 
+def table(i, cos_far, sin_far, cos_near, sin_near):
+    cos_at = cos_far[i : i + 1, :] * cos_near[...] - sin_far[i : i + 1, :] * sin_near[...]
+    sin_at = sin_far[i : i + 1, :] * cos_near[...] + cos_far[i : i + 1, :] * sin_near[...]
+    first = lax.broadcasted_iota(jnp.int32, sin_at.shape, 1) < HALF
+    return cos_at, jnp.where(first, -sin_at, sin_at)
+
+
 def kv_kernel(
-    pair, x, same, low, high, own, cos_far, sin_far, cos_near, sin_near, k_out, v_out, cosine, sine, decay, column, totals, message, last, x_kept, weight, semaphores
+    pair, x, same, low, high, own, cos_far, sin_far, cos_near, sin_near, k_out, v_out, decay, column, totals, message, last, x_early, x_late, weight, semaphores
 ):
     per = BLOCK // x.shape[1]
+    early = x_early.shape[0] // per
     copies = [
-        pltpu.make_async_copy(x.at[pl.ds(i * per, per)], x_kept.at[pl.ds(i * per, per)], semaphores.at[i])
+        pltpu.make_async_copy(
+            x.at[pl.ds(i * per, per)],
+            (x_early.at[pl.ds(i * per, per)] if i < early else x_late.at[pl.ds((i - early) * per, per)]),
+            semaphores.at[i],
+        )
         for i in range(x.shape[0] // per)
     ]
     for copy in copies:
@@ -160,14 +172,9 @@
     state = jnp.zeros((HEAD, HEAD), F32)
     for i in range(rows // BLOCK):
         at = pl.ds(i * BLOCK, BLOCK)
-        cos_at = cos_far[i : i + 1, :] * cos_near[...] - sin_far[i : i + 1, :] * sin_near[...]
-        sin_at = sin_far[i : i + 1, :] * cos_near[...] + cos_far[i : i + 1, :] * sin_near[...]
-        first = lax.broadcasted_iota(jnp.int32, sin_at.shape, 1) < HALF
-        sin_at = jnp.where(first, -sin_at, sin_at)
-        cosine[at, :] = cos_at
-        sine[at, :] = sin_at
+        cos_at, sin_at = table(i, cos_far, sin_far, cos_near, sin_near)
         copies[i].wait()
-        both = dot(block_rows(x_kept, i), weight[...], ((1,), (0,))).astype(BF16)
+        both = dot(block_rows(x_early, i) if i < early else block_rows(x_late, i - early), weight[...], ((1,), (0,))).astype(BF16)
         key = rotated(both[:, :HEAD].astype(F32), cos_at, sin_at) * HEAD ** (-0.5)
         k_out[at, :] = key.astype(BF16)
         value = both[:, HEAD:]
@@ -177,7 +184,7 @@
         state = state + dot(faded, value, ((0,), (0,)))
     for copy in range(message.shape[0]):
         message[copy] = state.astype(BF16)
-    last[...] = x_kept[x.shape[0] - 1, x.shape[1] - RIM :, :]
+    last[...] = x_late[x_late.shape[0] - 1, x.shape[1] - RIM :, :]
 
 
 def block_rows(x, i):
@@ -228,9 +235,12 @@
     core,
     weights,
     x_far,
+    x_early,
     halo,
-    cosine,
-    sine,
+    cos_far,
+    sin_far,
+    cos_near,
+    sin_near,
     decay,
     column,
     keys,
@@ -240,46 +250,36 @@
     fade,
     taps,
     branches,
-    out_weight,
-    x,
+    x_late,
     weight,
     semaphores,
 ):
-    rows = x.shape[0] * x.shape[1]
+    rows = x_far.shape[0] * x_far.shape[1]
     blocks = rows // BLOCK
     own = core[0]
     start_at = pl.multiple_of(own * COLUMNS, HEAD)
-    other_at = pl.multiple_of((1 - own) * COLUMNS, HEAD)
     piece = weight.shape[0] // PIECES
     copies = [
         *(
             pltpu.make_async_copy(
                 weights.at[pl.ds(at, piece), pl.ds(start_at, PROJECTED)],
                 weight.at[pl.ds(at, piece), :],
-                semaphores.at[2 + at // piece],
+                semaphores.at[at // piece],
             )
             for at in range(0, weight.shape[0], piece)
         ),
-        pltpu.make_async_copy(
-            weights.at[:, pl.ds(start_at + PROJECTED, 2 * HEAD)], out_weight.at[0], semaphores.at[0]
-        ),
-        pltpu.make_async_copy(
-            weights.at[:, pl.ds(other_at + PROJECTED, 2 * HEAD)], out_weight.at[1], semaphores.at[1]
-        ),
     ]
-    per_block = x.shape[0] // blocks
+    per_block = x_far.shape[0] // blocks
+    early = x_early.shape[0] // per_block
     x_copies = [
         pltpu.make_async_copy(
             x_far.at[pl.ds(i * per_block, per_block)],
-            x.at[pl.ds(i * per_block, per_block)],
-            semaphores.at[PIECES + 2 + i],
+            x_late.at[pl.ds((i - early) * per_block, per_block)],
+            semaphores.at[PIECES + i - early],
         )
-        for i in range(blocks)
+        for i in range(early, blocks)
     ]
-    x_copies[0].start()
-    for copy in copies[:PIECES]:
-        copy.start()
-    for copy in x_copies[1:]:
+    for copy in (*copies, *x_copies):
         copy.start()
     incoming = jnp.concatenate([base[at].astype(F32) for at in range(base.shape[0])], axis=0)
     state = fade[0:1, :] * incoming + before[...]
@@ -291,13 +291,10 @@
     start = jnp.zeros((1, 1), F32)
     per = BLOCK // HEAD
     first = jnp.zeros((BLOCK, PROJECTED), F32)
-    x_copies[0].wait()
     for at in range(PIECES):
         copies[at].wait()
         cut = slice(at * piece, (at + 1) * piece)
-        first = first + dot(block_rows(x, 0)[:, cut], weight[cut, :], ((1,), (0,)))
-    for copy in copies[PIECES:]:
-        copy.start()
+        first = first + dot(block_rows(x_early, 0)[:, cut], weight[cut, :], ((1,), (0,)))
     rim = dot(halo[...], weight[:, HEAD : 3 * HEAD], ((1,), (0,))).astype(BF16).astype(F32)
     tail = (rim[:, :HEAD] * rim[:, HEAD:])[RIM - 8 :]
     for i in range(rows // BLOCK):
@@ -305,9 +302,11 @@
         half = (i * BLOCK) // (rows // 2)
         place = slice(i * BLOCK - half * (rows // 2), (i + 1) * BLOCK - half * (rows // 2))
         slot = jnp.where(own == half, 0, 1)
-        if i:
-            x_copies[i].wait()
-        projected = (dot(block_rows(x, i), weight[...], ((1,), (0,))) if i else first).astype(BF16)
+        if i >= early:
+            x_copies[i - early].wait()
+        rows_at = block_rows(x_early, i) if i < early else block_rows(x_late, i - early)
+        cos_at, sin_at = table(i, cos_far, sin_far, cos_near, sin_near)
+        projected = (dot(rows_at, weight[...], ((1,), (0,))) if i else first).astype(BF16)
         outer = projected[:, :HEAD].astype(F32)
         mixed = projected[:, HEAD : 2 * HEAD].astype(F32) * projected[:, 2 * HEAD : 3 * HEAD].astype(F32)
         one = jnp.where(row == 0, tail[7:8], pltpu.roll(mixed, 1, 0))
@@ -316,7 +315,7 @@
         tail = mixed[BLOCK - 8 :]
         branches[slot, place, :HEAD] = (outer * conv).astype(BF16)
 
-        query = rotated(projected[:, 3 * HEAD : 4 * HEAD].astype(F32), cosine[at, :], sine[at, :])
+        query = rotated(projected[:, 3 * HEAD : 4 * HEAD].astype(F32), cos_at, sin_at)
         query = query.astype(BF16)
         key, value = keys[at, :], values[at, :]
         here = block_column(column, i)
@@ -336,8 +335,20 @@
 
         branches[slot, place, HEAD:] = ret_branch
 
-    copies[PIECES].wait()
-    copies[PIECES + 1].wait()
+
+def fetch_kernel(core, weights, after, out, semaphores):
+    del after
+    own = core[0]
+    copies = []
+    for side, half in enumerate((own, 1 - own)):
+        at = pl.multiple_of(half * COLUMNS + PROJECTED, HEAD)
+        copies.append(
+            pltpu.make_async_copy(weights.at[:, pl.ds(at, 2 * HEAD)], out.at[side], semaphores.at[side])
+        )
+    for copy in copies:
+        copy.start()
+    for copy in copies:
+        copy.wait()
 
 
 def out_kernel(mine, theirs, weight, out):
@@ -421,29 +432,30 @@
     inv_freq = jnp.concatenate([inv_freq, inv_freq])[None, :]
     far_angle = ((chip * rows).astype(F32) + BLOCK * jnp.arange(8, dtype=F32))[:, None] * inv_freq
     near_angle = jnp.arange(BLOCK, dtype=F32)[:, None] * inv_freq
-
-    keys, values, cosine, sine, decay, column, totals, message, last = call(
+    tables = (jnp.cos(far_angle), jnp.sin(far_angle), jnp.cos(near_angle), jnp.sin(near_angle))
+
+    held = BLOCK // own_rows
+    keys, values, decay, column, totals, message, last, x_early = call(
         kv_kernel,
         [
             fast((rows, HEAD), BF16),
             fast((rows, HEAD), BF16),
-            fast((rows, HEAD), F32),
-            fast((rows, HEAD), F32),
             fast((rows // HEAD, HEAD), F32),
             fast((HEAD, HEAD), F32),
             fast((chips, HEAD), F32),
             fast((near, HEAD, HEAD), BF16),
             fast((RIM, width), BF16),
+            fast((held, own_rows, width), BF16),
         ],
         "kv",
         specs=[SMEM, ANY] + [VMEM] * 8,
         scratch=[
-            pltpu.VMEM(x.shape, BF16),
+            pltpu.VMEM((2 * tp - held, own_rows, width), BF16),
             pltpu.VMEM((width, 2 * HEAD), BF16),
             pltpu.SemaphoreType.DMA((rows // BLOCK,)),
         ],
         flops=4 * rows * width * HEAD,
-    )(lax.axis_index("zc").reshape(1), x, same, low, high, own, jnp.cos(far_angle), jnp.sin(far_angle), jnp.cos(near_angle), jnp.sin(near_angle))
+    )(lax.axis_index("zc").reshape(1), x, same, low, high, own, *tables)
 
     halo = lax.ppermute(last, CHIPS, [(i, i + 1) for i in range(chips - 1)])
 
@@ -461,24 +473,24 @@
     )
     base = exchanged(message, NEAR)
 
-    branches, out_weight = call(
+    (branches,) = call(
         branch_kernel,
-        [fast((2, rows // 2, 2 * HEAD), BF16), fast((2, width, 2 * HEAD), BF16)],
+        [fast((2, rows // 2, 2 * HEAD), BF16)],
         "branch",
-        specs=[SMEM, ANY, ANY] + [VMEM] * 11,
+        specs=[SMEM, ANY, ANY] + [VMEM] * 14,
         scratch=[
-            pltpu.VMEM(x.shape, BF16),
+            pltpu.VMEM((2 * tp - held, own_rows, width), BF16),
             pltpu.VMEM((width, PROJECTED), BF16),
-            pltpu.SemaphoreType.DMA((PIECES + 2 + rows // BLOCK,)),
+            pltpu.SemaphoreType.DMA((PIECES + rows // BLOCK,)),
         ],
         flops=10 * rows * width * HEAD,
     )(
         core.reshape(1),
         weights,
         x,
+        x_early,
         halo,
-        cosine,
-        sine,
+        *tables,
         decay,
         column,
         keys,
@@ -489,6 +501,14 @@
         conv_taps,
     )
     theirs = lax.ppermute(branches, "core", [(0, 1), (1, 0)])
+    (out_weight,) = call(
+        fetch_kernel,
+        [fast((2, width, 2 * HEAD), BF16)],
+        "fetch",
+        specs=[SMEM, ANY, VMEM],
+        scratch=[pltpu.SemaphoreType.DMA((2,))],
+        flops=1 << 28,
+    )(core.reshape(1), weights, branches)
     (partial,) = call(out_kernel, [fast((tp, own_rows, width), BF16)], "out", flops=rows * width * 4 * HEAD)(
         branches, theirs, out_weight
     )

time: 231 us -> 231 us (level)
  waiting for transfers between devices: 25.4 us -> 20 us
  blocking collectives: 105 us -> 108 us
    all_gather x1, waiting for transfers between devices: 14.1 us -> 10.6 us  [body(): weights = lax.all_gather(rest, STRETCHES, axis=0, tiled=True)]
    all_to_all x3, blocking collectives: 70 us -> 72.6 us  [exchanged(): return lax.all_to_all(x, axes, 0, 0, tiled=True)]
    pallas_call x8 -> x9, Pallas kernels: 20.8 us -> 22.1 us  [run(): pl.pallas_call(kernel, out_shape=[o[0] for o in outs], in_specs=in_specs,...]
  transfers between devices with their start and end apart: 8 -> 8, of which waited for: 5 -> 4; matrix products, arithmetic and copies ran while one was open for 0% -> 0% of each run, Pallas kernels for 4% -> 5%
where the time goes in v7:
time: 231 us; the launch traced here: 230 us
  blocking collectives  108 us (47%)
  starting transfers between devices  65.5 us (28%)
  Pallas kernels  22.1 us (10%)
  waiting for transfers between devices  20 us (9%)
  between operations  13.5 us (6%)
    all_to_all x3, blocking collectives, exchanged(): return lax.all_to_all(x, axes, 0, 0, tiled=True)  72.6 us
    all_to_all x3, starting transfers between devices, exchanged(): return lax.all_to_all(x, axes, 0, 0, tiled=True)  52.8 us
    all_gather x1, blocking collectives, body(): same = lax.all_gather(own.reshape(2 * (shard + EXTRA), 2 * HEAD), FAR)  35.3 us
    pallas_call x9, Pallas kernels, run(): pl.pallas_call(kernel, out_shape=[o[0] for o in outs], in_specs=in_specs,...  22.1 us
    all_gather x1, waiting for transfers between devices, body(): weights = lax.all_gather(rest, STRETCHES, axis=0, tiled=True)  10.6 us
    ppermute x1, starting transfers between devices, body(): lax.ppermute(same[:half], CHIPS, [(i, (i - 1) % chips) for i in range(chi...  5.13 us
  transfers between devices with their start and end apart: 8, of which 4 were waited for; matrix products, arithmetic and copies ran while one was open for 0% of the time, Pallas kernels for 5%

profile of v7, /device:TPU:33, one launch (start us, length us, event | category | flops | bytes accessed | tf_op | source)
XLA Modules:
  0.0 229.8 jit_solution(9401436681687710676)
XLA Ops:
  6.5 0.0 all-gather.2.cloned.1.call-start
  6.6 1.5 pack.1
  8.1 0.1 all-gather.2.cloned.1.call-update
  8.1 44.7 %all-to-all-start.1 = ((bf16[2,40,256]{2,1,0:T(8,128)(2,1)}), bf16[2,40,256]{2,1,0:T(8,128)(2,1)S(1)}, u32[]{:S(2)}, u32[]{:S(2)}) async-start(bf16[2,40,256]{2,1,0:T(8,128)(2,1)} %get-tuple-element.19), calls=%async_computation.1 | async-start | bytes 81920 | tf_op jit(solution)/shard_map/all_to_all | solution.py:373
  52.9 3.5 %norm.1 = bf16[8,128,2048]{2,1,0:T(8,128)(2,1)} custom-call(bf16[128,2048]{1,0:T(8,128)(2,1)} %tokens.1, bf16[2048]{0:T(1024)(128)(2,1)} %gain.1), custom_call_target="tpu_custom_call" | custom-call | tf_op jit(solution)/shard_map/norm/pallas_call | solution.py:38
  56.4 0.0 all-to-all-done.1.own
  56.4 4.6 %all-to-all-start = ((bf16[8,128,2048]{2,1,0:T(8,128)(2,1)}), bf16[8,128,2048]{2,1,0:T(8,128)(2,1)}, u32[]{:S(2)}, u32[]{:S(2)}) async-start(bf16[8,128,2048]{2,1,0:T(8,128)(2,1)} %norm.1), calls=%async_computation | async-start | bytes 8388608 | tf_op jit(solution)/shard_map/all_to_all | solution.py:373
  61.0 35.3 %all_gather.7.same = bf16[16,80,256]{2,1,0:T(8,128)(2,1)S(1)} all-gather(bf16[1,80,256]{2,1,0:T(8,128)(2,1)S(1)} %bitcast.8), channel_id=1, replica_groups=mesh['grp'=2,'za'=8,'zb'=2,'zc'=2,'core'=2,'tp'=4] {'za','zb'}, dimensions={0}, use_global_device_ids=true | all-gather | bytes 696320 | tf_op jit(solution)/shard_map/all_gather | solution.py:421
  96.4 0.0 copy-start
  96.4 5.1 %collective-permute-start = (bf16[8,80,256]{2,1,0:T(8,128)(2,1)S(1)}, bf16[8,80,256]{2,1,0:T(8,128)(2,1)S(1)}, u32[]{:S(2)}, u32[]{:S(2)}) collective-permute-start(bf16[8,80,256]{2,1,0:T(8,128)(2,1)S(1)} %get-tuple-element.32), channel_id=1, source_target_pairs={{0,248},{8,0},{16,8},{24,16},{32,24},{40,32},{48,40},{56,48},{64,5... | collective-permute-start | bytes 983048 | tf_op jit(solution)/shard_map/ppermute | solution.py:423
  101.5 2.0 collective-permute-start.1
  103.5 0.1 pad_maximum_fusion
  103.6 0.1 multiply_sine_fusion
  103.7 0.5 fusion
  104.2 4.2 %collective-permute-done.low = bf16[8,80,256]{2,1,0:T(8,128)(2,1)S(1)} collective-permute-done((bf16[8,80,256]{2,1,0:T(8,128)(2,1)S(1)}, bf16[8,80,256]{2,1,0:T(8,128)(2,1)S(1)}, u32[]{:S(2)}, u32[]{:S(2)}) %collective-permute-start) | collective-permute-done | bytes 327712 | tf_op jit(solution)/shard_map/ppermute | solution.py:423
  108.5 3.8 %collective-permute-done.1.high = bf16[8,80,256]{2,1,0:T(8,128)(2,1)S(1)} collective-permute-done((bf16[8,80,256]{2,1,0:T(8,128)(2,1)S(1)}, bf16[8,80,256]{2,1,0:T(8,128)(2,1)S(1)}, u32[]{:S(2)}, u32[]{:S(2)}) %collective-permute-start.1) | collective-permute-done | bytes 327712 | tf_op jit(solution)/shard_map/ppermute | solution.py:424
  112.3 0.0 all-to-all-done.x.x_far
  112.3 5.4 %kv.1 = (bf16[1024,128]{1,0:T(8,128)(2,1)S(1)}, bf16[1024,128]{1,0:T(8,128)(2,1)S(1)}, f32[8,128]{1,0:T(8,128)S(1)}, f32[128,128]{1,0:T(8,128)S(1)}, f32[32,128]...) custom-call(s32[1]{0:T(128)} %bitcast.4.pair, ...), custom_call_target="tpu_custom_call" | custom-call | flops 1073741824 | tf_op jit(solution)/shard_map/kv/pallas_call | solution.py:38
  117.7 8.0 %all_to_all.30.gathered = bf16[4,128,128]{2,1,0:T(8,128)(2,1)S(1)} all-to-all(bf16[4,128,128]{2,1,0:T(8,128)(2,1)S(1)} %get-tuple-element.27), channel_id=1, replica_groups=mesh['grp'=2,'za'=8,'zb'=2,'zc'=2,'core'=2,'tp'=4] {'zb','zc'}, dimensions={0} | all-to-all | bytes 262144 | tf_op jit(solution)/shard_map/all_to_all | solution.py:373
  125.7 34.4 %all_to_all.31.gathered = bf16[8,32,128]{2,1,0:T(8,128)(2,1)S(1)} all-to-all(bf16[8,32,128]{2,1,0:T(8,128)(2,1)S(1)} %get-tuple-element.28), channel_id=1, replica_groups=mesh['grp'=2,'za'=8,'zb'=2,'zc'=2,'core'=2,'tp'=4] {'za'}, dimensions={0} | all-to-all | bytes 131072 | tf_op jit(solution)/shard_map/all_to_all | solution.py:373
  160.1 0.6 far.1
  160.8 3.4 %all-to-all-start.4 = ((bf16[4,32,128]{2,1,0:T(8,128)(2,1)}), bf16[4,32,128]{2,1,0:T(8,128)(2,1)S(1)}, u32[]{:S(2)}, u32[]{:S(2)}) async-start(bf16[4,32,128]{2,1,0:T(8,128)(2,1)} %far.1), calls=%async_computation.4 | async-start | bytes 65536 | tf_op jit(solution)/shard_map/all_to_all | solution.py:373
  164.2 3.4 %collective-permute-start.2 = (bf16[16,2048]{1,0:T(8,128)(2,1)S(1)}, bf16[16,2048]{1,0:T(8,128)(2,1)S(1)}, u32[]{:S(2)}, u32[]{:S(2)}) collective-permute-start(bf16[16,2048]{1,0:T(8,128)(2,1)S(1)} %get-tuple-element.21), channel_id=1, source_target_pairs={{0,8},{8,16},{16,24},{24,32},{32,40},{40,48},{48,56},{56,64},{64,7... | collective-permute-start | bytes 196616 | tf_op jit(solution)/shard_map/ppermute | solution.py:460
  167.6 1.3 collective-permute-done.2.halo
  168.9 0.0 all-to-all-done.4.base
  168.9 10.6 %all-gather.2.cloned.1.call-done.weights = bf16[2048,1792]{1,0:T(8,128)(2,1)} async-done(((bf16[32,1792]{1,0:T(8,128)(2,1)}), bf16[2048,1792]{1,0:T(8,128)(2,1)}) %all-gather.2.cloned.1.call-update) | async-done | bytes 7340048 | tf_op jit(solution)/shard_map/all_gather | solution.py:418
  179.5 0.0 copy-done
  179.5 7.0 %branch.1.after.mine = bf16[2,512,256]{2,1,0:T(8,128)(2,1)S(1)} custom-call(s32[1]{0:T(128)} %bitcast.core, bf16[2048,1792]{1,0:T(8,128)(2,1)} %all-gather.2.cloned.1.call-done.weights, bf16[8,128,2048]{2,1,0:T(8,128)(2,1)} %all-to-all-done.x.x_far, bf16[2,128,2048]{2,1,0:T(8,128)(2,1)S(1)} %get-tuple-element.20.x_early, ...), custom_call_target="tpu_custom_call" | custom-call | flops 2684354560 | tf_op jit(solution)/shard_map/branch/pallas_call | solution.py:38
  186.5 2.2 collective-permute-start.3
  188.8 1.6 fetch.1.weight
  190.4 0.0 collective-permute-done.3.theirs
  190.4 1.3 out.1
  191.7 30.3 %all_to_all.32.parts = bf16[4,128,2048]{2,1,0:T(8,128)(2,1)S(1)} all-to-all(bf16[4,128,2048]{2,1,0:T(8,128)(2,1)S(1)} %out.1), channel_id=1, replica_groups=mesh['grp'=2,'za'=8,'zb'=2,'zc'=2,'core'=2,'tp'=4] {'tp'}, dimensions={0} | all-to-all | bytes 4194304 | tf_op jit(solution)/shard_map/all_to_all | solution.py:373
  221.9 1.0 sum.1
  (4 shorter events, 0.1 us)
Async XLA Ops:
  6.5 172.9 %all-gather.2.cloned.1.call-start = ((), (), s32[]{:S(2)}) async-start(), calls=%async_computation.6 | async-start | bytes 7454720 | tf_op jit(solution)/shard_map/all_gather | solution.py:418
  8.1 48.3 %all-to-all-start.1 = ((bf16[2,40,256]{2,1,0:T(8,128)(2,1)}), bf16[2,40,256]{2,1,0:T(8,128)(2,1)S(1)}, u32[]{:S(2)}, u32[]{:S(2)}) async-start(bf16[2,40,256]{2,1,0:T(8,128)(2,1)} %get-tuple-element.19), calls=%async_computation.1 | async-start | bytes 81920 | tf_op jit(solution)/shard_map/all_to_all | solution.py:373
  56.4 55.9 %all-to-all-start = ((bf16[8,128,2048]{2,1,0:T(8,128)(2,1)}), bf16[8,128,2048]{2,1,0:T(8,128)(2,1)}, u32[]{:S(2)}, u32[]{:S(2)}) async-start(bf16[8,128,2048]{2,1,0:T(8,128)(2,1)} %norm.1), calls=%async_computation | async-start | bytes 8388608 | tf_op jit(solution)/shard_map/all_to_all | solution.py:373
  96.4 83.1 %copy-start = (bf16[3,256]{1,0:T(4,128)(2,1)S(1)}, bf16[3,256]{1,0:T(4,128)(2,1)}, u32[]{:S(2)}) copy-start(bf16[3,256]{1,0:T(4,128)(2,1)} %taps.1) | copy-start | bytes 4612
  96.4 12.1 %collective-permute-start = (bf16[8,80,256]{2,1,0:T(8,128)(2,1)S(1)}, bf16[8,80,256]{2,1,0:T(8,128)(2,1)S(1)}, u32[]{:S(2)}, u32[]{:S(2)}) collective-permute-start(bf16[8,80,256]{2,1,0:T(8,128)(2,1)S(1)} %get-tuple-element.32), channel_id=1, source_target_pairs={{0,248},{8,0},{16,8},{24,16},{32,24},{40,32},{48,40},{56,48},{64,5... | collective-permute-start | bytes 983048 | tf_op jit(solution)/shard_map/ppermute | solution.py:423
  101.5 10.7 %collective-permute-start.1 = (bf16[8,80,256]{2,1,0:T(8,128)(2,1)S(1)}, bf16[8,80,256]{2,1,0:T(8,128)(2,1)S(1)}, u32[]{:S(2)}, u32[]{:S(2)}) collective-permute-start(bf16[8,80,256]{2,1,0:T(8,128)(2,1)S(1)} %get-tuple-element.31), channel_id=1, source_target_pairs={{0,8},{8,16},{16,24},{24,32},{32,40},{40,48},{48,56},{56,64},{64,7... | collective-permute-start | bytes 983048 | tf_op jit(solution)/shard_map/ppermute | solution.py:424
  160.8 8.1 %all-to-all-start.4 = ((bf16[4,32,128]{2,1,0:T(8,128)(2,1)}), bf16[4,32,128]{2,1,0:T(8,128)(2,1)S(1)}, u32[]{:S(2)}, u32[]{:S(2)}) async-start(bf16[4,32,128]{2,1,0:T(8,128)(2,1)} %far.1), calls=%async_computation.4 | async-start | bytes 65536 | tf_op jit(solution)/shard_map/all_to_all | solution.py:373
  164.2 4.7 %collective-permute-start.2 = (bf16[16,2048]{1,0:T(8,128)(2,1)S(1)}, bf16[16,2048]{1,0:T(8,128)(2,1)S(1)}, u32[]{:S(2)}, u32[]{:S(2)}) collective-permute-start(bf16[16,2048]{1,0:T(8,128)(2,1)S(1)} %get-tuple-element.21), channel_id=1, source_target_pairs={{0,8},{8,16},{16,24},{24,32},{32,40},{40,48},{48,56},{56,64},{64,7... | collective-permute-start | bytes 196616 | tf_op jit(solution)/shard_map/ppermute | solution.py:460
  186.5 3.8 %collective-permute-start.3 = (bf16[2,512,256]{2,1,0:T(8,128)(2,1)S(1)}, bf16[2,512,256]{2,1,0:T(8,128)(2,1)S(1)}, u32[]{:S(2)}, u32[]{:S(2)}) collective-permute-start(bf16[2,512,256]{2,1,0:T(8,128)(2,1)S(1)} %branch.1.after.mine), channel_id=1, source_target_pairs={{0,4},{4,0},{1,5},{5,1},{2,6},{6,2},{3,7},{7,3},{8,12},{12,8},{9,1... | collective-permute-start | bytes 1572872 | tf_op jit(solution)/shard_map/ppermute | solution.py:503
Sparse Core Ops, SparseCore 0:
  9.5 169.9 all-gather.1

commit v8 on v7

--- a/solution.py
+++ b/solution.py
@@ -279,7 +279,7 @@
         )
         for i in range(early, blocks)
     ]
-    for copy in (*copies, *x_copies):
+    for copy in copies:
         copy.start()
     incoming = jnp.concatenate([base[at].astype(F32) for at in range(base.shape[0])], axis=0)
     state = fade[0:1, :] * incoming + before[...]
@@ -293,8 +293,12 @@
     first = jnp.zeros((BLOCK, PROJECTED), F32)
     for at in range(PIECES):
         copies[at].wait()
+        if at == PIECES // 2:
+            x_copies[0].start()
         cut = slice(at * piece, (at + 1) * piece)
         first = first + dot(block_rows(x_early, 0)[:, cut], weight[cut, :], ((1,), (0,)))
+    for copy in x_copies[1:]:
+        copy.start()
     rim = dot(halo[...], weight[:, HEAD : 3 * HEAD], ((1,), (0,))).astype(BF16).astype(F32)
     tail = (rim[:, :HEAD] * rim[:, HEAD:])[RIM - 8 :]
     for i in range(rows // BLOCK):

time: 231 us -> 231 us (level)
  no operation moved by 1% of the time
where the time goes in v8:
time: 231 us; the launch traced here: 230 us
  blocking collectives  108 us (47%)
  starting transfers between devices  65.5 us (28%)
  Pallas kernels  22.1 us (10%)
  waiting for transfers between devices  20 us (9%)
  between operations  13.5 us (6%)
    all_to_all x3, blocking collectives, exchanged(): return lax.all_to_all(x, axes, 0, 0, tiled=True)  72.6 us
    all_to_all x3, starting transfers between devices, exchanged(): return lax.all_to_all(x, axes, 0, 0, tiled=True)  52.8 us
    all_gather x1, blocking collectives, body(): same = lax.all_gather(own.reshape(2 * (shard + EXTRA), 2 * HEAD), FAR)  35.3 us
    pallas_call x9, Pallas kernels, run(): pl.pallas_call(kernel, out_shape=[o[0] for o in outs], in_specs=in_specs,...  22.1 us
    all_gather x1, waiting for transfers between devices, body(): weights = lax.all_gather(rest, STRETCHES, axis=0, tiled=True)  10.6 us
    ppermute x1, starting transfers between devices, body(): lax.ppermute(same[:half], CHIPS, [(i, (i - 1) % chips) for i in range(chi...  5.13 us
  transfers between devices with their start and end apart: 8, of which 4 were waited for; matrix products, arithmetic and copies ran while one was open for 0% of the time, Pallas kernels for 5%

profile of v8, /device:TPU:33, one launch (start us, length us, event | category | flops | bytes accessed | tf_op | source)
XLA Modules:
  0.0 229.9 jit_solution(18129386365736220980)
XLA Ops:
  6.5 0.0 all-gather.2.cloned.1.call-start
  6.6 1.5 pack.1
  8.1 0.1 all-gather.2.cloned.1.call-update
  8.1 44.7 %all-to-all-start.1 = ((bf16[2,40,256]{2,1,0:T(8,128)(2,1)}), bf16[2,40,256]{2,1,0:T(8,128)(2,1)S(1)}, u32[]{:S(2)}, u32[]{:S(2)}) async-start(bf16[2,40,256]{2,1,0:T(8,128)(2,1)} %get-tuple-element.19), calls=%async_computation.1 | async-start | bytes 81920 | tf_op jit(solution)/shard_map/all_to_all | solution.py:377
  52.9 3.5 %norm.1 = bf16[8,128,2048]{2,1,0:T(8,128)(2,1)} custom-call(bf16[128,2048]{1,0:T(8,128)(2,1)} %tokens.1, bf16[2048]{0:T(1024)(128)(2,1)} %gain.1), custom_call_target="tpu_custom_call" | custom-call | tf_op jit(solution)/shard_map/norm/pallas_call | solution.py:38
  56.4 0.0 all-to-all-done.1.own
  56.4 4.6 %all-to-all-start = ((bf16[8,128,2048]{2,1,0:T(8,128)(2,1)}), bf16[8,128,2048]{2,1,0:T(8,128)(2,1)}, u32[]{:S(2)}, u32[]{:S(2)}) async-start(bf16[8,128,2048]{2,1,0:T(8,128)(2,1)} %norm.1), calls=%async_computation | async-start | bytes 8388608 | tf_op jit(solution)/shard_map/all_to_all | solution.py:377
  61.0 35.3 %all_gather.7.same = bf16[16,80,256]{2,1,0:T(8,128)(2,1)S(1)} all-gather(bf16[1,80,256]{2,1,0:T(8,128)(2,1)S(1)} %bitcast.8), channel_id=1, replica_groups=mesh['grp'=2,'za'=8,'zb'=2,'zc'=2,'core'=2,'tp'=4] {'za','zb'}, dimensions={0}, use_global_device_ids=true | all-gather | bytes 696320 | tf_op jit(solution)/shard_map/all_gather | solution.py:425
  96.4 0.0 copy-start
  96.4 5.1 %collective-permute-start = (bf16[8,80,256]{2,1,0:T(8,128)(2,1)S(1)}, bf16[8,80,256]{2,1,0:T(8,128)(2,1)S(1)}, u32[]{:S(2)}, u32[]{:S(2)}) collective-permute-start(bf16[8,80,256]{2,1,0:T(8,128)(2,1)S(1)} %get-tuple-element.32), channel_id=1, source_target_pairs={{0,248},{8,0},{16,8},{24,16},{32,24},{40,32},{48,40},{56,48},{64,5... | collective-permute-start | bytes 983048 | tf_op jit(solution)/shard_map/ppermute | solution.py:427
  101.5 2.0 collective-permute-start.1
  103.5 0.1 pad_maximum_fusion
  103.6 0.1 multiply_sine_fusion
  103.7 0.5 fusion
  104.2 4.2 %collective-permute-done.low = bf16[8,80,256]{2,1,0:T(8,128)(2,1)S(1)} collective-permute-done((bf16[8,80,256]{2,1,0:T(8,128)(2,1)S(1)}, bf16[8,80,256]{2,1,0:T(8,128)(2,1)S(1)}, u32[]{:S(2)}, u32[]{:S(2)}) %collective-permute-start) | collective-permute-done | bytes 327712 | tf_op jit(solution)/shard_map/ppermute | solution.py:427
  108.5 3.8 %collective-permute-done.1.high = bf16[8,80,256]{2,1,0:T(8,128)(2,1)S(1)} collective-permute-done((bf16[8,80,256]{2,1,0:T(8,128)(2,1)S(1)}, bf16[8,80,256]{2,1,0:T(8,128)(2,1)S(1)}, u32[]{:S(2)}, u32[]{:S(2)}) %collective-permute-start.1) | collective-permute-done | bytes 327712 | tf_op jit(solution)/shard_map/ppermute | solution.py:428
  112.3 0.0 all-to-all-done.x.x_far
  112.3 5.4 %kv.1 = (bf16[1024,128]{1,0:T(8,128)(2,1)S(1)}, bf16[1024,128]{1,0:T(8,128)(2,1)S(1)}, f32[8,128]{1,0:T(8,128)S(1)}, f32[128,128]{1,0:T(8,128)S(1)}, f32[32,128]...) custom-call(s32[1]{0:T(128)} %bitcast.4.pair, ...), custom_call_target="tpu_custom_call" | custom-call | flops 1073741824 | tf_op jit(solution)/shard_map/kv/pallas_call | solution.py:38
  117.7 8.0 %all_to_all.30.gathered = bf16[4,128,128]{2,1,0:T(8,128)(2,1)S(1)} all-to-all(bf16[4,128,128]{2,1,0:T(8,128)(2,1)S(1)} %get-tuple-element.27), channel_id=1, replica_groups=mesh['grp'=2,'za'=8,'zb'=2,'zc'=2,'core'=2,'tp'=4] {'zb','zc'}, dimensions={0} | all-to-all | bytes 262144 | tf_op jit(solution)/shard_map/all_to_all | solution.py:377
  125.7 34.4 %all_to_all.31.gathered = bf16[8,32,128]{2,1,0:T(8,128)(2,1)S(1)} all-to-all(bf16[8,32,128]{2,1,0:T(8,128)(2,1)S(1)} %get-tuple-element.28), channel_id=1, replica_groups=mesh['grp'=2,'za'=8,'zb'=2,'zc'=2,'core'=2,'tp'=4] {'za'}, dimensions={0} | all-to-all | bytes 131072 | tf_op jit(solution)/shard_map/all_to_all | solution.py:377
  160.1 0.6 far.1
  160.8 3.4 %all-to-all-start.4 = ((bf16[4,32,128]{2,1,0:T(8,128)(2,1)}), bf16[4,32,128]{2,1,0:T(8,128)(2,1)S(1)}, u32[]{:S(2)}, u32[]{:S(2)}) async-start(bf16[4,32,128]{2,1,0:T(8,128)(2,1)} %far.1), calls=%async_computation.4 | async-start | bytes 65536 | tf_op jit(solution)/shard_map/all_to_all | solution.py:377
  164.2 3.4 %collective-permute-start.2 = (bf16[16,2048]{1,0:T(8,128)(2,1)S(1)}, bf16[16,2048]{1,0:T(8,128)(2,1)S(1)}, u32[]{:S(2)}, u32[]{:S(2)}) collective-permute-start(bf16[16,2048]{1,0:T(8,128)(2,1)S(1)} %get-tuple-element.21), channel_id=1, source_target_pairs={{0,8},{8,16},{16,24},{24,32},{32,40},{40,48},{48,56},{56,64},{64,7... | collective-permute-start | bytes 196616 | tf_op jit(solution)/shard_map/ppermute | solution.py:464
  167.6 1.3 collective-permute-done.2.halo
  168.9 0.0 all-to-all-done.4.base
  168.9 10.6 %all-gather.2.cloned.1.call-done.weights = bf16[2048,1792]{1,0:T(8,128)(2,1)} async-done(((bf16[32,1792]{1,0:T(8,128)(2,1)}), bf16[2048,1792]{1,0:T(8,128)(2,1)}) %all-gather.2.cloned.1.call-update) | async-done | bytes 7340048 | tf_op jit(solution)/shard_map/all_gather | solution.py:422
  179.5 0.0 copy-done
  179.5 7.1 %branch.1.after.mine = bf16[2,512,256]{2,1,0:T(8,128)(2,1)S(1)} custom-call(s32[1]{0:T(128)} %bitcast.core, bf16[2048,1792]{1,0:T(8,128)(2,1)} %all-gather.2.cloned.1.call-done.weights, bf16[8,128,2048]{2,1,0:T(8,128)(2,1)} %all-to-all-done.x.x_far, bf16[2,128,2048]{2,1,0:T(8,128)(2,1)S(1)} %get-tuple-element.20.x_early, ...), custom_call_target="tpu_custom_call" | custom-call | flops 2684354560 | tf_op jit(solution)/shard_map/branch/pallas_call | solution.py:38
  186.6 2.2 collective-permute-start.3
  188.8 1.6 fetch.1.weight
  190.4 0.0 collective-permute-done.3.theirs
  190.4 1.3 out.1
  191.7 30.3 %all_to_all.32.parts = bf16[4,128,2048]{2,1,0:T(8,128)(2,1)S(1)} all-to-all(bf16[4,128,2048]{2,1,0:T(8,128)(2,1)S(1)} %out.1), channel_id=1, replica_groups=mesh['grp'=2,'za'=8,'zb'=2,'zc'=2,'core'=2,'tp'=4] {'tp'}, dimensions={0} | all-to-all | bytes 4194304 | tf_op jit(solution)/shard_map/all_to_all | solution.py:377
  222.0 1.0 sum.1
  (4 shorter events, 0.1 us)
Async XLA Ops:
  6.5 172.9 %all-gather.2.cloned.1.call-start = ((), (), s32[]{:S(2)}) async-start(), calls=%async_computation.6 | async-start | bytes 7454720 | tf_op jit(solution)/shard_map/all_gather | solution.py:422
  8.1 48.3 %all-to-all-start.1 = ((bf16[2,40,256]{2,1,0:T(8,128)(2,1)}), bf16[2,40,256]{2,1,0:T(8,128)(2,1)S(1)}, u32[]{:S(2)}, u32[]{:S(2)}) async-start(bf16[2,40,256]{2,1,0:T(8,128)(2,1)} %get-tuple-element.19), calls=%async_computation.1 | async-start | bytes 81920 | tf_op jit(solution)/shard_map/all_to_all | solution.py:377
  56.4 55.9 %all-to-all-start = ((bf16[8,128,2048]{2,1,0:T(8,128)(2,1)}), bf16[8,128,2048]{2,1,0:T(8,128)(2,1)}, u32[]{:S(2)}, u32[]{:S(2)}) async-start(bf16[8,128,2048]{2,1,0:T(8,128)(2,1)} %norm.1), calls=%async_computation | async-start | bytes 8388608 | tf_op jit(solution)/shard_map/all_to_all | solution.py:377
  96.4 83.1 %copy-start = (bf16[3,256]{1,0:T(4,128)(2,1)S(1)}, bf16[3,256]{1,0:T(4,128)(2,1)}, u32[]{:S(2)}) copy-start(bf16[3,256]{1,0:T(4,128)(2,1)} %taps.1) | copy-start | bytes 4612
  96.4 12.1 %collective-permute-start = (bf16[8,80,256]{2,1,0:T(8,128)(2,1)S(1)}, bf16[8,80,256]{2,1,0:T(8,128)(2,1)S(1)}, u32[]{:S(2)}, u32[]{:S(2)}) collective-permute-start(bf16[8,80,256]{2,1,0:T(8,128)(2,1)S(1)} %get-tuple-element.32), channel_id=1, source_target_pairs={{0,248},{8,0},{16,8},{24,16},{32,24},{40,32},{48,40},{56,48},{64,5... | collective-permute-start | bytes 983048 | tf_op jit(solution)/shard_map/ppermute | solution.py:427
  101.5 10.7 %collective-permute-start.1 = (bf16[8,80,256]{2,1,0:T(8,128)(2,1)S(1)}, bf16[8,80,256]{2,1,0:T(8,128)(2,1)S(1)}, u32[]{:S(2)}, u32[]{:S(2)}) collective-permute-start(bf16[8,80,256]{2,1,0:T(8,128)(2,1)S(1)} %get-tuple-element.31), channel_id=1, source_target_pairs={{0,8},{8,16},{16,24},{24,32},{32,40},{40,48},{48,56},{56,64},{64,7... | collective-permute-start | bytes 983048 | tf_op jit(solution)/shard_map/ppermute | solution.py:428
  160.8 8.1 %all-to-all-start.4 = ((bf16[4,32,128]{2,1,0:T(8,128)(2,1)}), bf16[4,32,128]{2,1,0:T(8,128)(2,1)S(1)}, u32[]{:S(2)}, u32[]{:S(2)}) async-start(bf16[4,32,128]{2,1,0:T(8,128)(2,1)} %far.1), calls=%async_computation.4 | async-start | bytes 65536 | tf_op jit(solution)/shard_map/all_to_all | solution.py:377
  164.2 4.7 %collective-permute-start.2 = (bf16[16,2048]{1,0:T(8,128)(2,1)S(1)}, bf16[16,2048]{1,0:T(8,128)(2,1)S(1)}, u32[]{:S(2)}, u32[]{:S(2)}) collective-permute-start(bf16[16,2048]{1,0:T(8,128)(2,1)S(1)} %get-tuple-element.21), channel_id=1, source_target_pairs={{0,8},{8,16},{16,24},{24,32},{32,40},{40,48},{48,56},{56,64},{64,7... | collective-permute-start | bytes 196616 | tf_op jit(solution)/shard_map/ppermute | solution.py:464
  186.6 3.8 %collective-permute-start.3 = (bf16[2,512,256]{2,1,0:T(8,128)(2,1)S(1)}, bf16[2,512,256]{2,1,0:T(8,128)(2,1)S(1)}, u32[]{:S(2)}, u32[]{:S(2)}) collective-permute-start(bf16[2,512,256]{2,1,0:T(8,128)(2,1)S(1)} %branch.1.after.mine), channel_id=1, source_target_pairs={{0,4},{4,0},{1,5},{5,1},{2,6},{6,2},{3,7},{7,3},{8,12},{12,8},{9,1... | collective-permute-start | bytes 1572872 | tf_op jit(solution)/shard_map/ppermute | solution.py:507
Sparse Core Ops, SparseCore 0:
  9.5 169.9 all-gather.1
